TPU v7x, 512 devices: a whole 4x4x16 slice. The times are simulated.
512 devices in a mesh: sp: 16 (over z), fs: 4 (over y), tp: 8 (over x, core).
Axes of the slice: x: 4, y: 4, z: 16, core: 2. Of those that a mesh axis runs over, the one named last changes fastest.
Arguments:
- tokens: bfloat16 [4, 4096, 2048], P('fs', 'sp'), may hold values from -6 to 6
- norm_gain: float32 [2048], replicated, may hold values from 0.1 to 1.9
- query_weight: bfloat16 [2048, 1024], P(('sp', 'fs'), 'tp'), may hold values from -0.125 to 0.125
- key_weight: bfloat16 [2048, 1024], P(('sp', 'fs'), 'tp'), may hold values from -0.125 to 0.125
- value_weight: bfloat16 [2048, 1024], P(('sp', 'fs'), 'tp'), may hold values from -0.125 to 0.125
- outgate_weight: bfloat16 [2048, 1024], P(('sp', 'fs'), 'tp'), may hold values from -0.125 to 0.125
- gate_weight: bfloat16 [4, 8, 2048], P(None, 'tp'), may hold values from -0.125 to 0.125
- gate_bias: float32 [4, 8], P(None, 'tp'), may hold values from -1 to 100
- decay_extra: float32 [4, 2, 8, 4096], P('fs', None, 'tp', 'sp'), may hold values from -0.75 to 0
- init_memory: float32 [4, 2, 8, 128, 128], P('fs', None, 'tp'), may hold values from -96 to 96
- init_normalizer: float32 [4, 2, 8, 128], P('fs', None, 'tp'), may hold values from -96 to 96
- head_gain: float32 [8, 128], P('tp'), may hold values from 0.1 to 1.9
- pool_weight: bfloat16 [2048, 2048], P(('sp', 'fs'), 'tp'), may hold values from -0.125 to 0.125
- mem_out_weight: bfloat16 [2048, 1024], P(('sp', 'fs'), 'tp'), may hold values from -0.1875 to 0.1875
- pool_out_weight: bfloat16 [2048, 2048], P(('sp', 'fs'), 'tp'), may hold values from -0.125 to 0.125
Outputs:
- mixed: bfloat16 [4, 4096, 2048], P('fs', ('sp', 'tp'))
All inputs are finite; a program needn't handle non-finite values.
Results may differ from a plain program's by a relative error of at most 0.014.
Values may be sent and summed in bfloat16 or wider, within the bound.
No kernel may reach another device: no remote copies, remote signals or barrier semaphores. Data moves between devices by JAX's collectives and lax.ppermute only.
A program may use at most 64 MiB of HBM per device.

v0:
```python
import math

import jax
import jax.numpy as jnp
from jax import lax
from jax.sharding import PartitionSpec as P

HALO = 8


norm_eps = 1e-06
exact_mode = lax.Precision.HIGHEST


def in_one_piece(arrays, axis, dim, along):
    widths = [a.shape[along] for a in arrays]
    both = jnp.concatenate(arrays, axis=along)
    out = lax.all_gather(both, axis, axis=dim, tiled=True)
    return tuple(jnp.split(out, [sum(widths[:k]) for k in range(1, len(widths))], axis=along))


def from_everyone(x, axis):
    copies = jnp.broadcast_to(x, (lax.axis_size(axis), *x.shape))
    return lax.all_to_all(copies, axis, split_axis=0, concat_axis=0, tiled=True)


def collected_together(x, axis):
    leaves = jax.tree.leaves(x)
    order = sorted(range(len(leaves)), key=lambda k: -leaves[k].size)
    width = (1, *leaves[order[0]].shape)[-1]
    lines = [
        jnp.pad(leaves[k].reshape(-1), (0, -leaves[k].size % width)).reshape(-1, width)
        for k in order
    ]
    both, at, found = (from_everyone(jnp.concatenate(lines), axis), 0, {})
    for k, line in zip(order, lines):
        section = both[:, at : at + len(line)].reshape(len(both), -1)
        found[k] = section[:, : leaves[k].size].reshape(-1, *leaves[k].shape)
        at += len(line)
    numbers = iter(range(len(leaves)))
    return jax.tree.map(lambda _: found[next(numbers)], x)


def combined_pairwise(pieces, combine):
    while len(jax.tree.leaves(pieces)[0]) > 1:
        pieces = jax.vmap(combine)(
            *(jax.tree.map(lambda part: part[side::2], pieces) for side in (0, 1))
        )
    return jax.tree.map(lambda part: part[0], pieces)


def carried_in(x, axis, combine, identity):
    length, position = (lax.axis_size(axis), lax.axis_index(axis))
    passed = jnp.arange(length) < position

    def kept(part, zero, own):
        part = jnp.where(
            passed.reshape(-1, *(1 for _ in own.shape)), part, jnp.asarray(zero, own.dtype)
        )
        return part

    pieces = collected_together(x, axis)
    return combined_pairwise(jax.tree.map(kept, pieces, identity, x), combine)


def collected_together_2(x, axis):
    leaves = jax.tree.leaves(x)
    order = sorted(range(len(leaves)), key=lambda k: -leaves[k].size)
    width = (1, *leaves[order[0]].shape)[-1]
    lines = [
        jnp.pad(leaves[k].reshape(-1), (0, -leaves[k].size % width)).reshape(-1, width)
        for k in order
    ]
    both, at, found = (lax.all_gather(jnp.concatenate(lines), axis), 0, {})
    for k, line in zip(order, lines):
        section = both[:, at : at + len(line)].reshape(len(both), -1)
        found[k] = section[:, : leaves[k].size].reshape(-1, *leaves[k].shape)
        at += len(line)
    numbers = iter(range(len(leaves)))
    return jax.tree.map(lambda _: found[next(numbers)], x)


def entering(x, axis, combine, identity):
    length, position = (lax.axis_size(axis), lax.axis_index(axis))
    everything = collected_together_2(x, axis)
    start = jax.tree.map(
        lambda part, zero: jnp.broadcast_to(jnp.asarray(zero, part.dtype), part.shape), x, identity
    )

    def lap(k, before):
        at = length - 1 - k
        reached = at > position
        new = combine(before, jax.tree.map(lambda part: part[at], everything))
        return jax.tree.map(lambda a, b: jnp.where(reached, a, b), new, before)

    return lax.fori_loop(0, length, lap, start)


def padded_2(block, sides, width):
    for axis, dim in sides:
        count = lax.axis_size(axis)
        forward = [(i, i + 1) for i in range(count - 1)]
        backward = [(target, source) for source, target in forward]
        low = lax.ppermute(
            lax.slice_in_dim(block, block.shape[dim] - width, None, axis=dim), axis, forward
        )
        high = lax.ppermute(lax.slice_in_dim(block, 0, width, axis=dim), axis, backward)
        block = jnp.concatenate([low, block, high], axis=dim)
    return block


def in_blocks(x, dim, length):
    dims = x.shape
    parts = x.reshape(*dims[:dim], length, dims[dim] // length, *dims[dim + 1 :])
    return jnp.moveaxis(parts, dim, 0)


def sum_at_owner(x, axis, dim):
    length = lax.axis_size(axis)
    parts = lax.all_to_all(in_blocks(x, dim, length), axis, 0, 0, tiled=True)
    return jnp.sum(parts.astype(jnp.float32), axis=0)


def block_output(
    query_rows, key_rows, value_rows, input_gate, log_forget, memory, normalizer, stabilizer
):
    block_len = query_rows.shape[1]
    key_scale = key_rows.shape[-1] ** (-0.5)
    lower_mask = jnp.tril(jnp.ones((block_len, block_len), dtype=bool))
    summed = jnp.cumsum(log_forget, axis=-1)
    log_decay = jnp.where(
        lower_mask, summed[:, :, None] - summed[:, None, :] + input_gate[:, None, :], -jnp.inf
    )
    log_carry = stabilizer[:, None] + summed
    running_max = jnp.maximum(log_carry, jnp.max(log_decay, axis=-1))
    scores = (
        jnp.einsum("btd,bsd->bts", query_rows, key_rows, preferred_element_type=jnp.float32)
        * key_scale
    )
    inner_weight = jnp.exp(log_decay - running_max[:, :, None]) * scores
    weight_rounded = inner_weight.astype(jnp.bfloat16)
    carry_weight = jnp.exp(log_carry - running_max)
    query_wide = query_rows.astype(jnp.float32)
    numerator = carry_weight[:, :, None] * jnp.einsum(
        "bed,btd->bte", memory, query_wide, precision=exact_mode
    )
    numerator = numerator + jnp.einsum(
        "bts,bse->bte", weight_rounded, value_rows, preferred_element_type=jnp.float32
    )
    denominator = carry_weight * jnp.einsum(
        "bd,btd->bt", normalizer, query_wide, precision=exact_mode
    )
    denominator = denominator + jnp.sum(inner_weight, axis=-1)
    return numerator / jnp.maximum(jnp.abs(denominator), jnp.exp(-running_max))[:, :, None]


def block_summary(key_rows, value_rows, input_gate, log_forget):
    key_wide = key_rows.astype(jnp.float32) * key_rows.shape[-1] ** (-0.5)
    summed = jnp.cumsum(log_forget, axis=-1)
    forget_total = summed[:, -1]
    log_weight = forget_total[:, None] - summed + input_gate
    running_max = jnp.max(log_weight, axis=-1)
    weights = jnp.exp(log_weight - running_max[:, None])
    memory = jnp.einsum(
        "bse,bsd->bed",
        weights[:, :, None] * value_rows.astype(jnp.float32),
        key_wide,
        precision=exact_mode,
    )
    normalizer = jnp.einsum("bs,bsd->bd", weights, key_wide, precision=exact_mode)
    return (memory, normalizer, running_max, forget_total)


def combine(earlier, latter):
    early_memory, early_norm, early_max, early_total = earlier
    late_memory, late_norm, late_max, late_total = latter
    joint_max = jnp.maximum(early_max + late_total, late_max)
    early_scale = jnp.exp(early_max + late_total - joint_max)
    late_scale = jnp.exp(late_max - joint_max)
    memory = early_scale[:, None, None] * early_memory + late_scale[:, None, None] * late_memory
    normalizer = early_scale[:, None] * early_norm + late_scale[:, None] * late_norm
    return (memory, normalizer, joint_max, early_total + late_total)


def span_sweep(
    query_rows, key_rows, value_rows, input_gate, log_forget, memory, normalizer, stabilizer, span
):
    block_count = query_rows.shape[1] // span

    def to_blocks(array):
        shaped = array.reshape((array.shape[0], block_count, span) + array.shape[2:])
        return jnp.moveaxis(shaped, 1, 0)

    def advance(carried, pieces):
        query_blk, key_blk, value_blk, gate_blk, forget_blk = pieces
        result = block_output(
            query_blk, key_blk, value_blk, gate_blk, forget_blk, carried[0], carried[1], carried[2]
        )
        return (combine(carried, block_summary(key_blk, value_blk, gate_blk, forget_blk)), result)

    initial = (memory, normalizer, stabilizer, jnp.zeros_like(stabilizer))
    ignored, outputs = lax.scan(
        advance,
        initial,
        tuple(
            (
                to_blocks(array)
                for array in (query_rows, key_rows, value_rows, input_gate, log_forget)
            )
        ),
    )
    return jnp.moveaxis(outputs, 0, 1).reshape(query_rows.shape[:2] + (value_rows.shape[2],))


def reverse_time(array):
    return jnp.flip(array, axis=1)


def to_heads(matrix, head_count):
    shaped = matrix.reshape(matrix.shape[0], head_count, matrix.shape[1] // head_count)
    return shaped.transpose(1, 0, 2)


def pool_window(padded, positions, channels, seq_len, group_size):
    row_count = positions.shape[0]
    group_index = channels // group_size
    reach_left = jnp.left_shift(jnp.ones_like(group_index), group_index)
    reach_right = reach_left - 1
    window_sum = jnp.zeros((row_count, channels.shape[0]), jnp.float32)
    for offset in range(-HALO, HALO):
        inside = ((offset >= -reach_left) & (offset <= reach_right)).astype(jnp.float32)
        window_sum = window_sum + inside * padded[HALO + offset : HALO + offset + row_count]
    first_pos = jnp.maximum(positions[:, None] - reach_left[None, :], 0)
    last_pos = jnp.minimum(positions[:, None] + reach_right[None, :], seq_len - 1)
    counted = (last_pos - first_pos + 1).astype(jnp.float32)
    centre = padded[HALO : HALO + row_count]
    return (window_sum / counted - centre).astype(jnp.bfloat16)


def per_device(
    tokens,
    norm_gain,
    query_weight,
    key_weight,
    value_weight,
    outgate_weight,
    gate_weight,
    gate_bias,
    decay_extra,
    init_memory,
    init_normalizer,
    head_gain,
    pool_weight,
    mem_out_weight,
    pool_out_weight,
):
    block_len = tokens.shape[1]
    model_width = tokens.shape[2]
    head_count, head_width = head_gain.shape
    span = math.gcd(block_len, 256)
    flattened = tokens[0].astype(jnp.float32)
    normed = (
        flattened
        * lax.rsqrt(jnp.mean(flattened * flattened, axis=-1, keepdims=True) + norm_eps)
        * norm_gain
    ).astype(jnp.bfloat16)
    zero_start = tuple(
        (
            jnp.zeros((block_len, weight.shape[1]), jnp.float32)
            for weight in (query_weight, key_weight, value_weight, outgate_weight, pool_weight)
        )
    )
    zero_start = zero_start + (
        jnp.zeros((model_width, mem_out_weight.shape[1]), jnp.bfloat16),
        jnp.zeros((model_width, pool_out_weight.shape[1]), jnp.bfloat16),
    )
    line_query, line_key, line_value, line_outgate, line_pool, line_mem_out, line_pool_out = (
        in_one_piece(
            (
                query_weight,
                key_weight,
                value_weight,
                outgate_weight,
                pool_weight,
                mem_out_weight,
                pool_out_weight,
            ),
            "fs",
            0,
            1,
        )
    )
    pieces = in_one_piece(
        (line_query, line_key, line_value, line_outgate, line_pool, line_mem_out, line_pool_out),
        "sp",
        0,
        1,
    )
    partial_sums = tuple(
        (
            jnp.dot(normed, weight_rows, preferred_element_type=jnp.float32)
            for weight_rows in pieces[:5]
        )
    )
    collected = tuple((weight_rows for weight_rows in pieces[5:]))
    folded = partial_sums + collected
    query_proj, key_proj, value_proj, outgate, pool_input = tuple(
        (running.astype(jnp.bfloat16) for running in folded[:5])
    )
    mem_weight_all = folded[5]
    pool_weight_all = folded[6]
    gate_pre = lax.dot_general(
        normed,
        gate_weight.reshape(4 * head_count, model_width),
        (((1,), (1,)), ((), ())),
        preferred_element_type=jnp.float32,
    ) + gate_bias.reshape(4 * head_count)
    gate_pre = gate_pre.reshape(block_len, 4, head_count).transpose(1, 2, 0)
    query_heads = to_heads(query_proj, head_count)
    key_heads = to_heads(key_proj, head_count)
    value_heads = to_heads(value_proj, head_count)
    forward_forget = jax.nn.log_sigmoid(gate_pre[1]) + decay_extra[0, 0]
    backward_forget = jax.nn.log_sigmoid(gate_pre[3]) + decay_extra[0, 1]
    zero_rows = jnp.zeros((head_count,), jnp.float32)
    identity = (
        jnp.zeros((head_count, head_width, head_width), jnp.float32),
        jnp.zeros((head_count, head_width), jnp.float32),
        jnp.full((head_count,), -1e30, jnp.float32),
        zero_rows,
    )
    front_memory, front_norm, front_max, front_total = block_summary(
        key_heads, value_heads, gate_pre[0], forward_forget
    )
    prefix = carried_in((front_memory, front_norm, front_max, front_total), "sp", combine, identity)
    incoming = combine((init_memory[0, 0], init_normalizer[0, 0], zero_rows, zero_rows), prefix)
    forward_out = span_sweep(
        query_heads,
        key_heads,
        value_heads,
        gate_pre[0],
        forward_forget,
        incoming[0],
        incoming[1],
        incoming[2],
        span,
    )
    back_query = reverse_time(query_heads)
    back_key = reverse_time(key_heads)
    back_value = reverse_time(value_heads)
    back_gate = reverse_time(gate_pre[2])
    back_forget = reverse_time(backward_forget)
    rear_memory, rear_norm, rear_max, rear_total = block_summary(
        back_key, back_value, back_gate, back_forget
    )
    suffix = entering((rear_memory, rear_norm, rear_max, rear_total), "sp", combine, identity)
    back_incoming = combine(
        (init_memory[0, 1], init_normalizer[0, 1], zero_rows, zero_rows), suffix
    )
    backward_out = reverse_time(
        span_sweep(
            back_query,
            back_key,
            back_value,
            back_gate,
            back_forget,
            back_incoming[0],
            back_incoming[1],
            back_incoming[2],
            span,
        )
    )
    summed_dirs = (forward_out + backward_out).transpose(1, 0, 2)
    normed_heads = (
        summed_dirs
        * lax.rsqrt(jnp.mean(summed_dirs * summed_dirs, axis=-1, keepdims=True) + norm_eps)
        * head_gain
    )
    out_gate = jax.nn.sigmoid(
        outgate.astype(jnp.float32).reshape(block_len, head_count, head_width)
    )
    memory_out = (
        (normed_heads * out_gate).astype(jnp.bfloat16).reshape(block_len, head_count * head_width)
    )
    padded = padded_2(pool_input, (("sp", 0),), HALO).astype(jnp.float32)
    feature_count = pool_input.shape[1]
    positions = lax.axis_index("sp") * block_len + jnp.arange(block_len, dtype=jnp.int32)
    channels = lax.axis_index("tp") * feature_count + jnp.arange(feature_count, dtype=jnp.int32)
    pool_out = pool_window(
        padded, positions, channels, block_len * lax.axis_size("sp"), model_width // 4
    )
    own_rows = block_len // lax.axis_size("tp")
    result = lax.dot_general(
        memory_out, mem_weight_all, (((1,), (1,)), ((), ())), preferred_element_type=jnp.float32
    )
    mixed = sum_at_owner(
        (
            result
            + lax.dot_general(
                pool_out,
                pool_weight_all,
                (((1,), (1,)), ((), ())),
                preferred_element_type=jnp.float32,
            )
        ).astype(jnp.bfloat16),
        "tp",
        0,
    )
    return mixed.astype(jnp.bfloat16).reshape(1, own_rows, model_width)


def solution(mesh):
    placed = (
        P("fs", "sp", None),
        P(),
        P(("sp", "fs"), "tp"),
        P(("sp", "fs"), "tp"),
        P(("sp", "fs"), "tp"),
        P(("sp", "fs"), "tp"),
        P(None, "tp", None),
        P(None, "tp"),
        P("fs", None, "tp", "sp"),
        P("fs", None, "tp", None, None),
        P("fs", None, "tp", None),
        P("tp", None),
        P(("sp", "fs"), "tp"),
        P(("sp", "fs"), "tp"),
        P(("sp", "fs"), "tp"),
    )
    return jax.shard_map(
        per_device,
        mesh=mesh,
        in_specs=placed,
        out_specs=P("fs", ("sp", "tp"), None),
        check_vma=False,
    )
```

profile of v0, /device:TPU:1, one launch (start us, length us, event | category | flops | bytes accessed | tf_op | source)
XLA Modules:
  0.0 331.7 jit_solution(2550282281906693215)
XLA Ops:
  11.6 11.5 %all_gather.12 = bf16[128,1152]{1,0:T(8,128)(2,1)} all-gather(bf16[32,1152]{1,0:T(8,128)(2,1)S(1)} %constant_dynamic-update-slice_fusion), channel_id=1, replica_groups=mesh['sp'=16,'fs'=4,'tp'=8] {'fs'}, dimensions={0}, use_global_device_ids=true | all-gather | bytes 368640 | tf_op jit(solution)/shard_map/all_gather | solution.py:18
  23.2 1.5 fusion.7
  24.8 1.7 fusion.25
  28.1 1.3 fusion.129
  32.8 1.3 fusion.165
  34.1 1.3 pad_bitcast_fusion
  40.8 1.3 subtract_exponential_fusion.1
  42.1 1.4 subtract_exponential_fusion.3
  43.5 57.4 %all-gather.5.cloned.1.call-done = bf16[2048,1152]{1,0:T(8,128)(2,1)} async-done(((bf16[128,1152]{1,0:T(8,128)(2,1)}), bf16[2048,1152]{1,0:T(8,128)(2,1)}) %all-gather.5.cloned.1.call-update) | async-done | bytes 4718608 | tf_op jit(solution)/shard_map/all_gather | solution.py:18
  100.9 1.5 convolution_convert_fusion.3
  102.5 1.5 convolution_convert_fusion.4
  107.7 1.7 convolution_convert_fusion
  109.4 2.5 collective-permute-start
  112.0 1.3 collective-permute-start.1
  113.3 1.5 fusion.90
  115.2 1.5 convolution_convert_fusion.2
  118.0 9.1 %all-to-all-start = ((f32[16,131,128]{2,1,0:T(8,128)}), f32[16,131,128]{2,1,0:T(8,128)S(1)}, u32[]{:S(2)}, u32[]{:S(2)}) async-start(f32[16,131,128]{2,1,0:T(8,128)} %broadcast_in_dim.121), calls=%async_computation | async-start | bytes 2228224 | tf_op jit(solution)/shard_map/all_to_all | solution.py:24
  127.9 66.1 %all-gather.7.cloned.1.call-done = f32[16,131,128]{2,1,0:T(8,128)} async-done(((f32[1,131,128]{2,1,0:T(8,128)}), f32[16,131,128]{2,1,0:T(8,128)}) %all-gather.7.cloned.1.call-update) | async-done | bytes 1073168 | tf_op jit(solution)/shard_map/all_gather | solution.py:74
  194.0 1.6 fusion.173
  195.6 1.3 slice_bitcast_fusion
  196.9 81.6 %while.14 = (s32[]{:T(128)}, f32[1,128,128]{2,1,0:T(8,128)S(1)}, f32[1,128]{1,0:T(1,128)}, f32[1]{0:T(128)}, f32[1]{0:T(128)}, /*index=5*/s32[]{:T(128)}, f32[16...) while((s32[]{:T(128)}, f32[1,128,128]{2,1,0:T(8,128)S(1)}, ...), condition=%wide.region_10.11_spmd.clone, body=%wide.region_9.10_spmd.clone.sunk | while | flops 82575 | bytes 198499 | solution.py:96
  196.9 1.3 constant_dynamic-slice_fusion.4
  200.8 1.2 broadcast_select_fusion.4
  202.0 1.3 constant_dynamic-slice_fusion.4
  205.9 1.2 broadcast_select_fusion.4
  207.1 1.3 constant_dynamic-slice_fusion.4
  211.0 1.2 broadcast_select_fusion.4
  212.2 1.3 constant_dynamic-slice_fusion.4
  216.1 1.2 broadcast_select_fusion.4
  217.3 1.3 constant_dynamic-slice_fusion.4
  221.2 1.2 broadcast_select_fusion.4
  222.4 1.3 constant_dynamic-slice_fusion.4
  226.3 1.2 broadcast_select_fusion.4
  227.5 1.3 constant_dynamic-slice_fusion.4
  232.6 1.3 constant_dynamic-slice_fusion.4
  237.7 1.3 constant_dynamic-slice_fusion.4
  242.8 1.3 constant_dynamic-slice_fusion.4
  247.9 1.3 constant_dynamic-slice_fusion.4
  253.0 1.3 constant_dynamic-slice_fusion.4
  258.1 1.3 constant_dynamic-slice_fusion.4
  262.0 1.2 broadcast_select_fusion.4
  263.2 1.3 constant_dynamic-slice_fusion.4
  267.1 1.2 broadcast_select_fusion.4
  268.3 1.3 constant_dynamic-slice_fusion.4
  273.4 1.3 constant_dynamic-slice_fusion.4
  292.8 2.8 fusion.24
  295.8 2.2 fusion.6
  298.0 26.1 %all_to_all.10 = bf16[8,32,2048]{2,1,0:T(8,128)(2,1)S(1)} all-to-all(bf16[8,32,2048]{2,1,0:T(8,128)(2,1)S(1)} %bitcast.206), channel_id=1, replica_groups=mesh['sp'=16,'fs'=4,'tp'=8] {'tp'}, dimensions={0} | all-to-all | bytes 2097152 | tf_op jit(solution)/shard_map/all_to_all | solution.py:120
  (214 shorter events, 41.7 us)
Async XLA Ops:
  6.5 18.2 %copy-start = (bf16[4,1,2048]{2,0,1:T(4,128)(2,1)S(1)}, bf16[4,1,2048]{2,0,1:T(4,128)(2,1)}, u32[]{:S(2)}) copy-start(bf16[4,1,2048]{2,0,1:T(4,128)(2,1)} %param.23) | copy-start | bytes 49156
  6.5 20.0 %slice-start = ((f32[1,2,1,256]{3,2,1,0:T(1,128)}), f32[1,1,1,256]{3,2,1,0:T(1,128)S(1)}, s32[]{:S(2)}) async-start(f32[1,2,1,256]{3,2,1,0:T(1,128)} %param.25), calls=%async_computation.4 | async-start | bytes 2048 | tf_op jit(solution)/shard_map/slice | solution.py:322
  6.5 21.6 %copy-start.15 = (f32[1,2,1,256]{3,2,1,0:T(1,128)S(1)}, f32[1,2,1,256]{3,2,1,0:T(1,128)}, u32[]{:S(2)}) copy-start(f32[1,2,1,256]{3,2,1,0:T(1,128)} %param.25) | copy-start | bytes 6148
  6.5 94.3 %copy-start.1 = (bf16[1,256,2048]{2,1,0:T(8,128)(2,1)S(1)}, bf16[1,256,2048]{2,1,0:T(8,128)(2,1)}, u32[]{:S(2)}) copy-start(bf16[1,256,2048]{2,1,0:T(8,128)(2,1)} %param.17) | copy-start | bytes 3145732
  6.5 94.3 %copy-start.13 = (f32[2048]{0:T(1024)S(1)}, f32[2048]{0:T(1024)}, u32[]{:S(2)}) copy-start(f32[2048]{0:T(1024)} %param.18) | copy-start | bytes 24580
  6.6 94.3 %all-gather.5.cloned.1.call-start = ((), (), s32[]{:S(2)}) async-start(), calls=%async_computation.2 | async-start | bytes 5013504 | tf_op jit(solution)/shard_map/all_gather | solution.py:18
  23.2 170.8 %all-gather.7.cloned.1.call-start = ((), (), s32[]{:S(2)}) async-start(), calls=%async_computation.3 | async-start | bytes 1183744 | tf_op jit(solution)/shard_map/all_gather | solution.py:74
  24.8 90.5 %copy-start.17 = (f32[256]{0:T(256)}, f32[256]{0:T(256)S(1)}, u32[]{:S(2)}) copy-start(f32[256]{0:T(256)S(1)} %add_rsqrt_fusion.1) | copy-start | bytes 3076
  26.5 79.6 %copy-start.11 = (f32[1,1,256]{2,0,1:T(1,128)}, f32[1,1,256]{2,0,1:T(1,128)S(1)}, u32[]{:S(2)}) copy-start(f32[1,1,256]{2,0,1:T(1,128)S(1)} %get-tuple-element.424) | copy-start | bytes 3076
  27.4 79.6 %copy-start.10 = (f32[1,256]{1,0:T(1,128)}, f32[1,256]{1,0:T(1,128)S(1)}, u32[]{:S(2)}) copy-start(f32[1,256]{1,0:T(1,128)S(1)} %rev.16) | copy-start | bytes 3076
  43.5 62.6 %copy-start.8 = (f32[256]{0:T(256)}, f32[256]{0:T(256)S(1)}, u32[]{:S(2)}) copy-start(f32[256]{0:T(256)S(1)} %get-tuple-element.409) | copy-start | bytes 3076
  102.4 12.3 %copy-start.3 = (bf16[256,128]{1,0:T(8,128)(2,1)}, bf16[256,128]{1,0:T(8,128)(2,1)S(1)}, u32[]{:S(2)}) copy-start(bf16[256,128]{1,0:T(8,128)(2,1)S(1)} %convolution_convert_fusion.3) | copy-start | bytes 196612
  104.2 5.3 %copy-start.5 = (bf16[256,128]{1,0:T(8,128)(2,1)}, bf16[256,128]{1,0:T(8,128)(2,1)S(1)}, u32[]{:S(2)}) copy-start(bf16[256,128]{1,0:T(8,128)(2,1)S(1)} %reverse.13) | copy-start | bytes 196612
  107.0 8.3 %copy-start.7 = (f32[256]{0:T(256)}, f32[256]{0:T(256)S(1)}, u32[]{:S(2)}) copy-start(f32[256]{0:T(256)S(1)} %bitcast_add_fusion.3) | copy-start | bytes 3076
  109.4 17.6 %collective-permute-start = (bf16[8,256]{1,0:T(8,128)(2,1)S(1)}, bf16[8,256]{1,0:T(8,128)(2,1)S(1)}, u32[]{:S(2)}, u32[]{:S(2)}) collective-permute-start(bf16[8,256]{1,0:T(8,128)(2,1)S(1)} %get-tuple-element.420), channel_id=1, source_target_pairs={{0,32},{32,64},{64,96},{96,128},{128,160},{160,192},{192,224},{224... | collective-permute-start | bytes 12296 | tf_op jit(solution)/shard_map/ppermute | solution.py:104
  112.0 15.2 %collective-permute-start.1 = (bf16[8,256]{1,0:T(8,128)(2,1)S(1)}, bf16[8,256]{1,0:T(8,128)(2,1)S(1)}, u32[]{:S(2)}, u32[]{:S(2)}) collective-permute-start(bf16[8,256]{1,0:T(8,128)(2,1)S(1)} %get-tuple-element.421), channel_id=1, source_target_pairs={{32,0},{64,32},{96,64},{128,96},{160,128},{192,160},{224,192},{256... | collective-permute-start | bytes 12296 | tf_op jit(solution)/shard_map/ppermute | solution.py:107
  118.0 166.1 %all-to-all-start = ((f32[16,131,128]{2,1,0:T(8,128)}), f32[16,131,128]{2,1,0:T(8,128)S(1)}, u32[]{:S(2)}, u32[]{:S(2)}) async-start(f32[16,131,128]{2,1,0:T(8,128)} %broadcast_in_dim.121), calls=%async_computation | async-start | bytes 2228224 | tf_op jit(solution)/shard_map/all_to_all | solution.py:24
  278.5 5.6 %copy-start.19 = (pred[16]{0:T(512)(128)(4,1)S(1)}, pred[16]{0:T(512)(128)(4,1)}, u32[]{:S(2)}) copy-start(pred[16]{0:T(512)(128)(4,1)} %iota_compare_fusion.2) | copy-start | bytes 52
  289.9 1.0 copy-start.9
  289.9 1.0 copy-start.16
  290.0 1.0 copy-start.4
  290.0 1.0 copy-start.12
  290.1 1.1 copy-start.20
  290.1 1.3 copy-start.6
  290.1 2.4 copy-start.14
  290.2 2.4 copy-start.18
  290.2 2.4 copy-start.39
  292.6 3.0 copy-start.2
  292.6 3.0 copy-start.21
  292.6 3.0 copy-start.22
  292.6 3.0 copy-start.23
  292.6 3.0 copy-start.24
  292.6 3.0 copy-start.25
  292.6 3.0 copy-start.26
  292.6 3.0 copy-start.27
  292.7 3.0 copy-start.28
  292.7 3.0 copy-start.29
  292.7 3.0 copy-start.30
  292.7 3.0 copy-start.31
  292.7 3.0 copy-start.32
  292.7 3.0 copy-start.33
  292.7 3.0 copy-start.34
  292.7 3.0 copy-start.35
  292.7 3.0 copy-start.36
  292.7 3.0 copy-start.37
  292.8 3.0 copy-start.38
  292.8 3.0 copy-start.40
Sparse Core Ops, SparseCore 0:
  23.3 77.5 all-gather.4
  105.6 88.3 all-gather.6
where the time goes:
time: 334 us; the launch traced here: 332 us
  waiting for transfers between devices  124 us (37%)
  loops' own time  42.5 us (13%)
  other arithmetic  39.5 us (12%)
  blocking collectives  37.6 us (11%)
  local copies, waits for them, and re-layouts  36.1 us (11%)
  matrix products  21 us (6%)
  between operations  18.4 us (6%)
  starting transfers between devices  13 us (4%)
    all_gather x1, waiting for transfers between devices, collected_together_2(): both, at, found = (lax.all_gather(jnp.concatenate(lines), axis), 0, {})  66.1 us
    all_gather x1, waiting for transfers between devices, in_one_piece(): out = lax.all_gather(both, axis, axis=dim, tiled=True)  57.4 us
    another operation x1, loops' own time, entering(): return lax.fori_loop(0, length, lap, start)  42.5 us
    all_to_all x1, blocking collectives, sum_at_owner(): parts = lax.all_to_all(in_blocks(x, dim, length), axis, 0, 0, tiled=True)  26.1 us
    dynamic_slice x16, local copies, waits for them, and re-layouts, lap(): new = combine(before, jax.tree.map(lambda part: part[at], everything))  20.4 us
    select_n x32, other arithmetic, lap(): return jax.tree.map(lambda a, b: jnp.where(reached, a, b), new, before)  18.7 us
    all_gather x1, blocking collectives, in_one_piece(): out = lax.all_gather(both, axis, axis=dim, tiled=True)  11.5 us
    all_to_all x1, starting transfers between devices, from_everyone(): return lax.all_to_all(copies, axis, split_axis=0, concat_axis=0, tiled=True)  9.1 us
  transfers between devices with their start and end apart: 5, of which 2 were waited for; matrix products, arithmetic and copies ran while one was open for 23% of the time, Pallas kernels for 0%

commit v1 on v0

v1 whole, which is shorter than its diff:
```python
import jax
import jax.numpy as jnp
from jax import lax
from jax.experimental import pallas as pl
from jax.experimental.pallas import tpu as pltpu
from jax.sharding import PartitionSpec as P

HALO = 8
norm_eps = 1e-06
NZ = 16
NY = 4
ROWS = 32
LOWEST = -1e30
PACKET = 144

f32 = jnp.float32
bf16 = jnp.bfloat16
smem = pl.BlockSpec(memory_space=pltpu.SMEM)
vmem = pl.BlockSpec(memory_space=pltpu.VMEM)


def from_everyone(x, axis):
    copies = jnp.broadcast_to(x, (lax.axis_size(axis), *x.shape))
    return lax.all_to_all(copies, axis, split_axis=0, concat_axis=0, tiled=True)


def pack_kernel(k_ref, v_ref, q_ref, o_ref, p_ref, m_ref, po_ref, kv_ref, rest_ref):
    kv_ref[:, :128] = k_ref[...]
    kv_ref[:, 128:] = v_ref[...]
    at = 0
    for ref in (q_ref, o_ref, p_ref, m_ref, po_ref):
        width = ref.shape[1]
        rest_ref[:, at : at + width] = ref[...]
        at += width


def in_order(w_ref, lo, hi):
    return jnp.concatenate(
        [w_ref[y, z * ROWS : (z + 1) * ROWS, lo:hi] for z in range(NZ) for y in range(NY)], axis=0
    )


def log_sigmoid(x):
    return jnp.minimum(x, 0.0) - jnp.log1p(jnp.exp(-jnp.abs(x)))


def gates_kernel(tok_ref, gain_ref, gw_ref, bias_ref, decay_ref, normed_ref, cols_ref, rows_ref):
    x = tok_ref[...].astype(f32)
    count = x.shape[0]
    normed = x * lax.rsqrt(jnp.mean(x * x, axis=-1, keepdims=True) + norm_eps) * gain_ref[...]
    normed = normed.astype(bf16)
    normed_ref[...] = normed
    pre = lax.dot_general(
        gw_ref[...], normed, (((1,), (1,)), ((), ())), preferred_element_type=f32
    )
    pre = pre + bias_ref[...]
    in_rows = (pre[0:1], pre[2:3])
    lf_rows = (
        log_sigmoid(pre[1:2]) + decay_ref[0:1],
        log_sigmoid(pre[3:4]) + decay_ref[1:2],
    )
    stacked = jnp.concatenate(
        [in_rows[0], in_rows[1], lf_rows[0], lf_rows[1], jnp.zeros((124, count), f32)], axis=0
    )
    turned = stacked.T
    first = lax.broadcasted_iota(jnp.int32, (count, count), 0)
    second = lax.broadcasted_iota(jnp.int32, (count, count), 1)
    lane = lax.broadcasted_iota(jnp.int32, (count, 128), 1)
    cols = jnp.zeros((count, 128), f32)
    rows = []
    tails = []
    for r in range(2):
        reach = second <= first if r == 0 else second >= first
        reach_t = first <= second if r == 0 else first >= second
        lf_row = lf_rows[r]
        lf_col = turned[:, 2 + r : 3 + r]
        b_col = jnp.sum(jnp.where(reach, lf_row, 0.0), axis=1, keepdims=True)
        b_row = jnp.sum(jnp.where(reach_t, lf_col, 0.0), axis=0, keepdims=True)
        a_row = in_rows[r] - b_row
        a_col = turned[:, r : r + 1] - b_col
        m_col = jnp.max(jnp.where(reach, a_row, LOWEST), axis=1, keepdims=True)
        top = jnp.max(a_row, axis=1, keepdims=True)
        w_col = jnp.exp(a_col - top)
        total = jnp.sum(lf_row, axis=1, keepdims=True)
        for n, col in enumerate((b_col, m_col, w_col)):
            cols = jnp.where(lane == 3 * r + n, col, cols)
        rows.append(a_row)
        tails.append(jnp.broadcast_to(total + top, (1, count)))
        tails.append(jnp.broadcast_to(total, (1, count)))
    cols_ref[...] = cols
    rows_ref[...] = jnp.concatenate(rows + tails + [jnp.zeros((2, count), f32)], axis=0)


def in_three(x):
    high = x.astype(bf16).astype(f32)
    rest = x - high
    mid = rest.astype(bf16).astype(f32)
    low = (rest - mid).astype(bf16).astype(f32)
    return [high, mid, low]


def state_kernel(z_ref, w_ref, normed_ref, cols_ref, rows_ref, k_ref, v_ref, out_ref):
    position = z_ref[0]
    weight = in_order(w_ref, 0, 256)
    kv = jnp.dot(normed_ref[...], weight, preferred_element_type=f32).astype(bf16)
    k = kv[:, :128]
    v = kv[:, 128:]
    k_ref[...] = k
    v_ref[...] = v
    scale = 128**-0.5
    k_wide = k.astype(f32)
    v_wide = v.astype(f32)
    packets = []
    for r in range(2):
        w = cols_ref[:, 3 * r + 2 : 3 * r + 3]
        wv = w * v_wide
        high = wv.astype(bf16)
        low = (wv - high.astype(f32)).astype(bf16)
        over_time = (((0,), (0,)), ((), ()))
        memory = lax.dot_general(high, k, over_time, preferred_element_type=f32)
        memory = memory + lax.dot_general(low, k, over_time, preferred_element_type=f32)
        norm = jnp.sum(w * k_wide, axis=0, keepdims=True) * scale
        extra = in_three(norm)
        extra = extra + in_three(rows_ref[2 + 2 * r : 3 + 2 * r, :128])
        extra = extra + in_three(rows_ref[3 + 2 * r : 4 + 2 * r, :128])
        extra = jnp.concatenate(extra + [jnp.zeros((7, 128), f32)], axis=0)
        packets.append(jnp.concatenate([memory * scale, extra], axis=0).astype(bf16))
    for j in range(NZ):

        @pl.when(j > position)
        def _():
            out_ref[j] = packets[0]

        @pl.when(j <= position)
        def _():
            out_ref[j] = packets[1]


def local_kernel(
    w_ref, normed_ref, k_ref, v_ref, cols_ref, rows_ref,
    q_ref, o_ref, p_ref, num_ref, den_ref,
):
    weight = w_ref[:, :512]
    both = jnp.dot(normed_ref[...], weight, preferred_element_type=f32).astype(bf16)
    q = both[:, :128]
    q_ref[...] = q
    o_ref[...] = both[:, 128:256]
    p_ref[...] = both[:, 256:512]
    count = q.shape[0]
    scores = lax.dot_general(
        q, k_ref[...], (((1,), (1,)), ((), ())), preferred_element_type=f32
    ) * (128**-0.5)
    first = lax.broadcasted_iota(jnp.int32, (count, count), 0)
    second = lax.broadcasted_iota(jnp.int32, (count, count), 1)
    lane = lax.broadcasted_iota(jnp.int32, (count, 128), 1)
    dens = jnp.zeros((count, 128), f32)
    for r in range(2):
        reach = second <= first if r == 0 else second >= first
        m_col = cols_ref[:, 3 * r + 1 : 3 * r + 2]
        a_row = rows_ref[r : r + 1]
        weights = jnp.exp(jnp.where(reach, a_row - m_col, LOWEST)) * scores
        num_ref[r] = jnp.dot(weights.astype(bf16), v_ref[...], preferred_element_type=f32)
        dens = jnp.where(lane == r, jnp.sum(weights, axis=1, keepdims=True), dens)
    den_ref[...] = dens


def pool_kernel(s_ref, p_ref, lo_ref, hi_ref, out_ref, a_ref, b_ref):
    count = p_ref.shape[0]
    group = s_ref[1]
    centre = p_ref[...].astype(f32)
    a_ref[0:8] = jnp.zeros_like(a_ref[0:8])
    a_ref[8:16] = lo_ref[...].astype(f32)
    a_ref[16 : 16 + count] = centre
    a_ref[16 + count : 24 + count] = hi_ref[...].astype(f32)
    a_ref[24 + count : 32 + count] = jnp.zeros_like(a_ref[0:8])
    width = count + 16
    b_ref[...] = jnp.zeros_like(b_ref)
    b_ref[8 : 8 + width] = a_ref[7 : 7 + width] + a_ref[8 : 8 + width]
    total = b_ref[16 : 16 + count]
    refs = (b_ref, a_ref)
    for g in range(1, 4):
        step = 1 << (g - 1)
        src, dst = refs[(g - 1) % 2], refs[g % 2]
        dst[8 : 8 + width] = src[8 - step : 8 - step + width] + src[8 + step : 8 + step + width]
        total = jnp.where(group == g, dst[16 : 16 + count], total)
    left = jnp.left_shift(1, group)
    position = s_ref[0] * count + lax.broadcasted_iota(jnp.int32, (count, 1), 0)
    begin = jnp.maximum(position - left, 0)
    end = jnp.minimum(position + left - 1, NZ * count - 1)
    counted = (end - begin + 1).astype(f32)
    out_ref[...] = (total / counted - centre).astype(bf16)


def final_kernel(
    s_ref, got_ref, mem_ref, nrm_ref, cols_ref, q_ref, o_ref, num_ref, den_ref,
    gain_ref, pool_ref, w_ref, out_ref,
):
    position = s_ref[0]
    got_n, got_m, got_f = [], [], []
    for j in range(NZ):
        extra = got_ref[j, 128:PACKET].astype(f32)
        got_n.append(extra[0:1] + extra[1:2] + extra[2:3])
        got_m.append(extra[3:4] + extra[4:5] + extra[5:6])
        got_f.append(extra[6:7] + extra[7:8] + extra[8:9])
    q = q_ref[...]
    q_wide = q.astype(f32)
    last = (((1,), (1,)), ((), ()))
    summed = None
    for r in range(2):
        order = range(NZ - 1, -1, -1) if r == 0 else range(NZ)
        levels = [None] * NZ
        passed = jnp.zeros((1, 128), f32)
        for j in order:
            ahead = j < position if r == 0 else j > position
            levels[j] = jnp.where(ahead, got_m[j] + passed, LOWEST)
            passed = passed + jnp.where(ahead, got_f[j], 0.0)
        top = passed
        for j in range(NZ):
            top = jnp.maximum(top, levels[j])
        share = jnp.exp(passed - top)
        memory = share * mem_ref[r]
        norm = share * nrm_ref[r : r + 1]
        for j in range(NZ):
            share = jnp.exp(levels[j] - top)
            memory = memory + share * got_ref[j, 0:128].astype(f32)
            norm = norm + share * got_n[j]
        high = memory.astype(bf16)
        low = (memory - high.astype(f32)).astype(bf16)
        carried = lax.dot_general(q, high, last, preferred_element_type=f32)
        carried = carried + lax.dot_general(q, low, last, preferred_element_type=f32)
        carried_den = jnp.sum(q_wide * norm, axis=1, keepdims=True)
        b_col = cols_ref[:, 3 * r : 3 * r + 1]
        m_col = cols_ref[:, 3 * r + 1 : 3 * r + 2]
        stab = top[:, 0:1]
        joint = jnp.maximum(stab, m_col)
        carry = jnp.exp(stab - joint)
        keep = jnp.exp(m_col - joint)
        numerator = carry * carried + keep * num_ref[r]
        denominator = carry * carried_den + keep * den_ref[:, r : r + 1]
        floor = jnp.exp(-(b_col + joint))
        part = numerator / jnp.maximum(jnp.abs(denominator), floor)
        summed = part if summed is None else summed + part
    scaled = summed * lax.rsqrt(jnp.mean(summed * summed, axis=-1, keepdims=True) + norm_eps)
    gate = 1.0 / (1.0 + jnp.exp(-o_ref[...].astype(f32)))
    memory_out = (scaled * gain_ref[...] * gate).astype(bf16)
    result = lax.dot_general(memory_out, w_ref[:, 512:640], last, preferred_element_type=f32)
    result = result + lax.dot_general(pool_ref[...], w_ref[:, 640:], last, preferred_element_type=f32)
    out_ref[...] = result.astype(bf16)


def sds(shape, dtype):
    return jax.ShapeDtypeStruct(shape, dtype)


def call(kernel, name, outs, scalars, *args, flops=0, scratch=()):
    many = isinstance(outs, tuple)
    return pl.pallas_call(
        kernel,
        in_specs=[smem] * len(scalars) + [vmem] * len(args),
        out_specs=(vmem,) * len(outs) if many else vmem,
        out_shape=outs,
        scratch_shapes=list(scratch),
        cost_estimate=pl.CostEstimate(flops=flops, bytes_accessed=0, transcendentals=0),
        name=name,
    )(*scalars, *args)


def per_device(
    tokens,
    norm_gain,
    query_weight,
    key_weight,
    value_weight,
    outgate_weight,
    gate_weight,
    gate_bias,
    decay_extra,
    init_memory,
    init_normalizer,
    head_gain,
    pool_weight,
    mem_out_weight,
    pool_out_weight,
):
    count, width = tokens.shape[1:]
    z = lax.axis_index("sp")
    scalars = jnp.stack([z, lax.axis_index("tp") // 2]).astype(jnp.int32)
    packed, packed_rest = call(
        pack_kernel, "pack", (sds((ROWS, 256), bf16), sds((ROWS, 896), bf16)), (),
        key_weight, value_weight, query_weight, outgate_weight, pool_weight, mem_out_weight,
        pool_out_weight,
        flops=10**6,
    )
    along_y = lax.all_gather(packed_rest, "fs", axis=0, tiled=True)
    rest = lax.all_gather(along_y, "sp", axis=0, tiled=True)
    packed, along_y = lax.optimization_barrier((packed, along_y))
    along_z = lax.all_gather(packed, "sp", axis=0, tiled=True)
    kv_weight = from_everyone(along_z, "fs")
    own_tokens, along_z = lax.optimization_barrier((tokens[0], along_z))
    normed, cols, rows = call(
        gates_kernel, "gates",
        (sds((count, width), bf16), sds((count, 128), f32), sds((8, count), f32)), (),
        own_tokens,
        norm_gain[None],
        jnp.pad(gate_weight[:, 0], ((0, 4), (0, 0))),
        jnp.pad(gate_bias, ((0, 4), (0, 0))),
        decay_extra[0, :, 0],
        flops=4 * 10**9,
    )
    k, v, packets = call(
        state_kernel, "state",
        (sds((count, 128), bf16), sds((count, 128), bf16), sds((NZ, PACKET, 128), bf16)),
        (scalars,), kv_weight, normed, cols, rows,
        flops=2 * 10**9,
    )
    got = lax.all_to_all(packets, "sp", 0, 0, tiled=True)
    q, outgate, pool_in, nums, dens = call(
        local_kernel, "local",
        (
            sds((count, 128), bf16),
            sds((count, 128), bf16),
            sds((count, 256), bf16),
            sds((2, count, 128), f32),
            sds((count, 128), f32),
        ),
        (), rest, normed, k, v, cols, rows,
        flops=5 * 10**9,
    )
    length = lax.axis_size("sp")
    up = [(i, i + 1) for i in range(length - 1)]
    down = [(i + 1, i) for i in range(length - 1)]
    low = lax.ppermute(pool_in[count - HALO :], "sp", up)
    high = lax.ppermute(pool_in[:HALO], "sp", down)
    pool_out = call(
        pool_kernel, "pool", sds((count, 256), bf16), (scalars,), pool_in, low, high,
        flops=10**9, scratch=[pltpu.VMEM((count + 32, 256), f32)] * 2,
    )
    partial = call(
        final_kernel, "final", sds((count, width), bf16), (scalars,),
        got, init_memory[0, :, 0], init_normalizer[0, :, 0], cols, q, outgate,
        nums, dens, head_gain, pool_out, rest,
        flops=2 * 10**9,
    )
    own = count // lax.axis_size("tp")
    parts = lax.all_to_all(partial.reshape(-1, own, width), "tp", 0, 0, tiled=True)
    mixed = jnp.sum(parts.astype(f32), axis=0).astype(bf16)
    return mixed.reshape(1, own, width)


def solution(mesh):
    placed = (
        P("fs", "sp", None),
        P(),
        P(("sp", "fs"), "tp"),
        P(("sp", "fs"), "tp"),
        P(("sp", "fs"), "tp"),
        P(("sp", "fs"), "tp"),
        P(None, "tp", None),
        P(None, "tp"),
        P("fs", None, "tp", "sp"),
        P("fs", None, "tp", None, None),
        P("fs", None, "tp", None),
        P("tp", None),
        P(("sp", "fs"), "tp"),
        P(("sp", "fs"), "tp"),
        P(("sp", "fs"), "tp"),
    )
    return jax.shard_map(
        per_device,
        mesh=mesh,
        in_specs=placed,
        out_specs=P("fs", ("sp", "tp"), None),
        check_vma=False,
    )
```

time: 334 us -> 175 us (0.52)
  waiting for transfers between devices: 124 us -> 49 us
  loops' own time: 42.5 us -> 0 us
  other arithmetic: 39.5 us -> 1.46 us
  blocking collectives: 37.6 us -> 71.2 us
  local copies, waits for them, and re-layouts: 36.1 us -> 6.06 us
  matrix products: 21 us -> 0 us
  Pallas kernels: 0 us -> 19.8 us
  between operations: 18.4 us -> 13.4 us
    all_gather x2 -> x1, waiting for transfers between devices: 123 us -> 41.9 us  [per_device(): rest = lax.all_gather(along_y, 'sp', axis=0, tiled=True)]
    another operation x1 -> x0, loops' own time: 42.5 us -> none  [entering(): return lax.fori_loop(0, length, lap, start)]
    all_gather x1 -> x2, blocking collectives: 11.5 us -> 42.5 us  [the longest x1 29.9 us: per_device(): along_z = lax.all_gather(packed, 'sp', axis=0, tiled=True)]
    dot_general x19 -> x0, matrix products: 21 us -> none  [the longest x4 6.33 us: per_device(): jnp.dot(normed, weight_rows, preferred_element_type=jnp.float32)]
    dynamic_slice x16 -> x0, local copies, waits for them, and re-layouts: 20.4 us -> none  [lap(): new = combine(before, jax.tree.map(lambda part: part[at], everything))]
    pallas_call x0 -> x6, Pallas kernels: none -> 19.8 us  [call(): pl.pallas_call(kernel, in_specs=[smem] * len(scalars) + [vmem] * len(args...]
    select_n x35 -> x0, other arithmetic: 19 us -> none  [the longest x32 18.7 us: lap(): return jax.tree.map(lambda a, b: jnp.where(reached, a, b), new, before)]
    all_to_all x0 -> x1, starting transfers between devices: none -> 6.73 us  [per_device(): got = lax.all_to_all(packets, 'sp', 0, 0, tiled=True)]
  transfers between devices with their start and end apart: 5 -> 5, of which waited for: 2 -> 3; matrix products, arithmetic and copies ran while one was open for 23% -> 2% of each run, Pallas kernels for 0% -> 7%
where the time goes in v1:
time: 175 us; the launch traced here: 174 us
  blocking collectives  71.2 us (41%)
  waiting for transfers between devices  49 us (28%)
  Pallas kernels  19.8 us (11%)
  starting transfers between devices  13.5 us (8%)
  between operations  13.4 us (8%)
  local copies, waits for them, and re-layouts  6.06 us (3%)
    all_gather x1, waiting for transfers between devices, per_device(): rest = lax.all_gather(along_y, 'sp', axis=0, tiled=True)  41.9 us
    all_gather x1, blocking collectives, per_device(): along_z = lax.all_gather(packed, 'sp', axis=0, tiled=True)  29.9 us
    all_to_all x1, blocking collectives, per_device(): lax.all_to_all(partial.reshape(-1, own, width), 'tp', 0, 0, tiled=True)  28.7 us
    pallas_call x6, Pallas kernels, call(): pl.pallas_call(kernel, in_specs=[smem] * len(scalars) + [vmem] * len(args...  19.8 us
    all_gather x1, blocking collectives, per_device(): along_y = lax.all_gather(packed_rest, 'fs', axis=0, tiled=True)  12.6 us
    all_to_all x1, starting transfers between devices, per_device(): got = lax.all_to_all(packets, 'sp', 0, 0, tiled=True)  6.73 us
    all_to_all x1, waiting for transfers between devices, from_everyone(): return lax.all_to_all(copies, axis, split_axis=0, concat_axis=0, tiled=True)  4.04 us
    all_to_all x1, starting transfers between devices, from_everyone(): return lax.all_to_all(copies, axis, split_axis=0, concat_axis=0, tiled=True)  3.75 us
  transfers between devices with their start and end apart: 5, of which 3 were waited for; matrix products, arithmetic and copies ran while one was open for 2% of the time, Pallas kernels for 7%

profile of v1, /device:TPU:1, one launch (start us, length us, event | category | flops | bytes accessed | tf_op | source)
XLA Modules:
  0.0 174.4 jit_solution(8563913115333044241)
XLA Ops:
  6.5 0.0 copy-start.4
  6.5 0.0 copy-start.3
  6.5 0.0 copy-start.2
  6.5 0.0 all-gather.2.cloned.1.call-start
  6.5 1.5 pack.1
  8.0 12.6 %all_gather.9 = bf16[128,896]{1,0:T(8,128)(2,1)} all-gather(bf16[32,896]{1,0:T(8,128)(2,1)} %get-tuple-element.21), channel_id=1, replica_groups=mesh['sp'=16,'fs'=4,'tp'=8] {'fs'}, dimensions={0}, use_global_device_ids=true | all-gather | bytes 286720 | tf_op jit(solution)/shard_map/all_gather | solution.py:294
  20.6 0.0 all-gather.2.cloned.1.call-update
  20.6 29.9 %all_gather.10 = bf16[512,256]{1,0:T(8,128)(2,1)S(1)} all-gather(bf16[32,256]{1,0:T(8,128)(2,1)} %get-tuple-element.22), channel_id=1, replica_groups=mesh['sp'=16,'fs'=4,'tp'=8] {'sp'}, dimensions={0}, use_global_device_ids=true | all-gather | bytes 278528 | tf_op jit(solution)/shard_map/all_gather | solution.py:297
  50.5 1.1 broadcast_in_dim.6
  51.6 3.7 %all-to-all-start = ((bf16[4,512,256]{2,1,0:T(8,128)(2,1)}), bf16[4,512,256]{2,1,0:T(8,128)(2,1)S(1)}, u32[]{:S(2)}, u32[]{:S(2)}) async-start(bf16[4,512,256]{2,1,0:T(8,128)(2,1)} %broadcast_in_dim.6), calls=%async_computation | async-start | bytes 2097152 | tf_op jit(solution)/shard_map/all_to_all | solution.py:24
  55.3 0.0 copy-done.4
  55.3 0.1 copy.16
  55.4 0.0 copy-done.3
  55.4 0.6 copy.19
  56.0 0.0 copy-done.2
  56.0 0.6 pad.8.gw_ref
  56.7 0.6 pad.9.bias_ref
  57.2 0.6 pad_add_fusion.z_ref.s_ref
  57.9 3.2 %gates.1 = (bf16[256,2048]{1,0:T(8,128)(2,1)}, f32[256,128]{1,0:T(8,128)}, f32[8,256]{1,0:T(8,128)}) custom-call(bf16[256,2048]{1,0:T(8,128)(2,1)} %bitcast.15, f32[1,2048]{1,0:T(1,128)} %bitcast.17, bf16[8,2048]{1,0:T(8,128)(2,1)} %pad.8.gw_ref, f32[8,1]{1,0:T(8,128)} %pad.9.bias_ref, f32[2,256]{1,0:T(2,128)} %bitcast.14), custom_call_target="tpu_custom_call" | custom-call | flops 4000000000 | tf_op jit(solution)/shard_map/gates/pallas_call | solution.py:257
  61.1 4.0 %all-to-all-done.w_ref = bf16[4,512,256]{2,1,0:T(8,128)(2,1)S(1)} async-done(((bf16[4,512,256]{2,1,0:T(8,128)(2,1)}), bf16[4,512,256]{2,1,0:T(8,128)(2,1)S(1)}, u32[]{:S(2)}, u32[]{:S(2)}) %all-to-all-start) | async-done | bytes 1048608 | tf_op jit(solution)/shard_map/all_to_all | solution.py:24
  65.1 0.0 copy-start
  65.1 1.0 copy-done
  66.1 3.4 %state.1 = (bf16[256,128]{1,0:T(8,128)(2,1)}, bf16[256,128]{1,0:T(8,128)(2,1)}, bf16[16,144,128]{2,1,0:T(8,128)(2,1)}) custom-call(s32[2]{0:T(128)} %pad_add_fusion.z_ref.s_ref, bf16[4,512,256]{2,1,0:T(8,128)(2,1)} %copy-done, bf16[256,2048]{1,0:T(8,128)(2,1)} %get-tuple-element.24.normed_ref, f32[256,128]{1,0:T(8,128)} %get-tuple-element.25.cols_ref, ...), custom_call_target="tpu_custom_call" | custom-call | flops 2000000000 | tf_op jit(solution)/shard_map/state/pallas_call | solution.py:257
  69.5 6.7 %all-to-all-start.1 = ((bf16[16,144,128]{2,1,0:T(8,128)(2,1)}), bf16[16,144,128]{2,1,0:T(8,128)(2,1)S(1)}, u32[]{:S(2)}, u32[]{:S(2)}) async-start(bf16[16,144,128]{2,1,0:T(8,128)(2,1)} %get-tuple-element.27), calls=%async_computation.1 | async-start | bytes 1179648 | tf_op jit(solution)/shard_map/all_to_all | solution.py:316
  76.3 41.9 %all-gather.2.cloned.1.call-done.w_ref = bf16[2048,896]{1,0:T(8,128)(2,1)} async-done(((bf16[128,896]{1,0:T(8,128)(2,1)}), bf16[2048,896]{1,0:T(8,128)(2,1)}) %all-gather.2.cloned.1.call-update) | async-done | bytes 3670032 | tf_op jit(solution)/shard_map/all_gather | solution.py:295
  118.1 4.1 %local.1 = (bf16[256,128]{1,0:T(8,128)(2,1)}, bf16[256,128]{1,0:T(8,128)(2,1)}, bf16[256,256]{1,0:T(8,128)(2,1)}, f32[2,256,128]{2,1,0:T(8,128)}, f32[256,128]{1,0:T(8,128)}) custom-call(bf16[2048,896]{1,0:T(8,128)(2,1)} %all-gather.2.cloned.1.call-done.w_ref, bf16[256,2048]{1,0:T(8,128)(2,1)} %get-tuple-element.24.normed_ref, ...), custom_call_target="tpu_custom_call" | custom-call | flops 5000000000 | tf_op jit(solution)/shard_map/local/pallas_call | solution.py:257
  122.2 0.7 fusion
  122.9 1.7 %collective-permute-start = (bf16[8,256]{1,0:T(8,128)(2,1)S(1)}, bf16[8,256]{1,0:T(8,128)(2,1)S(1)}, u32[]{:S(2)}, u32[]{:S(2)}) collective-permute-start(bf16[8,256]{1,0:T(8,128)(2,1)S(1)} %get-tuple-element.36), channel_id=1, source_target_pairs={{0,32},{32,64},{64,96},{96,128},{128,160},{160,192},{192,224},{224... | collective-permute-start | bytes 12296 | tf_op jit(solution)/shard_map/ppermute | solution.py:332
  124.7 1.3 collective-permute-start.1
  126.0 0.0 collective-permute-done.lo_ref
  126.0 0.0 copy-start.5
  126.0 3.0 %collective-permute-done.1.hi_ref = bf16[8,256]{1,0:T(8,128)(2,1)S(1)} collective-permute-done((bf16[8,256]{1,0:T(8,128)(2,1)S(1)}, bf16[8,256]{1,0:T(8,128)(2,1)S(1)}, u32[]{:S(2)}, u32[]{:S(2)}) %collective-permute-start.1) | collective-permute-done | bytes 4128 | tf_op jit(solution)/shard_map/ppermute | solution.py:333
  129.0 0.0 copy-done.5
  129.0 0.0 copy-start.6
  129.0 0.6 copy-done.6
  129.6 1.9 %pool.1.pool_ref = bf16[256,256]{1,0:T(8,128)(2,1)} custom-call(s32[2]{0:T(128)} %pad_add_fusion.z_ref.s_ref, bf16[256,256]{1,0:T(8,128)(2,1)} %get-tuple-element.34.p_ref, bf16[8,256]{1,0:T(8,128)(2,1)} %copy-done.5, bf16[8,256]{1,0:T(8,128)(2,1)} %copy-done.6), custom_call_target="tpu_custom_call" | custom-call | flops 1000000000 | tf_op jit(solution)/shard_map/pool/pallas_call | solution.py:257
  131.5 0.0 all-to-all-done.1.got_ref
  131.5 0.0 copy-start.1
  131.5 0.8 copy-done.1
  132.3 5.7 %final.1 = bf16[256,2048]{1,0:T(8,128)(2,1)} custom-call(s32[2]{0:T(128)} %pad_add_fusion.z_ref.s_ref, bf16[16,144,128]{2,1,0:T(8,128)(2,1)} %copy-done.1, f32[2,128,128]{2,1,0:T(8,128)} %bitcast.16, f32[2,128]{1,0:T(2,128)} %bitcast.18, f32[256,128]{1,0:T(8,128)} %get-tuple-element.25.cols_ref, bf16[256,128]{1,0:T(8,128)(2,1)} %get-tuple-element.30.q_ref, ...), custom_call_target="tpu_custom_call" | custom-call | flops 2000000000 | tf_op jit(solution)/shard_map/final/pallas_call | solution.py:257
  138.0 28.7 %all_to_all.15 = bf16[8,32,2048]{2,1,0:T(8,128)(2,1)S(1)} all-to-all(bf16[8,32,2048]{2,1,0:T(8,128)(2,1)} %bitcast.12), channel_id=1, replica_groups=mesh['sp'=16,'fs'=4,'tp'=8] {'tp'}, dimensions={0} | all-to-all | bytes 2097152 | tf_op jit(solution)/shard_map/all_to_all | solution.py:345
  166.7 0.8 reduce_sum.12
Async XLA Ops:
  6.5 48.8 %copy-start.4 = (f32[4,1]{0,1:T(1,128)S(1)}, f32[4,1]{0,1:T(1,128)}, u32[]{:S(2)}) copy-start(f32[4,1]{0,1:T(1,128)} %param.22) | copy-start | bytes 52
  6.5 48.9 %copy-start.3 = (f32[1,2,1,256]{3,2,1,0:T(1,128)S(1)}, f32[1,2,1,256]{3,2,1,0:T(1,128)}, u32[]{:S(2)}) copy-start(f32[1,2,1,256]{3,2,1,0:T(1,128)} %param.23) | copy-start | bytes 6148
  6.5 49.5 %copy-start.2 = (bf16[4,1,2048]{2,0,1:T(4,128)(2,1)S(1)}, bf16[4,1,2048]{2,0,1:T(4,128)(2,1)}, u32[]{:S(2)}) copy-start(bf16[4,1,2048]{2,0,1:T(4,128)(2,1)} %param.21) | copy-start | bytes 49156
  6.5 111.6 %all-gather.2.cloned.1.call-start = ((), (), s32[]{:S(2)}) async-start(), calls=%async_computation.3 | async-start | bytes 3899392 | tf_op jit(solution)/shard_map/all_gather | solution.py:295
  51.6 13.5 %all-to-all-start = ((bf16[4,512,256]{2,1,0:T(8,128)(2,1)}), bf16[4,512,256]{2,1,0:T(8,128)(2,1)S(1)}, u32[]{:S(2)}, u32[]{:S(2)}) async-start(bf16[4,512,256]{2,1,0:T(8,128)(2,1)} %broadcast_in_dim.6), calls=%async_computation | async-start | bytes 2097152 | tf_op jit(solution)/shard_map/all_to_all | solution.py:24
  65.1 1.0 copy-start
  69.5 62.0 %all-to-all-start.1 = ((bf16[16,144,128]{2,1,0:T(8,128)(2,1)}), bf16[16,144,128]{2,1,0:T(8,128)(2,1)S(1)}, u32[]{:S(2)}, u32[]{:S(2)}) async-start(bf16[16,144,128]{2,1,0:T(8,128)(2,1)} %get-tuple-element.27), calls=%async_computation.1 | async-start | bytes 1179648 | tf_op jit(solution)/shard_map/all_to_all | solution.py:316
  122.9 3.1 %collective-permute-start = (bf16[8,256]{1,0:T(8,128)(2,1)S(1)}, bf16[8,256]{1,0:T(8,128)(2,1)S(1)}, u32[]{:S(2)}, u32[]{:S(2)}) collective-permute-start(bf16[8,256]{1,0:T(8,128)(2,1)S(1)} %get-tuple-element.36), channel_id=1, source_target_pairs={{0,32},{32,64},{64,96},{96,128},{128,160},{160,192},{192,224},{224... | collective-permute-start | bytes 12296 | tf_op jit(solution)/shard_map/ppermute | solution.py:332
  124.7 4.4 %collective-permute-start.1 = (bf16[8,256]{1,0:T(8,128)(2,1)S(1)}, bf16[8,256]{1,0:T(8,128)(2,1)S(1)}, u32[]{:S(2)}, u32[]{:S(2)}) collective-permute-start(bf16[8,256]{1,0:T(8,128)(2,1)S(1)} %get-tuple-element.35), channel_id=1, source_target_pairs={{32,0},{64,32},{96,64},{128,96},{160,128},{192,160},{224,192},{256... | collective-permute-start | bytes 12296 | tf_op jit(solution)/shard_map/ppermute | solution.py:333
  126.0 3.0 %copy-start.5 = (bf16[8,256]{1,0:T(8,128)(2,1)}, bf16[8,256]{1,0:T(8,128)(2,1)S(1)}, u32[]{:S(2)}) copy-start(bf16[8,256]{1,0:T(8,128)(2,1)S(1)} %collective-permute-done.lo_ref) | copy-start | bytes 12292
  129.0 0.6 copy-start.6
  131.5 0.8 copy-start.1
Sparse Core Ops, SparseCore 0:
  20.7 97.3 all-gather.1

commit v2 on v1

--- a/solution.py
+++ b/solution.py
@@ -24,20 +24,32 @@
     return lax.all_to_all(copies, axis, split_axis=0, concat_axis=0, tiled=True)
 
 
-def pack_kernel(k_ref, v_ref, q_ref, o_ref, p_ref, m_ref, po_ref, kv_ref, rest_ref):
-    kv_ref[:, :128] = k_ref[...]
-    kv_ref[:, 128:] = v_ref[...]
+def pack_kernel(k_ref, v_ref, q_ref, o_ref, p_ref, m_ref, out_ref):
     at = 0
-    for ref in (q_ref, o_ref, p_ref, m_ref, po_ref):
+    for ref in (k_ref, v_ref, q_ref, o_ref, p_ref, m_ref):
         width = ref.shape[1]
-        rest_ref[:, at : at + width] = ref[...]
+        out_ref[:, at : at + width] = ref[...]
         at += width
 
 
-def in_order(w_ref, lo, hi):
+def in_order(w_ref):
     return jnp.concatenate(
-        [w_ref[y, z * ROWS : (z + 1) * ROWS, lo:hi] for z in range(NZ) for y in range(NY)], axis=0
-    )
+        [w_ref[y, z * ROWS : (z + 1) * ROWS] for z in range(NZ) for y in range(NY)], axis=0
+    )
+
+
+def around(x, axis):
+    count = lax.axis_size(axis)
+    return [x] + [lax.ppermute(x, axis, [(i, (i + s) % count) for i in range(count)]) for s in (1, 2, 3)]
+
+
+def placed_by_source(y, refs, out_ref):
+    for shift, ref in enumerate(refs):
+        out_ref[lax.rem(y + NY - shift, NY)] = ref[...]
+
+
+def rms_normed(x, gain):
+    return x * lax.rsqrt(jnp.mean(x * x, axis=-1, keepdims=True) + norm_eps) * gain
 
 
 def log_sigmoid(x):
@@ -47,8 +59,7 @@
 def gates_kernel(tok_ref, gain_ref, gw_ref, bias_ref, decay_ref, normed_ref, cols_ref, rows_ref):
     x = tok_ref[...].astype(f32)
     count = x.shape[0]
-    normed = x * lax.rsqrt(jnp.mean(x * x, axis=-1, keepdims=True) + norm_eps) * gain_ref[...]
-    normed = normed.astype(bf16)
+    normed = rms_normed(x, gain_ref[...]).astype(bf16)
     normed_ref[...] = normed
     pre = lax.dot_general(
         gw_ref[...], normed, (((1,), (1,)), ((), ())), preferred_element_type=f32
@@ -101,7 +112,7 @@
 
 def state_kernel(z_ref, w_ref, normed_ref, cols_ref, rows_ref, k_ref, v_ref, out_ref):
     position = z_ref[0]
-    weight = in_order(w_ref, 0, 256)
+    weight = in_order(w_ref)
     kv = jnp.dot(normed_ref[...], weight, preferred_element_type=f32).astype(bf16)
     k = kv[:, :128]
     v = kv[:, 128:]
@@ -136,17 +147,50 @@
             out_ref[j] = packets[1]
 
 
+def pooled(position, group, centre, low, high, a_ref, b_ref):
+    count = centre.shape[0]
+    a_ref[0:8] = jnp.zeros_like(a_ref[0:8])
+    a_ref[8:16] = low
+    a_ref[16 : 16 + count] = centre
+    a_ref[16 + count : 24 + count] = high
+    a_ref[24 + count : 32 + count] = jnp.zeros_like(a_ref[0:8])
+    width = count + 16
+    b_ref[...] = jnp.zeros_like(b_ref)
+    b_ref[8 : 8 + width] = a_ref[7 : 7 + width] + a_ref[8 : 8 + width]
+    total = b_ref[16 : 16 + count]
+    refs = (b_ref, a_ref)
+    for g in range(1, 4):
+        step = 1 << (g - 1)
+        src, dst = refs[(g - 1) % 2], refs[g % 2]
+        dst[8 : 8 + width] = src[8 - step : 8 - step + width] + src[8 + step : 8 + step + width]
+        total = jnp.where(group == g, dst[16 : 16 + count], total)
+    left = jnp.left_shift(1, group)
+    place = position * count + lax.broadcasted_iota(jnp.int32, (count, 1), 0)
+    begin = jnp.maximum(place - left, 0)
+    end = jnp.minimum(place + left - 1, NZ * count - 1)
+    counted = (end - begin + 1).astype(f32)
+    return (total / counted - centre).astype(bf16)
+
+
 def local_kernel(
-    w_ref, normed_ref, k_ref, v_ref, cols_ref, rows_ref,
-    q_ref, o_ref, p_ref, num_ref, den_ref,
+    s_ref, w0_ref, w1_ref, w2_ref, w3_ref, normed_ref, lo_ref, hi_ref, gain_ref,
+    k_ref, v_ref, cols_ref, rows_ref,
+    q_ref, o_ref, pool_ref, num_ref, den_ref, w_ref, a_ref, b_ref,
 ):
-    weight = w_ref[:, :512]
-    both = jnp.dot(normed_ref[...], weight, preferred_element_type=f32).astype(bf16)
-    q = both[:, :128]
+    placed_by_source(s_ref[2], (w0_ref, w1_ref, w2_ref, w3_ref), w_ref)
+    weight = in_order(w_ref)
+    halo = jnp.concatenate([lo_ref[...], hi_ref[...]], axis=0).astype(f32)
+    halo = rms_normed(halo, gain_ref[...]).astype(bf16)
+    left = jnp.concatenate([normed_ref[...], halo], axis=0)
+    all_three = jnp.dot(left, weight, preferred_element_type=f32).astype(bf16)
+    count = normed_ref.shape[0]
+    q = all_three[:count, :128]
     q_ref[...] = q
-    o_ref[...] = both[:, 128:256]
-    p_ref[...] = both[:, 256:512]
-    count = q.shape[0]
+    o_ref[...] = all_three[:count, 128:256]
+    p = all_three[:, 256:512].astype(f32)
+    pool_ref[...] = pooled(
+        s_ref[0], s_ref[1], p[:count], p[count : count + HALO], p[count + HALO :], a_ref, b_ref
+    )
     scores = lax.dot_general(
         q, k_ref[...], (((1,), (1,)), ((), ())), preferred_element_type=f32
     ) * (128**-0.5)
@@ -164,37 +208,11 @@
     den_ref[...] = dens
 
 
-def pool_kernel(s_ref, p_ref, lo_ref, hi_ref, out_ref, a_ref, b_ref):
-    count = p_ref.shape[0]
-    group = s_ref[1]
-    centre = p_ref[...].astype(f32)
-    a_ref[0:8] = jnp.zeros_like(a_ref[0:8])
-    a_ref[8:16] = lo_ref[...].astype(f32)
-    a_ref[16 : 16 + count] = centre
-    a_ref[16 + count : 24 + count] = hi_ref[...].astype(f32)
-    a_ref[24 + count : 32 + count] = jnp.zeros_like(a_ref[0:8])
-    width = count + 16
-    b_ref[...] = jnp.zeros_like(b_ref)
-    b_ref[8 : 8 + width] = a_ref[7 : 7 + width] + a_ref[8 : 8 + width]
-    total = b_ref[16 : 16 + count]
-    refs = (b_ref, a_ref)
-    for g in range(1, 4):
-        step = 1 << (g - 1)
-        src, dst = refs[(g - 1) % 2], refs[g % 2]
-        dst[8 : 8 + width] = src[8 - step : 8 - step + width] + src[8 + step : 8 + step + width]
-        total = jnp.where(group == g, dst[16 : 16 + count], total)
-    left = jnp.left_shift(1, group)
-    position = s_ref[0] * count + lax.broadcasted_iota(jnp.int32, (count, 1), 0)
-    begin = jnp.maximum(position - left, 0)
-    end = jnp.minimum(position + left - 1, NZ * count - 1)
-    counted = (end - begin + 1).astype(f32)
-    out_ref[...] = (total / counted - centre).astype(bf16)
-
-
 def final_kernel(
     s_ref, got_ref, mem_ref, nrm_ref, cols_ref, q_ref, o_ref, num_ref, den_ref,
-    gain_ref, pool_ref, w_ref, out_ref,
+    gain_ref, pool_ref, w0_ref, w1_ref, w2_ref, w3_ref, out_ref, w_ref,
 ):
+    placed_by_source(s_ref[2], (w0_ref, w1_ref, w2_ref, w3_ref), w_ref)
     position = s_ref[0]
     got_n, got_m, got_f = [], [], []
     for j in range(NZ):
@@ -243,8 +261,9 @@
     scaled = summed * lax.rsqrt(jnp.mean(summed * summed, axis=-1, keepdims=True) + norm_eps)
     gate = 1.0 / (1.0 + jnp.exp(-o_ref[...].astype(f32)))
     memory_out = (scaled * gain_ref[...] * gate).astype(bf16)
-    result = lax.dot_general(memory_out, w_ref[:, 512:640], last, preferred_element_type=f32)
-    result = result + lax.dot_general(pool_ref[...], w_ref[:, 640:], last, preferred_element_type=f32)
+    weight = in_order(w_ref)
+    result = lax.dot_general(memory_out, weight[:, :128], last, preferred_element_type=f32)
+    result = result + lax.dot_general(pool_ref[...], weight[:, 128:], last, preferred_element_type=f32)
     out_ref[...] = result.astype(bf16)
 
 
@@ -283,19 +302,18 @@
     pool_out_weight,
 ):
     count, width = tokens.shape[1:]
-    z = lax.axis_index("sp")
-    scalars = jnp.stack([z, lax.axis_index("tp") // 2]).astype(jnp.int32)
-    packed, packed_rest = call(
-        pack_kernel, "pack", (sds((ROWS, 256), bf16), sds((ROWS, 896), bf16)), (),
+    scalars = jnp.stack(
+        [lax.axis_index("sp"), lax.axis_index("tp") // 2, lax.axis_index("fs")]
+    ).astype(jnp.int32)
+    packed = call(
+        pack_kernel, "pack", sds((ROWS, 896), bf16), (),
         key_weight, value_weight, query_weight, outgate_weight, pool_weight, mem_out_weight,
-        pool_out_weight,
         flops=10**6,
     )
-    along_y = lax.all_gather(packed_rest, "fs", axis=0, tiled=True)
-    rest = lax.all_gather(along_y, "sp", axis=0, tiled=True)
-    packed, along_y = lax.optimization_barrier((packed, along_y))
+    pool_z = from_everyone(pool_out_weight, "sp").reshape(NZ * ROWS, 256)
     along_z = lax.all_gather(packed, "sp", axis=0, tiled=True)
-    kv_weight = from_everyone(along_z, "fs")
+    kv_z, pool_z = lax.optimization_barrier((along_z[:, :256], pool_z))
+    kv_weight = from_everyone(kv_z, "fs")
     own_tokens, along_z = lax.optimization_barrier((tokens[0], along_z))
     normed, cols, rows = call(
         gates_kernel, "gates",
@@ -314,7 +332,20 @@
         flops=2 * 10**9,
     )
     got = lax.all_to_all(packets, "sp", 0, 0, tiled=True)
-    q, outgate, pool_in, nums, dens = call(
+    ends, first_rest, last_rest, k = lax.optimization_barrier(
+        (
+            (own_tokens[:HALO], own_tokens[count - HALO :]),
+            along_z[:, 256:768],
+            jnp.concatenate([along_z[:, 768:], pool_z], axis=1),
+            k,
+        )
+    )
+    length = lax.axis_size("sp")
+    first_rest = around(first_rest, "fs")
+    low = lax.ppermute(ends[1], "sp", [(i, i + 1) for i in range(length - 1)])
+    high = lax.ppermute(ends[0], "sp", [(i + 1, i) for i in range(length - 1)])
+    last_rest = around(last_rest, "fs")
+    q, outgate, pool_out, nums, dens = call(
         local_kernel, "local",
         (
             sds((count, 128), bf16),
@@ -323,23 +354,17 @@
             sds((2, count, 128), f32),
             sds((count, 128), f32),
         ),
-        (), rest, normed, k, v, cols, rows,
+        (scalars,), *first_rest, normed, low, high, norm_gain[None], k, v, cols, rows,
         flops=5 * 10**9,
-    )
-    length = lax.axis_size("sp")
-    up = [(i, i + 1) for i in range(length - 1)]
-    down = [(i + 1, i) for i in range(length - 1)]
-    low = lax.ppermute(pool_in[count - HALO :], "sp", up)
-    high = lax.ppermute(pool_in[:HALO], "sp", down)
-    pool_out = call(
-        pool_kernel, "pool", sds((count, 256), bf16), (scalars,), pool_in, low, high,
-        flops=10**9, scratch=[pltpu.VMEM((count + 32, 256), f32)] * 2,
+        scratch=[pltpu.VMEM((NY, NZ * ROWS, 512), bf16)]
+        + [pltpu.VMEM((count + 32, 256), f32)] * 2,
     )
     partial = call(
         final_kernel, "final", sds((count, width), bf16), (scalars,),
         got, init_memory[0, :, 0], init_normalizer[0, :, 0], cols, q, outgate,
-        nums, dens, head_gain, pool_out, rest,
+        nums, dens, head_gain, pool_out, *last_rest,
         flops=2 * 10**9,
+        scratch=[pltpu.VMEM((NY, NZ * ROWS, 384), bf16)],
     )
     own = count // lax.axis_size("tp")
     parts = lax.all_to_all(partial.reshape(-1, own, width), "tp", 0, 0, tiled=True)

time: 175 us -> 161 us (0.920)
  starting transfers between devices: 13.5 us -> 51.1 us
  waiting for transfers between devices: 49 us -> 19.7 us
  between operations: 13.4 us -> 0.24 us
  blocking collectives: 71.2 us -> 61 us
  local copies, waits for them, and re-layouts: 6.06 us -> 8.98 us
  Pallas kernels: 19.8 us -> 17.3 us
    all_gather x1 -> x0, waiting for transfers between devices: 41.9 us -> none  [per_device(): rest = lax.all_gather(along_y, 'sp', axis=0, tiled=True)]
    ppermute x2 -> x8, starting transfers between devices: 3.04 us -> 21.5 us  [the longest x6 16.9 us: around(): lax.ppermute(x, axis, [(i, (i + s) % count) for i in range(count)])]
    all_to_all x1 -> x2, starting transfers between devices: 3.75 us -> 20 us  [from_everyone(): return lax.all_to_all(copies, axis, split_axis=0, concat_axis=0, tiled=True)]
    ppermute x2 -> x8, waiting for transfers between devices: 3.03 us -> 16.3 us  [the longest x6 10.5 us: around(): lax.ppermute(x, axis, [(i, (i + s) % count) for i in range(count)])]
    all_gather x1 -> x0, blocking collectives: 12.6 us -> none  [per_device(): along_y = lax.all_gather(packed_rest, 'fs', axis=0, tiled=True)]
    all_gather x1, blocking collectives: 29.9 us -> 36.5 us  [per_device(): along_z = lax.all_gather(packed, 'sp', axis=0, tiled=True)]
    all_to_all x1, blocking collectives: 28.7 us -> 24.5 us  [per_device(): lax.all_to_all(partial.reshape(-1, own, width), 'tp', 0, 0, tiled=True)]
    all_to_all x1, starting transfers between devices: 6.73 us -> 9.59 us  [per_device(): got = lax.all_to_all(packets, 'sp', 0, 0, tiled=True)]
  transfers between devices with their start and end apart: 5 -> 11, of which waited for: 3 -> 5; matrix products, arithmetic and copies ran while one was open for 2% -> 2% of each run, Pallas kernels for 7% -> 5%
where the time goes in v2:
time: 161 us; the launch traced here: 160 us
  blocking collectives  61 us (38%)
  starting transfers between devices  51.1 us (32%)
  waiting for transfers between devices  19.7 us (12%)
  Pallas kernels  17.3 us (11%)
  local copies, waits for them, and re-layouts  8.98 us (6%)
    all_gather x1, blocking collectives, per_device(): along_z = lax.all_gather(packed, 'sp', axis=0, tiled=True)  36.5 us
    all_to_all x1, blocking collectives, per_device(): lax.all_to_all(partial.reshape(-1, own, width), 'tp', 0, 0, tiled=True)  24.5 us
    all_to_all x2, starting transfers between devices, from_everyone(): return lax.all_to_all(copies, axis, split_axis=0, concat_axis=0, tiled=True)  20 us
    pallas_call x5, Pallas kernels, call(): pl.pallas_call(kernel, in_specs=[smem] * len(scalars) + [vmem] * len(args...  17.3 us
    ppermute x6, starting transfers between devices, around(): lax.ppermute(x, axis, [(i, (i + s) % count) for i in range(count)])  16.9 us
    ppermute x6, waiting for transfers between devices, around(): lax.ppermute(x, axis, [(i, (i + s) % count) for i in range(count)])  10.5 us
    all_to_all x1, starting transfers between devices, per_device(): got = lax.all_to_all(packets, 'sp', 0, 0, tiled=True)  9.59 us
    ppermute x1, waiting for transfers between devices, per_device(): high = lax.ppermute(ends[0], 'sp', [(i + 1, i) for i in range(length - 1)])  5.07 us
  transfers between devices with their start and end apart: 11, of which 5 were waited for; matrix products, arithmetic and copies ran while one was open for 2% of the time, Pallas kernels for 5%

profile of v2, /device:TPU:1, one launch (start us, length us, event | category | flops | bytes accessed | tf_op | source)
XLA Modules:
  0.0 159.9 jit_solution(7679731115324566478)
XLA Ops:
  0.0 1.4 broadcast_in_dim.10
  1.4 15.7 %all-to-all-start = ((bf16[16,32,256]{2,1,0:T(8,128)(2,1)}), bf16[16,32,256]{2,1,0:T(8,128)(2,1)S(1)}, u32[]{:S(2)}, u32[]{:S(2)}) async-start(bf16[16,32,256]{2,1,0:T(8,128)(2,1)} %broadcast_in_dim.10), calls=%async_computation | async-start | bytes 524288 | tf_op jit(solution)/shard_map/all_to_all | solution.py:24
  17.2 1.4 pack.1
  18.6 36.5 %all_gather.3 = bf16[512,896]{1,0:T(8,128)(2,1)S(1)} all-gather(bf16[32,896]{1,0:T(8,128)(2,1)} %pack.1), channel_id=1, replica_groups=mesh['sp'=16,'fs'=4,'tp'=8] {'sp'}, dimensions={0}, use_global_device_ids=true | all-gather | bytes 974848 | tf_op jit(solution)/shard_map/all_gather | solution.py:314
  55.1 0.0 all-to-all-done
  55.1 1.1 broadcast_in_dim.11
  56.3 4.3 %all-to-all-start.1 = ((bf16[4,512,256]{2,1,0:T(8,128)(2,1)}), bf16[4,512,256]{2,1,0:T(8,128)(2,1)S(1)}, u32[]{:S(2)}, u32[]{:S(2)}) async-start(bf16[4,512,256]{2,1,0:T(8,128)(2,1)} %broadcast_in_dim.11), calls=%async_computation.1 | async-start | bytes 2097152 | tf_op jit(solution)/shard_map/all_to_all | solution.py:24
  60.6 0.0 copy-done.7
  60.6 0.1 copy.16
  60.7 0.6 copy-done.6
  61.3 0.6 copy.19
  61.9 0.6 pad.8.gw_ref
  62.5 0.6 pad.9.bias_ref
  63.1 0.7 pad_add_fusion.z_ref.s_ref
  63.7 3.2 %gates.1 = (bf16[256,2048]{1,0:T(8,128)(2,1)}, f32[256,128]{1,0:T(8,128)}, f32[8,256]{1,0:T(8,128)}) custom-call(bf16[256,2048]{1,0:T(8,128)(2,1)} %bitcast.17, f32[1,2048]{1,0:T(1,128)} %bitcast.21, bf16[8,2048]{1,0:T(8,128)(2,1)} %pad.8.gw_ref, f32[8,1]{1,0:T(8,128)} %pad.9.bias_ref, f32[2,256]{1,0:T(2,128)} %bitcast.19), custom_call_target="tpu_custom_call" | custom-call | flops 4000000000 | tf_op jit(solution)/shard_map/gates/pallas_call | solution.py:276
  66.9 3.4 %all-to-all-done.1.w_ref = bf16[4,512,256]{2,1,0:T(8,128)(2,1)S(1)} async-done(((bf16[4,512,256]{2,1,0:T(8,128)(2,1)}), bf16[4,512,256]{2,1,0:T(8,128)(2,1)S(1)}, u32[]{:S(2)}, u32[]{:S(2)}) %all-to-all-start.1) | async-done | bytes 1048608 | tf_op jit(solution)/shard_map/all_to_all | solution.py:24
  70.3 1.0 copy-done.1
  71.3 3.4 %state.1 = (bf16[256,128]{1,0:T(8,128)(2,1)}, bf16[256,128]{1,0:T(8,128)(2,1)}, bf16[16,144,128]{2,1,0:T(8,128)(2,1)}) custom-call(s32[3]{0:T(128)} %pad_add_fusion.z_ref.s_ref, bf16[4,512,256]{2,1,0:T(8,128)(2,1)} %copy-done.1, bf16[256,2048]{1,0:T(8,128)(2,1)} %get-tuple-element.27.normed_ref, f32[256,128]{1,0:T(8,128)} %get-tuple-element.28.cols_ref, ...), custom_call_target="tpu_custom_call" | custom-call | flops 2000000000 | tf_op jit(solution)/shard_map/state/pallas_call | solution.py:276
  74.7 9.6 %all-to-all-start.2 = ((bf16[16,144,128]{2,1,0:T(8,128)(2,1)}), bf16[16,144,128]{2,1,0:T(8,128)(2,1)S(1)}, u32[]{:S(2)}, u32[]{:S(2)}) async-start(bf16[16,144,128]{2,1,0:T(8,128)(2,1)} %get-tuple-element.30), calls=%async_computation.2 | async-start | bytes 1179648 | tf_op jit(solution)/shard_map/all_to_all | solution.py:334
  84.4 0.0 slice-start
  84.4 1.0 fusion
  85.3 0.1 slice-done
  85.5 0.1 pad_maximum_fusion.w0_ref
  85.5 2.2 %collective-permute-start = (bf16[512,512]{1,0:T(8,128)(2,1)S(1)}, bf16[512,512]{1,0:T(8,128)(2,1)S(1)}, u32[]{:S(2)}, u32[]{:S(2)}) collective-permute-start(bf16[512,512]{1,0:T(8,128)(2,1)S(1)} %slice.18.w0_ref), channel_id=1, source_target_pairs={{0,8},{8,16},{16,24},{24,0},{1,9},{9,17},{17,25},{25,1},{2,10},{10... | collective-permute-start | bytes 1572872 | tf_op jit(solution)/shard_map/ppermute | solution.py:43
  87.7 3.7 %collective-permute-start.1 = (bf16[512,512]{1,0:T(8,128)(2,1)S(1)}, bf16[512,512]{1,0:T(8,128)(2,1)S(1)}, u32[]{:S(2)}, u32[]{:S(2)}) collective-permute-start(bf16[512,512]{1,0:T(8,128)(2,1)S(1)} %slice.18.w0_ref), channel_id=1, source_target_pairs={{0,16},{8,24},{16,0},{24,8},{1,17},{9,25},{17,1},{25,9},{2,18},{10... | collective-permute-start | bytes 1572872 | tf_op jit(solution)/shard_map/ppermute | solution.py:43
  91.4 0.0 copy-done.3
  91.5 2.5 %collective-permute-start.2 = (bf16[512,512]{1,0:T(8,128)(2,1)S(1)}, bf16[512,512]{1,0:T(8,128)(2,1)S(1)}, u32[]{:S(2)}, u32[]{:S(2)}) collective-permute-start(bf16[512,512]{1,0:T(8,128)(2,1)S(1)} %slice.18.w0_ref), channel_id=1, source_target_pairs={{0,24},{8,0},{16,8},{24,16},{1,25},{9,1},{17,9},{25,17},{2,26},{10... | collective-permute-start | bytes 1572872 | tf_op jit(solution)/shard_map/ppermute | solution.py:43
  94.0 3.3 %collective-permute-start.3 = (bf16[8,2048]{1,0:T(8,128)(2,1)S(1)}, bf16[8,2048]{1,0:T(8,128)(2,1)S(1)}, u32[]{:S(2)}, u32[]{:S(2)}) collective-permute-start(bf16[8,2048]{1,0:T(8,128)(2,1)S(1)} %get-tuple-element.35), channel_id=1, source_target_pairs={{0,32},{32,64},{64,96},{96,128},{128,160},{160,192},{192,224},{224... | collective-permute-start | bytes 98312 | tf_op jit(solution)/shard_map/ppermute | solution.py:345
  97.3 1.3 collective-permute-start.4
  98.6 0.8 collective-permute-done.3.lo_ref
  99.3 2.2 %collective-permute-start.5 = (bf16[512,384]{1,0:T(8,128)(2,1)S(1)}, bf16[512,384]{1,0:T(8,128)(2,1)}, u32[]{:S(2)}, u32[]{:S(2)}) collective-permute-start(bf16[512,384]{1,0:T(8,128)(2,1)S(1)} %pad_maximum_fusion.w0_ref), channel_id=1, source_target_pairs={{0,8},{8,16},{16,24},{24,0},{1,9},{9,17},{17,25},{25,1},{2,10},{10... | collective-permute-start | bytes 1179656 | tf_op jit(solution)/shard_map/ppermute | solution.py:43
  101.5 5.1 %collective-permute-done.4.hi_ref = bf16[8,2048]{1,0:T(8,128)(2,1)S(1)} collective-permute-done((bf16[8,2048]{1,0:T(8,128)(2,1)S(1)}, bf16[8,2048]{1,0:T(8,128)(2,1)S(1)}, u32[]{:S(2)}, u32[]{:S(2)}) %collective-permute-start.4) | collective-permute-done | bytes 32800 | tf_op jit(solution)/shard_map/ppermute | solution.py:346
  106.6 2.1 %collective-permute-start.6 = (bf16[512,384]{1,0:T(8,128)(2,1)S(1)}, bf16[512,384]{1,0:T(8,128)(2,1)}, u32[]{:S(2)}, u32[]{:S(2)}) collective-permute-start(bf16[512,384]{1,0:T(8,128)(2,1)S(1)} %pad_maximum_fusion.w0_ref), channel_id=1, source_target_pairs={{0,16},{8,24},{16,0},{24,8},{1,17},{9,25},{17,1},{25,9},{2,18},{10... | collective-permute-start | bytes 1179656 | tf_op jit(solution)/shard_map/ppermute | solution.py:43
  108.8 0.0 collective-permute-done.w1_ref
  108.8 4.2 %collective-permute-start.7 = (bf16[512,384]{1,0:T(8,128)(2,1)S(1)}, bf16[512,384]{1,0:T(8,128)(2,1)}, u32[]{:S(2)}, u32[]{:S(2)}) collective-permute-start(bf16[512,384]{1,0:T(8,128)(2,1)S(1)} %pad_maximum_fusion.w0_ref), channel_id=1, source_target_pairs={{0,24},{8,0},{16,8},{24,16},{1,25},{9,1},{17,9},{25,17},{2,26},{10... | collective-permute-start | bytes 1179656 | tf_op jit(solution)/shard_map/ppermute | solution.py:43
  113.0 0.0 collective-permute-done.1.w2_ref
  113.0 0.0 collective-permute-done.2.w3_ref
  113.0 0.8 copy-done.9
  113.8 0.2 copy-done.10
  114.0 4.1 %local.1 = (bf16[256,128]{1,0:T(8,128)(2,1)}, bf16[256,128]{1,0:T(8,128)(2,1)}, bf16[256,256]{1,0:T(8,128)(2,1)}, f32[2,256,128]{2,1,0:T(8,128)}, f32[256,128]{1,0:T(8,128)}) custom-call(s32[3]{0:T(128)} %pad_add_fusion.z_ref.s_ref, bf16[512,512]{1,0:T(8,128)(2,1)} %copy-done.3, bf16[512,512]{1,0:T(8,128)(2,1)} %copy-done.8, bf16[512,512]{1,0:T(8,128)(2,1)} %copy-done.9, ...), custom_call_target="tpu_custom_call" | custom-call | flops 5000000000 | tf_op jit(solution)/shard_map/local/pallas_call | solution.py:276
  118.0 4.8 %collective-permute-done.5.w1_ref = bf16[512,384]{1,0:T(8,128)(2,1)} collective-permute-done((bf16[512,384]{1,0:T(8,128)(2,1)S(1)}, bf16[512,384]{1,0:T(8,128)(2,1)}, u32[]{:S(2)}, u32[]{:S(2)}) %collective-permute-start.5) | collective-permute-done | bytes 393248 | tf_op jit(solution)/shard_map/ppermute | solution.py:43
  122.8 0.0 collective-permute-done.6.w2_ref
  122.8 5.7 %collective-permute-done.7.w3_ref = bf16[512,384]{1,0:T(8,128)(2,1)} collective-permute-done((bf16[512,384]{1,0:T(8,128)(2,1)S(1)}, bf16[512,384]{1,0:T(8,128)(2,1)}, u32[]{:S(2)}, u32[]{:S(2)}) %collective-permute-start.7) | collective-permute-done | bytes 393248 | tf_op jit(solution)/shard_map/ppermute | solution.py:43
  128.5 0.0 all-to-all-done.2.got_ref
  128.5 0.8 copy-done.2
  129.4 5.2 %final.1 = bf16[256,2048]{1,0:T(8,128)(2,1)} custom-call(s32[3]{0:T(128)} %pad_add_fusion.z_ref.s_ref, bf16[16,144,128]{2,1,0:T(8,128)(2,1)} %copy-done.2, f32[2,128,128]{2,1,0:T(8,128)} %bitcast.20, f32[2,128]{1,0:T(2,128)} %bitcast.23, f32[256,128]{1,0:T(8,128)} %get-tuple-element.28.cols_ref, bf16[256,128]{1,0:T(8,128)(2,1)} %get-tuple-element.39.q_ref, ...), custom_call_target="tpu_custom_call" | custom-call | flops 2000000000 | tf_op jit(solution)/shard_map/final/pallas_call | solution.py:276
  134.5 24.5 %all_to_all.20 = bf16[8,32,2048]{2,1,0:T(8,128)(2,1)S(1)} all-to-all(bf16[8,32,2048]{2,1,0:T(8,128)(2,1)} %bitcast.15), channel_id=1, replica_groups=mesh['sp'=16,'fs'=4,'tp'=8] {'tp'}, dimensions={0} | all-to-all | bytes 2097152 | tf_op jit(solution)/shard_map/all_to_all | solution.py:370
  159.0 0.8 reduce_sum.12
  (21 shorter events, 0.1 us)
Async XLA Ops:
  1.4 53.7 %all-to-all-start = ((bf16[16,32,256]{2,1,0:T(8,128)(2,1)}), bf16[16,32,256]{2,1,0:T(8,128)(2,1)S(1)}, u32[]{:S(2)}, u32[]{:S(2)}) async-start(bf16[16,32,256]{2,1,0:T(8,128)(2,1)} %broadcast_in_dim.10), calls=%async_computation | async-start | bytes 524288 | tf_op jit(solution)/shard_map/all_to_all | solution.py:24
  55.1 29.2 %copy-start = (bf16[512,896]{1,0:T(8,128)(2,1)}, bf16[512,896]{1,0:T(8,128)(2,1)S(1)}, u32[]{:S(2)}) copy-start(bf16[512,896]{1,0:T(8,128)(2,1)S(1)} %all_gather.3) | copy-start | bytes 2752516
  56.3 4.3 %copy-start.7 = (f32[4,1]{0,1:T(1,128)S(1)}, f32[4,1]{0,1:T(1,128)}, u32[]{:S(2)}) copy-start(f32[4,1]{0,1:T(1,128)} %param.22) | copy-start | bytes 52
  56.3 14.1 %all-to-all-start.1 = ((bf16[4,512,256]{2,1,0:T(8,128)(2,1)}), bf16[4,512,256]{2,1,0:T(8,128)(2,1)S(1)}, u32[]{:S(2)}, u32[]{:S(2)}) async-start(bf16[4,512,256]{2,1,0:T(8,128)(2,1)} %broadcast_in_dim.11), calls=%async_computation.1 | async-start | bytes 2097152 | tf_op jit(solution)/shard_map/all_to_all | solution.py:24
  60.6 1.3 copy-start.5
  60.6 0.7 copy-start.6
  70.3 1.0 copy-start.1
  74.7 53.8 %all-to-all-start.2 = ((bf16[16,144,128]{2,1,0:T(8,128)(2,1)}), bf16[16,144,128]{2,1,0:T(8,128)(2,1)S(1)}, u32[]{:S(2)}, u32[]{:S(2)}) async-start(bf16[16,144,128]{2,1,0:T(8,128)(2,1)} %get-tuple-element.30), calls=%async_computation.2 | async-start | bytes 1179648 | tf_op jit(solution)/shard_map/all_to_all | solution.py:334
  84.3 7.1 %copy-start.3 = (bf16[512,512]{1,0:T(8,128)(2,1)}, bf16[512,512]{1,0:T(8,128)(2,1)S(1)}, u32[]{:S(2)}) copy-start(bf16[512,512]{1,0:T(8,128)(2,1)S(1)} %slice.18.w0_ref) | copy-start | bytes 1572868
  84.4 1.1 slice-start
  85.5 32.5 %copy-start.4 = (bf16[512,384]{1,0:T(8,128)(2,1)}, bf16[512,384]{1,0:T(8,128)(2,1)S(1)}, u32[]{:S(2)}) copy-start(bf16[512,384]{1,0:T(8,128)(2,1)S(1)} %pad_maximum_fusion.w0_ref) | copy-start | bytes 1179652
  85.5 23.2 %collective-permute-start = (bf16[512,512]{1,0:T(8,128)(2,1)S(1)}, bf16[512,512]{1,0:T(8,128)(2,1)S(1)}, u32[]{:S(2)}, u32[]{:S(2)}) collective-permute-start(bf16[512,512]{1,0:T(8,128)(2,1)S(1)} %slice.18.w0_ref), channel_id=1, source_target_pairs={{0,8},{8,16},{16,24},{24,0},{1,9},{9,17},{17,25},{25,1},{2,10},{10... | collective-permute-start | bytes 1572872 | tf_op jit(solution)/shard_map/ppermute | solution.py:43
  87.7 25.2 %collective-permute-start.1 = (bf16[512,512]{1,0:T(8,128)(2,1)S(1)}, bf16[512,512]{1,0:T(8,128)(2,1)S(1)}, u32[]{:S(2)}, u32[]{:S(2)}) collective-permute-start(bf16[512,512]{1,0:T(8,128)(2,1)S(1)} %slice.18.w0_ref), channel_id=1, source_target_pairs={{0,16},{8,24},{16,0},{24,8},{1,17},{9,25},{17,1},{25,9},{2,18},{10... | collective-permute-start | bytes 1572872 | tf_op jit(solution)/shard_map/ppermute | solution.py:43
  91.5 21.5 %collective-permute-start.2 = (bf16[512,512]{1,0:T(8,128)(2,1)S(1)}, bf16[512,512]{1,0:T(8,128)(2,1)S(1)}, u32[]{:S(2)}, u32[]{:S(2)}) collective-permute-start(bf16[512,512]{1,0:T(8,128)(2,1)S(1)} %slice.18.w0_ref), channel_id=1, source_target_pairs={{0,24},{8,0},{16,8},{24,16},{1,25},{9,1},{17,9},{25,17},{2,26},{10... | collective-permute-start | bytes 1572872 | tf_op jit(solution)/shard_map/ppermute | solution.py:43
  94.0 5.3 %collective-permute-start.3 = (bf16[8,2048]{1,0:T(8,128)(2,1)S(1)}, bf16[8,2048]{1,0:T(8,128)(2,1)S(1)}, u32[]{:S(2)}, u32[]{:S(2)}) collective-permute-start(bf16[8,2048]{1,0:T(8,128)(2,1)S(1)} %get-tuple-element.35), channel_id=1, source_target_pairs={{0,32},{32,64},{64,96},{96,128},{128,160},{160,192},{192,224},{224... | collective-permute-start | bytes 98312 | tf_op jit(solution)/shard_map/ppermute | solution.py:345
  97.3 9.3 %collective-permute-start.4 = (bf16[8,2048]{1,0:T(8,128)(2,1)S(1)}, bf16[8,2048]{1,0:T(8,128)(2,1)S(1)}, u32[]{:S(2)}, u32[]{:S(2)}) collective-permute-start(bf16[8,2048]{1,0:T(8,128)(2,1)S(1)} %get-tuple-element.36), channel_id=1, source_target_pairs={{32,0},{64,32},{96,64},{128,96},{160,128},{192,160},{224,192},{256... | collective-permute-start | bytes 98312 | tf_op jit(solution)/shard_map/ppermute | solution.py:346
  99.3 13.7 %copy-start.11 = (bf16[8,2048]{1,0:T(8,128)(2,1)}, bf16[8,2048]{1,0:T(8,128)(2,1)S(1)}, u32[]{:S(2)}) copy-start(bf16[8,2048]{1,0:T(8,128)(2,1)S(1)} %collective-permute-done.3.lo_ref) | copy-start | bytes 98308
  99.3 23.5 %collective-permute-start.5 = (bf16[512,384]{1,0:T(8,128)(2,1)S(1)}, bf16[512,384]{1,0:T(8,128)(2,1)}, u32[]{:S(2)}, u32[]{:S(2)}) collective-permute-start(bf16[512,384]{1,0:T(8,128)(2,1)S(1)} %pad_maximum_fusion.w0_ref), channel_id=1, source_target_pairs={{0,8},{8,16},{16,24},{24,0},{1,9},{9,17},{17,25},{25,1},{2,10},{10... | collective-permute-start | bytes 1179656 | tf_op jit(solution)/shard_map/ppermute | solution.py:43
  106.6 6.4 %copy-start.12 = (bf16[8,2048]{1,0:T(8,128)(2,1)}, bf16[8,2048]{1,0:T(8,128)(2,1)S(1)}, u32[]{:S(2)}) copy-start(bf16[8,2048]{1,0:T(8,128)(2,1)S(1)} %collective-permute-done.4.hi_ref) | copy-start | bytes 98308
  106.6 16.2 %collective-permute-start.6 = (bf16[512,384]{1,0:T(8,128)(2,1)S(1)}, bf16[512,384]{1,0:T(8,128)(2,1)}, u32[]{:S(2)}, u32[]{:S(2)}) collective-permute-start(bf16[512,384]{1,0:T(8,128)(2,1)S(1)} %pad_maximum_fusion.w0_ref), channel_id=1, source_target_pairs={{0,16},{8,24},{16,0},{24,8},{1,17},{9,25},{17,1},{25,9},{2,18},{10... | collective-permute-start | bytes 1179656 | tf_op jit(solution)/shard_map/ppermute | solution.py:43
  108.8 4.3 %copy-start.8 = (bf16[512,512]{1,0:T(8,128)(2,1)}, bf16[512,512]{1,0:T(8,128)(2,1)S(1)}, u32[]{:S(2)}) copy-start(bf16[512,512]{1,0:T(8,128)(2,1)S(1)} %collective-permute-done.w1_ref) | copy-start | bytes 1572868
  108.8 19.7 %collective-permute-start.7 = (bf16[512,384]{1,0:T(8,128)(2,1)S(1)}, bf16[512,384]{1,0:T(8,128)(2,1)}, u32[]{:S(2)}, u32[]{:S(2)}) collective-permute-start(bf16[512,384]{1,0:T(8,128)(2,1)S(1)} %pad_maximum_fusion.w0_ref), channel_id=1, source_target_pairs={{0,24},{8,0},{16,8},{24,16},{1,25},{9,1},{17,9},{25,17},{2,26},{10... | collective-permute-start | bytes 1179656 | tf_op jit(solution)/shard_map/ppermute | solution.py:43
  113.0 0.8 copy-start.9
  113.0 1.0 copy-start.10
  128.5 0.8 copy-start.2

commit v3 on v2

--- a/solution.py
+++ b/solution.py
@@ -4,6 +4,7 @@
 from jax.experimental import pallas as pl
 from jax.experimental.pallas import tpu as pltpu
 from jax.sharding import PartitionSpec as P
+
 
 HALO = 8
 norm_eps = 1e-06
@@ -24,7 +25,9 @@
     return lax.all_to_all(copies, axis, split_axis=0, concat_axis=0, tiled=True)
 
 
-def pack_kernel(k_ref, v_ref, q_ref, o_ref, p_ref, m_ref, out_ref):
+def pack_kernel(k_ref, v_ref, q_ref, o_ref, p_ref, m_ref, po_ref, out_ref, copies_ref):
+    for z in range(NZ):
+        copies_ref[z] = po_ref[...]
     at = 0
     for ref in (k_ref, v_ref, q_ref, o_ref, p_ref, m_ref):
         width = ref.shape[1]
@@ -38,9 +41,9 @@
     )
 
 
-def around(x, axis):
+def from_shift(x, axis, shift):
     count = lax.axis_size(axis)
-    return [x] + [lax.ppermute(x, axis, [(i, (i + s) % count) for i in range(count)]) for s in (1, 2, 3)]
+    return lax.ppermute(x, axis, [(i, (i + shift) % count) for i in range(count)])
 
 
 def placed_by_source(y, refs, out_ref):
@@ -56,7 +59,7 @@
     return jnp.minimum(x, 0.0) - jnp.log1p(jnp.exp(-jnp.abs(x)))
 
 
-def gates_kernel(tok_ref, gain_ref, gw_ref, bias_ref, decay_ref, normed_ref, cols_ref, rows_ref):
+def gates_kernel(bias_ref, tok_ref, gain_ref, gw_ref, decay_ref, normed_ref, cols_ref, rows_ref):
     x = tok_ref[...].astype(f32)
     count = x.shape[0]
     normed = rms_normed(x, gain_ref[...]).astype(bf16)
@@ -64,12 +67,9 @@
     pre = lax.dot_general(
         gw_ref[...], normed, (((1,), (1,)), ((), ())), preferred_element_type=f32
     )
-    pre = pre + bias_ref[...]
-    in_rows = (pre[0:1], pre[2:3])
-    lf_rows = (
-        log_sigmoid(pre[1:2]) + decay_ref[0:1],
-        log_sigmoid(pre[3:4]) + decay_ref[1:2],
-    )
+    pre = [pre[g : g + 1] + bias_ref[g] for g in range(4)]
+    in_rows = (pre[0], pre[2])
+    lf_rows = (log_sigmoid(pre[1]) + decay_ref[0], log_sigmoid(pre[3]) + decay_ref[1])
     stacked = jnp.concatenate(
         [in_rows[0], in_rows[1], lf_rows[0], lf_rows[1], jnp.zeros((124, count), f32)], axis=0
     )
@@ -110,8 +110,8 @@
     return [high, mid, low]
 
 
-def state_kernel(z_ref, w_ref, normed_ref, cols_ref, rows_ref, k_ref, v_ref, out_ref):
-    position = z_ref[0]
+def state_kernel(w_ref, normed_ref, cols_ref, rows_ref, k_ref, v_ref, out_ref):
+    position = lax.axis_index("sp")
     weight = in_order(w_ref)
     kv = jnp.dot(normed_ref[...], weight, preferred_element_type=f32).astype(bf16)
     k = kv[:, :128]
@@ -173,12 +173,14 @@
 
 
 def local_kernel(
-    s_ref, w0_ref, w1_ref, w2_ref, w3_ref, normed_ref, lo_ref, hi_ref, gain_ref,
+    w0_ref, w1_ref, w2_ref, w3_ref, normed_ref, lo_ref, hi_ref, gain_ref,
     k_ref, v_ref, cols_ref, rows_ref,
-    q_ref, o_ref, pool_ref, num_ref, den_ref, w_ref, a_ref, b_ref,
+    q_ref, o_ref, pool_ref, num_ref, den_ref, wm_ref, w_ref, a_ref, b_ref,
 ):
-    placed_by_source(s_ref[2], (w0_ref, w1_ref, w2_ref, w3_ref), w_ref)
+    placed_by_source(lax.axis_index("fs"), (w0_ref, w1_ref, w2_ref, w3_ref), w_ref)
     weight = in_order(w_ref)
+    wm_ref[...] = weight[:, 512:]
+    weight = weight[:, :512]
     halo = jnp.concatenate([lo_ref[...], hi_ref[...]], axis=0).astype(f32)
     halo = rms_normed(halo, gain_ref[...]).astype(bf16)
     left = jnp.concatenate([normed_ref[...], halo], axis=0)
@@ -189,7 +191,7 @@
     o_ref[...] = all_three[:count, 128:256]
     p = all_three[:, 256:512].astype(f32)
     pool_ref[...] = pooled(
-        s_ref[0], s_ref[1], p[:count], p[count : count + HALO], p[count + HALO :], a_ref, b_ref
+        lax.axis_index("sp"), lax.div(lax.axis_index("tp"), 2), p[:count], p[count : count + HALO], p[count + HALO :], a_ref, b_ref
     )
     scores = lax.dot_general(
         q, k_ref[...], (((1,), (1,)), ((), ())), preferred_element_type=f32
@@ -209,11 +211,11 @@
 
 
 def final_kernel(
-    s_ref, got_ref, mem_ref, nrm_ref, cols_ref, q_ref, o_ref, num_ref, den_ref,
-    gain_ref, pool_ref, w0_ref, w1_ref, w2_ref, w3_ref, out_ref, w_ref,
+    got_ref, mem_ref, nrm_ref, cols_ref, q_ref, o_ref, num_ref, den_ref,
+    gain_ref, pool_ref, wm_ref, w0_ref, w1_ref, w2_ref, w3_ref, keep_ref, give_ref, w_ref,
 ):
-    placed_by_source(s_ref[2], (w0_ref, w1_ref, w2_ref, w3_ref), w_ref)
-    position = s_ref[0]
+    placed_by_source(lax.axis_index("fs"), (w0_ref, w1_ref, w2_ref, w3_ref), w_ref)
+    position = lax.axis_index("sp")
     got_n, got_m, got_f = [], [], []
     for j in range(NZ):
         extra = got_ref[j, 128:PACKET].astype(f32)
@@ -237,7 +239,7 @@
             top = jnp.maximum(top, levels[j])
         share = jnp.exp(passed - top)
         memory = share * mem_ref[r]
-        norm = share * nrm_ref[r : r + 1]
+        norm = share * nrm_ref[r]
         for j in range(NZ):
             share = jnp.exp(levels[j] - top)
             memory = memory + share * got_ref[j, 0:128].astype(f32)
@@ -261,17 +263,24 @@
     scaled = summed * lax.rsqrt(jnp.mean(summed * summed, axis=-1, keepdims=True) + norm_eps)
     gate = 1.0 / (1.0 + jnp.exp(-o_ref[...].astype(f32)))
     memory_out = (scaled * gain_ref[...] * gate).astype(bf16)
-    weight = in_order(w_ref)
-    result = lax.dot_general(memory_out, weight[:, :128], last, preferred_element_type=f32)
-    result = result + lax.dot_general(pool_ref[...], weight[:, 128:], last, preferred_element_type=f32)
-    out_ref[...] = result.astype(bf16)
+    result = lax.dot_general(memory_out, wm_ref[...], last, preferred_element_type=f32)
+    result = result + lax.dot_general(
+        pool_ref[...], in_order(w_ref), last, preferred_element_type=f32
+    )
+    core = lax.rem(lax.axis_index("tp"), 2)
+    own = keep_ref.shape[1]
+    for x in range(keep_ref.shape[0]):
+        south = result[2 * x * own : (2 * x + 1) * own]
+        north = result[(2 * x + 1) * own : (2 * x + 2) * own]
+        keep_ref[x] = jnp.where(core == 0, south, north).astype(bf16)
+        give_ref[x] = jnp.where(core == 0, north, south).astype(bf16)
 
 
 def sds(shape, dtype):
     return jax.ShapeDtypeStruct(shape, dtype)
 
 
-def call(kernel, name, outs, scalars, *args, flops=0, scratch=()):
+def call(kernel, outs, scalars, *args, flops=0, scratch=()):
     many = isinstance(outs, tuple)
     return pl.pallas_call(
         kernel,
@@ -280,7 +289,6 @@
         out_shape=outs,
         scratch_shapes=list(scratch),
         cost_estimate=pl.CostEstimate(flops=flops, bytes_accessed=0, transcendentals=0),
-        name=name,
     )(*scalars, *args)
 
 
@@ -302,72 +310,77 @@
     pool_out_weight,
 ):
     count, width = tokens.shape[1:]
-    scalars = jnp.stack(
-        [lax.axis_index("sp"), lax.axis_index("tp") // 2, lax.axis_index("fs")]
-    ).astype(jnp.int32)
-    packed = call(
-        pack_kernel, "pack", sds((ROWS, 896), bf16), (),
+    packed, pool_copies = call(
+        pack_kernel, (sds((ROWS, 896), bf16), sds((NZ, ROWS, 256), bf16)), (),
         key_weight, value_weight, query_weight, outgate_weight, pool_weight, mem_out_weight,
+        pool_out_weight,
         flops=10**6,
     )
-    pool_z = from_everyone(pool_out_weight, "sp").reshape(NZ * ROWS, 256)
+    pool_z = lax.all_to_all(pool_copies, "sp", 0, 0, tiled=True).reshape(NZ * ROWS, 256)
     along_z = lax.all_gather(packed, "sp", axis=0, tiled=True)
     kv_z, pool_z = lax.optimization_barrier((along_z[:, :256], pool_z))
     kv_weight = from_everyone(kv_z, "fs")
     own_tokens, along_z = lax.optimization_barrier((tokens[0], along_z))
     normed, cols, rows = call(
-        gates_kernel, "gates",
-        (sds((count, width), bf16), sds((count, 128), f32), sds((8, count), f32)), (),
+        gates_kernel,
+        (sds((count, width), bf16), sds((count, 128), f32), sds((8, count), f32)),
+        (gate_bias.reshape(4),),
         own_tokens,
         norm_gain[None],
-        jnp.pad(gate_weight[:, 0], ((0, 4), (0, 0))),
-        jnp.pad(gate_bias, ((0, 4), (0, 0))),
-        decay_extra[0, :, 0],
+        gate_weight[:, 0],
+        decay_extra[0, :, 0][:, None],
         flops=4 * 10**9,
     )
+    first_rest, rows = lax.optimization_barrier((along_z[:, 256:], rows))
+    first_from = {}
+    for shift in (1, 3):
+        first_from[shift] = from_shift(first_rest, "fs", shift)
     k, v, packets = call(
-        state_kernel, "state",
+        state_kernel,
         (sds((count, 128), bf16), sds((count, 128), bf16), sds((NZ, PACKET, 128), bf16)),
-        (scalars,), kv_weight, normed, cols, rows,
+        (), kv_weight, normed, cols, rows,
         flops=2 * 10**9,
     )
     got = lax.all_to_all(packets, "sp", 0, 0, tiled=True)
-    ends, first_rest, last_rest, k = lax.optimization_barrier(
-        (
-            (own_tokens[:HALO], own_tokens[count - HALO :]),
-            along_z[:, 256:768],
-            jnp.concatenate([along_z[:, 768:], pool_z], axis=1),
-            k,
-        )
+    ends, later_rest, pool_z, k = lax.optimization_barrier(
+        ((own_tokens[:HALO], own_tokens[count - HALO :]), first_rest, pool_z, k)
     )
     length = lax.axis_size("sp")
-    first_rest = around(first_rest, "fs")
+    first_from[2] = from_shift(later_rest, "fs", 2)
     low = lax.ppermute(ends[1], "sp", [(i, i + 1) for i in range(length - 1)])
     high = lax.ppermute(ends[0], "sp", [(i + 1, i) for i in range(length - 1)])
-    last_rest = around(last_rest, "fs")
-    q, outgate, pool_out, nums, dens = call(
-        local_kernel, "local",
+    last_from = [pool_z] + [from_shift(pool_z, "fs", s) for s in (1, 2, 3)]
+    q, outgate, pool_out, nums, dens, wm = call(
+        local_kernel,
         (
             sds((count, 128), bf16),
             sds((count, 128), bf16),
             sds((count, 256), bf16),
             sds((2, count, 128), f32),
             sds((count, 128), f32),
+            sds((width, 128), bf16),
         ),
-        (scalars,), *first_rest, normed, low, high, norm_gain[None], k, v, cols, rows,
+        (), first_rest, first_from[1], first_from[2], first_from[3], normed, low, high,
+        norm_gain[None], k, v, cols, rows,
         flops=5 * 10**9,
-        scratch=[pltpu.VMEM((NY, NZ * ROWS, 512), bf16)]
+        scratch=[pltpu.VMEM((NY, NZ * ROWS, 640), bf16)]
         + [pltpu.VMEM((count + 32, 256), f32)] * 2,
     )
-    partial = call(
-        final_kernel, "final", sds((count, width), bf16), (scalars,),
-        got, init_memory[0, :, 0], init_normalizer[0, :, 0], cols, q, outgate,
-        nums, dens, head_gain, pool_out, *last_rest,
+    cores = 2
+    chips = lax.axis_size("tp") // cores
+    own = count // (chips * cores)
+    keep, give = call(
+        final_kernel, (sds((chips, own, width), bf16),) * 2, (),
+        got, init_memory[0, :, 0], init_normalizer[0, :, 0][:, None], cols, q, outgate,
+        nums, dens, head_gain, pool_out, wm, *last_from,
         flops=2 * 10**9,
-        scratch=[pltpu.VMEM((NY, NZ * ROWS, 384), bf16)],
-    )
-    own = count // lax.axis_size("tp")
-    parts = lax.all_to_all(partial.reshape(-1, own, width), "tp", 0, 0, tiled=True)
+        scratch=[pltpu.VMEM((NY, NZ * ROWS, 256), bf16)],
+    )
+    swap = [(i, i ^ 1) for i in range(chips * cores)]
+    taken = lax.ppermute(give, "tp", swap)
+    pairs = (keep.astype(f32) + taken.astype(f32)).astype(bf16)
+    groups = [list(range(c, chips * cores, cores)) for c in range(cores)]
+    parts = lax.all_to_all(pairs, "tp", 0, 0, axis_index_groups=groups, tiled=True)
     mixed = jnp.sum(parts.astype(f32), axis=0).astype(bf16)
     return mixed.reshape(1, own, width)
 
@@ -390,6 +403,7 @@
         P(("sp", "fs"), "tp"),
         P(("sp", "fs"), "tp"),
     )
+
     return jax.shard_map(
         per_device,
         mesh=mesh,

time: 161 us -> 165 us (1.025)
  starting transfers between devices: 51.1 us -> 69.9 us
  blocking collectives: 61 us -> 50.3 us
  local copies, waits for them, and re-layouts: 8.98 us -> 4.53 us
    ppermute x6 -> x7, starting transfers between devices: 16.9 us -> 35.8 us  [the longest x6 18.6 us: from_shift(): lax.ppermute(x, axis, [(i, (i + shift) % count) for i in range(count)])]
    all_to_all x2 -> x1, starting transfers between devices: 20 us -> 4.18 us  [from_everyone(): return lax.all_to_all(copies, axis, split_axis=0, concat_axis=0, tiled=True)]
    all_to_all x0 -> x1, starting transfers between devices: none -> 15.9 us  [per_device(): lax.all_to_all(pool_copies, 'sp', 0, 0, tiled=True).reshape(NZ * ROWS, 256)]
    all_to_all x1, blocking collectives: 24.5 us -> 12.4 us  [per_device(): lax.all_to_all(pairs, 'tp', 0, 0, axis_index_groups=groups, tiled=True)]
    ppermute x1, waiting for transfers between devices: 5.07 us -> 0.01 us  [per_device(): high = lax.ppermute(ends[0], 'sp', [(i + 1, i) for i in range(length - 1)])]
    all_to_all x2 -> x1, waiting for transfers between devices: 3.39 us -> 6.17 us  [from_everyone(): return lax.all_to_all(copies, axis, split_axis=0, concat_axis=0, tiled=True)]
    ppermute x6 -> x7, waiting for transfers between devices: 10.5 us -> 13.1 us  [the longest x6 11.4 us: from_shift(): lax.ppermute(x, axis, [(i, (i + shift) % count) for i in range(count)])]
    unnamed x28 -> x20, local copies, waits for them, and re-layouts: 4.03 us -> 2.65 us
  transfers between devices with their start and end apart: 11 -> 12, of which waited for: 5 -> 6; matrix products, arithmetic and copies ran while one was open for 2% -> 1% of each run, Pallas kernels for 5% -> 5%
where the time goes in v3:
time: 165 us; the launch traced here: 164 us
  starting transfers between devices  69.9 us (42%)
  blocking collectives  50.3 us (30%)
  waiting for transfers between devices  19.3 us (12%)
  Pallas kernels  17.9 us (11%)
  local copies, waits for them, and re-layouts  4.53 us (3%)
  other arithmetic  1.91 us (1%)
    all_gather x1, blocking collectives, per_device(): along_z = lax.all_gather(packed, 'sp', axis=0, tiled=True)  37.9 us
    ppermute x6, starting transfers between devices, from_shift(): lax.ppermute(x, axis, [(i, (i + shift) % count) for i in range(count)])  18.6 us
    pallas_call x5, Pallas kernels, call(): pl.pallas_call(kernel, in_specs=[smem] * len(scalars) + [vmem] * len(args...  17.9 us
    ppermute x1, starting transfers between devices, per_device(): taken = lax.ppermute(give, 'tp', swap)  17.1 us
    all_to_all x1, starting transfers between devices, per_device(): lax.all_to_all(pool_copies, 'sp', 0, 0, tiled=True).reshape(NZ * ROWS, 256)  15.9 us
    all_to_all x1, blocking collectives, per_device(): lax.all_to_all(pairs, 'tp', 0, 0, axis_index_groups=groups, tiled=True)  12.4 us
    ppermute x6, waiting for transfers between devices, from_shift(): lax.ppermute(x, axis, [(i, (i + shift) % count) for i in range(count)])  11.4 us
    all_to_all x1, starting transfers between devices, per_device(): got = lax.all_to_all(packets, 'sp', 0, 0, tiled=True)  9.59 us
  transfers between devices with their start and end apart: 12, of which 6 were waited for; matrix products, arithmetic and copies ran while one was open for 1% of the time, Pallas kernels for 5%

profile of v3, /device:TPU:1, one launch (start us, length us, event | category | flops | bytes accessed | tf_op | source)
XLA Modules:
  0.0 164.1 jit_solution(16607192907047643470)
XLA Ops:
  0.0 1.6 shard_map.145
  1.6 15.9 %all-to-all-start = ((bf16[16,32,256]{2,1,0:T(8,128)(2,1)}), bf16[16,32,256]{2,1,0:T(8,128)(2,1)S(1)}, u32[]{:S(2)}, u32[]{:S(2)}) async-start(bf16[16,32,256]{2,1,0:T(8,128)(2,1)} %get-tuple-element.33), calls=%async_computation | async-start | bytes 524288 | tf_op jit(solution)/shard_map/all_to_all | solution.py:319
  17.4 0.0 copy-done.4
  17.4 37.9 %all_gather.3 = bf16[512,896]{1,0:T(8,128)(2,1)S(1)} all-gather(bf16[32,896]{1,0:T(8,128)(2,1)S(1)} %copy-done.4), channel_id=1, replica_groups=mesh['sp'=16,'fs'=4,'tp'=8] {'sp'}, dimensions={0}, use_global_device_ids=true | all-gather | bytes 974848 | tf_op jit(solution)/shard_map/all_gather | solution.py:320
  55.4 0.0 all-to-all-done
  55.4 0.0 copy-start.3
  55.4 1.0 broadcast_in_dim.7
  56.4 4.2 %all-to-all-start.1 = ((bf16[4,512,256]{2,1,0:T(8,128)(2,1)}), bf16[4,512,256]{2,1,0:T(8,128)(2,1)S(1)}, u32[]{:S(2)}, u32[]{:S(2)}) async-start(bf16[4,512,256]{2,1,0:T(8,128)(2,1)} %broadcast_in_dim.7), calls=%async_computation.1 | async-start | bytes 2097152 | tf_op jit(solution)/shard_map/all_to_all | solution.py:25
  60.6 0.1 slice.13.w0_ref
  60.6 0.0 copy-start.1
  60.7 3.5 %shard_map.146 = (bf16[256,2048]{1,0:T(8,128)(2,1)}, f32[256,128]{1,0:T(8,128)}, f32[8,256]{1,0:T(8,128)}) custom-call(f32[4]{0:T(128)} %bitcast.21, bf16[256,2048]{1,0:T(8,128)(2,1)} %bitcast.13, f32[1,2048]{1,0:T(1,128)} %bitcast.17, bf16[4,2048]{1,0:T(4,128)(2,1)} %bitcast.16, f32[2,1,256]{2,1,0:T(1,128)} %bitcast.19), custom_call_target="tpu_custom_call" | custom-call | flops 4000000000 | tf_op jit(solution)/shard_map/pallas_call | solution.py:285
  64.2 6.2 %all-to-all-done.1.w_ref = bf16[4,512,256]{2,1,0:T(8,128)(2,1)S(1)} async-done(((bf16[4,512,256]{2,1,0:T(8,128)(2,1)}), bf16[4,512,256]{2,1,0:T(8,128)(2,1)S(1)}, u32[]{:S(2)}, u32[]{:S(2)}) %all-to-all-start.1) | async-done | bytes 1048608 | tf_op jit(solution)/shard_map/all_to_all | solution.py:25
  70.3 1.0 copy-done
  71.3 3.4 %shard_map.147 = (bf16[256,128]{1,0:T(8,128)(2,1)}, bf16[256,128]{1,0:T(8,128)(2,1)}, bf16[16,144,128]{2,1,0:T(8,128)(2,1)}) custom-call(bf16[4,512,256]{2,1,0:T(8,128)(2,1)} %copy-done, bf16[256,2048]{1,0:T(8,128)(2,1)} %get-tuple-element.36.normed_ref, f32[256,128]{1,0:T(8,128)} %get-tuple-element.37.cols_ref, f32[8,256]{1,0:T(8,128)} %get-tuple-element.40.rows_ref), custom_call_target="tpu_custom_call" | custom-call | flops 2000000000 | tf_op jit(solution)/shard_map/pallas_call | solution.py:285
  74.7 9.6 %all-to-all-start.2 = ((bf16[16,144,128]{2,1,0:T(8,128)(2,1)}), bf16[16,144,128]{2,1,0:T(8,128)(2,1)S(1)}, u32[]{:S(2)}, u32[]{:S(2)}) async-start(bf16[16,144,128]{2,1,0:T(8,128)(2,1)} %get-tuple-element.41), calls=%async_computation.2 | async-start | bytes 1179648 | tf_op jit(solution)/shard_map/all_to_all | solution.py:344
  84.3 2.2 %collective-permute-start = (bf16[512,640]{1,0:T(8,128)(2,1)S(1)}, bf16[512,640]{1,0:T(8,128)(2,1)S(1)}, u32[]{:S(2)}, u32[]{:S(2)}) collective-permute-start(bf16[512,640]{1,0:T(8,128)(2,1)S(1)} %slice.13.w0_ref), channel_id=1, source_target_pairs={{0,8},{8,16},{16,24},{24,0},{1,9},{9,17},{17,25},{25,1},{2,10},{10... | collective-permute-start | bytes 1966088 | tf_op jit(solution)/shard_map/ppermute | solution.py:46
  86.5 4.3 %collective-permute-start.2 = (bf16[512,640]{1,0:T(8,128)(2,1)S(1)}, bf16[512,640]{1,0:T(8,128)(2,1)S(1)}, u32[]{:S(2)}, u32[]{:S(2)}) collective-permute-start(bf16[512,640]{1,0:T(8,128)(2,1)S(1)} %slice.13.w0_ref), channel_id=1, source_target_pairs={{0,24},{8,0},{16,8},{24,16},{1,25},{9,1},{17,9},{25,17},{2,26},{10... | collective-permute-start | bytes 1966088 | tf_op jit(solution)/shard_map/ppermute | solution.py:46
  90.8 0.8 fusion
  91.6 0.0 copy-done.1
  91.6 1.9 %collective-permute-start.1 = (bf16[512,640]{1,0:T(8,128)(2,1)S(1)}, bf16[512,640]{1,0:T(8,128)(2,1)S(1)}, u32[]{:S(2)}, u32[]{:S(2)}) collective-permute-start(bf16[512,640]{1,0:T(8,128)(2,1)S(1)} %slice.13.w0_ref), channel_id=1, source_target_pairs={{0,16},{8,24},{16,0},{24,8},{1,17},{9,25},{17,1},{25,9},{2,18},{10... | collective-permute-start | bytes 1966088 | tf_op jit(solution)/shard_map/ppermute | solution.py:46
  93.5 3.3 %collective-permute-start.3 = (bf16[8,2048]{1,0:T(8,128)(2,1)S(1)}, bf16[8,2048]{1,0:T(8,128)(2,1)S(1)}, u32[]{:S(2)}, u32[]{:S(2)}) collective-permute-start(bf16[8,2048]{1,0:T(8,128)(2,1)S(1)} %get-tuple-element.46), channel_id=1, source_target_pairs={{0,32},{32,64},{64,96},{96,128},{128,160},{160,192},{192,224},{224... | collective-permute-start | bytes 98312 | tf_op jit(solution)/shard_map/ppermute | solution.py:350
  96.8 1.3 collective-permute-start.4
  98.1 0.0 collective-permute-done.w1_ref
  98.1 0.0 copy-start.5
  98.1 2.5 %collective-permute-start.5 = (bf16[512,256]{1,0:T(8,128)(2,1)S(1)}, bf16[512,256]{1,0:T(8,128)(2,1)}, u32[]{:S(2)}, u32[]{:S(2)}) collective-permute-start(bf16[512,256]{1,0:T(8,128)(2,1)S(1)} %bitcast.9), channel_id=1, source_target_pairs={{0,8},{8,16},{16,24},{24,0},{1,9},{9,17},{17,25},{25,1},{2,10},{10... | collective-permute-start | bytes 786440 | tf_op jit(solution)/shard_map/ppermute | solution.py:46
  100.6 1.5 collective-permute-done.2.w3_ref
  102.1 2.8 %collective-permute-start.6 = (bf16[512,256]{1,0:T(8,128)(2,1)S(1)}, bf16[512,256]{1,0:T(8,128)(2,1)}, u32[]{:S(2)}, u32[]{:S(2)}) collective-permute-start(bf16[512,256]{1,0:T(8,128)(2,1)S(1)} %bitcast.10), channel_id=1, source_target_pairs={{0,16},{8,24},{16,0},{24,8},{1,17},{9,25},{17,1},{25,9},{2,18},{10... | collective-permute-start | bytes 786440 | tf_op jit(solution)/shard_map/ppermute | solution.py:46
  104.9 0.0 collective-permute-done.3.lo_ref
  104.9 0.0 copy-done.3
  104.9 0.0 copy-start.8
  104.9 4.9 %collective-permute-start.7 = (bf16[512,256]{1,0:T(8,128)(2,1)S(1)}, bf16[512,256]{1,0:T(8,128)(2,1)}, u32[]{:S(2)}, u32[]{:S(2)}) collective-permute-start(bf16[512,256]{1,0:T(8,128)(2,1)S(1)} %bitcast.11), channel_id=1, source_target_pairs={{0,24},{8,0},{16,8},{24,16},{1,25},{9,1},{17,9},{25,17},{2,26},{10... | collective-permute-start | bytes 786440 | tf_op jit(solution)/shard_map/ppermute | solution.py:46
  109.8 0.0 collective-permute-done.4.hi_ref
  109.9 1.2 collective-permute-done.1.w2_ref
  111.1 0.0 copy-done.6
  111.1 0.0 copy-done.9
  111.1 0.8 copy-done.7
  112.0 4.4 %shard_map.148 = (bf16[256,128]{1,0:T(8,128)(2,1)}, bf16[256,128]{1,0:T(8,128)(2,1)}, bf16[256,256]{1,0:T(8,128)(2,1)}, f32[2,256,128]{2,1,0:T(8,128)}, f32[256,128]{1,0:T(8,128)}, /*index=5*/bf16[2048,128]{1,0:T(8,128)(2,1)}) custom-call(bf16[512,640]{1,0:T(8,128)(2,1)} %copy-done.1, bf16[512,640]{1,0:T(8,128)(2,1)} %copy-done.5, ...), custom_call_target="tpu_custom_call" | custom-call | flops 5000000000 | tf_op jit(solution)/shard_map/pallas_call | solution.py:285
  116.3 0.0 collective-permute-done.5.w1_ref
  116.3 6.1 %collective-permute-done.6.w2_ref = bf16[512,256]{1,0:T(8,128)(2,1)} collective-permute-done((bf16[512,256]{1,0:T(8,128)(2,1)S(1)}, bf16[512,256]{1,0:T(8,128)(2,1)}, u32[]{:S(2)}, u32[]{:S(2)}) %collective-permute-start.6) | collective-permute-done | bytes 262176 | tf_op jit(solution)/shard_map/ppermute | solution.py:46
  122.4 2.6 %collective-permute-done.7.w3_ref = bf16[512,256]{1,0:T(8,128)(2,1)} collective-permute-done((bf16[512,256]{1,0:T(8,128)(2,1)S(1)}, bf16[512,256]{1,0:T(8,128)(2,1)}, u32[]{:S(2)}, u32[]{:S(2)}) %collective-permute-start.7) | collective-permute-done | bytes 262176 | tf_op jit(solution)/shard_map/ppermute | solution.py:46
  125.0 0.0 all-to-all-done.2.got_ref
  125.0 0.8 copy-done.2
  125.8 5.1 %shard_map.149 = (bf16[4,32,2048]{2,1,0:T(8,128)(2,1)}, bf16[4,32,2048]{2,1,0:T(8,128)(2,1)}) custom-call(bf16[16,144,128]{2,1,0:T(8,128)(2,1)} %copy-done.2, f32[2,128,128]{2,1,0:T(8,128)} %bitcast.15, f32[2,1,128]{2,1,0:T(1,128)} %bitcast.20, f32[256,128]{1,0:T(8,128)} %get-tuple-element.37.cols_ref, bf16[256,128]{1,0:T(8,128)(2,1)} %get-tuple-element.50.q_ref, ...), custom_call_target="tpu_custom_call" | custom-call | flops 2000000000 | tf_op jit(solution)/shard_map/pallas_call | solution.py:285
  130.9 17.1 %collective-permute-start.8 = (bf16[4,32,2048]{2,1,0:T(8,128)(2,1)}, bf16[4,32,2048]{2,1,0:T(8,128)(2,1)S(1)}, u32[]{:S(2)}, u32[]{:S(2)}) collective-permute-start(bf16[4,32,2048]{2,1,0:T(8,128)(2,1)} %get-tuple-element.58), channel_id=1, source_target_pairs={{0,1},{1,0},{2,3},{3,2},{4,5},{5,4},{6,7},{7,6},{8,9},{9,8},{10,11... | collective-permute-start | bytes 1572872 | tf_op jit(solution)/shard_map/ppermute | solution.py:380
  148.0 1.7 %collective-permute-done.8 = bf16[4,32,2048]{2,1,0:T(8,128)(2,1)S(1)} collective-permute-done((bf16[4,32,2048]{2,1,0:T(8,128)(2,1)}, bf16[4,32,2048]{2,1,0:T(8,128)(2,1)S(1)}, u32[]{:S(2)}, u32[]{:S(2)}) %collective-permute-start.8) | collective-permute-done | bytes 524320 | tf_op jit(solution)/shard_map/ppermute | solution.py:380
  149.8 1.2 add_convert_fusion
  150.9 12.4 %all_to_all.20 = bf16[4,32,2048]{2,1,0:T(8,128)(2,1)S(1)} all-to-all(bf16[4,32,2048]{2,1,0:T(8,128)(2,1)S(1)} %add_convert_fusion), channel_id=1, replica_groups={{0,2,4,6},{1,3,5,7},{8,10,12,14},{9,11,13,15},{16,18,20,22},{17,19,21,2..., dimensions={0} | all-to-all | bytes 1048576 | tf_op jit(solution)/shard_map/all_to_all | solution.py:383
  163.4 0.7 reduce_sum.12
  (9 shorter events, 0.0 us)
Async XLA Ops:
  1.6 15.9 %copy-start.4 = (bf16[32,896]{1,0:T(8,128)(2,1)S(1)}, bf16[32,896]{1,0:T(8,128)(2,1)}, u32[]{:S(2)}) copy-start(bf16[32,896]{1,0:T(8,128)(2,1)} %get-tuple-element.32) | copy-start | bytes 172036
  1.6 53.8 %all-to-all-start = ((bf16[16,32,256]{2,1,0:T(8,128)(2,1)}), bf16[16,32,256]{2,1,0:T(8,128)(2,1)S(1)}, u32[]{:S(2)}, u32[]{:S(2)}) async-start(bf16[16,32,256]{2,1,0:T(8,128)(2,1)} %get-tuple-element.33), calls=%async_computation | async-start | bytes 524288 | tf_op jit(solution)/shard_map/all_to_all | solution.py:319
  55.4 49.5 %copy-start.3 = (bf16[16,32,256]{2,1,0:T(8,128)(2,1)}, bf16[16,32,256]{2,1,0:T(8,128)(2,1)S(1)}, u32[]{:S(2)}) copy-start(bf16[16,32,256]{2,1,0:T(8,128)(2,1)S(1)} %all-to-all-done) | copy-start | bytes 786436
  56.4 13.9 %all-to-all-start.1 = ((bf16[4,512,256]{2,1,0:T(8,128)(2,1)}), bf16[4,512,256]{2,1,0:T(8,128)(2,1)S(1)}, u32[]{:S(2)}, u32[]{:S(2)}) async-start(bf16[4,512,256]{2,1,0:T(8,128)(2,1)} %broadcast_in_dim.7), calls=%async_computation.1 | async-start | bytes 2097152 | tf_op jit(solution)/shard_map/all_to_all | solution.py:25
  60.6 30.9 %copy-start.1 = (bf16[512,640]{1,0:T(8,128)(2,1)}, bf16[512,640]{1,0:T(8,128)(2,1)S(1)}, u32[]{:S(2)}) copy-start(bf16[512,640]{1,0:T(8,128)(2,1)S(1)} %slice.13.w0_ref) | copy-start | bytes 1966084
  70.3 1.0 copy-start
  74.7 50.3 %all-to-all-start.2 = ((bf16[16,144,128]{2,1,0:T(8,128)(2,1)}), bf16[16,144,128]{2,1,0:T(8,128)(2,1)S(1)}, u32[]{:S(2)}, u32[]{:S(2)}) async-start(bf16[16,144,128]{2,1,0:T(8,128)(2,1)} %get-tuple-element.41), calls=%async_computation.2 | async-start | bytes 1179648 | tf_op jit(solution)/shard_map/all_to_all | solution.py:344
  84.3 13.8 %collective-permute-start = (bf16[512,640]{1,0:T(8,128)(2,1)S(1)}, bf16[512,640]{1,0:T(8,128)(2,1)S(1)}, u32[]{:S(2)}, u32[]{:S(2)}) collective-permute-start(bf16[512,640]{1,0:T(8,128)(2,1)S(1)} %slice.13.w0_ref), channel_id=1, source_target_pairs={{0,8},{8,16},{16,24},{24,0},{1,9},{9,17},{17,25},{25,1},{2,10},{10... | collective-permute-start | bytes 1966088 | tf_op jit(solution)/shard_map/ppermute | solution.py:46
  86.5 15.6 %collective-permute-start.2 = (bf16[512,640]{1,0:T(8,128)(2,1)S(1)}, bf16[512,640]{1,0:T(8,128)(2,1)S(1)}, u32[]{:S(2)}, u32[]{:S(2)}) collective-permute-start(bf16[512,640]{1,0:T(8,128)(2,1)S(1)} %slice.13.w0_ref), channel_id=1, source_target_pairs={{0,24},{8,0},{16,8},{24,16},{1,25},{9,1},{17,9},{25,17},{2,26},{10... | collective-permute-start | bytes 1966088 | tf_op jit(solution)/shard_map/ppermute | solution.py:46
  91.6 19.5 %collective-permute-start.1 = (bf16[512,640]{1,0:T(8,128)(2,1)S(1)}, bf16[512,640]{1,0:T(8,128)(2,1)S(1)}, u32[]{:S(2)}, u32[]{:S(2)}) collective-permute-start(bf16[512,640]{1,0:T(8,128)(2,1)S(1)} %slice.13.w0_ref), channel_id=1, source_target_pairs={{0,16},{8,24},{16,0},{24,8},{1,17},{9,25},{17,1},{25,9},{2,18},{10... | collective-permute-start | bytes 1966088 | tf_op jit(solution)/shard_map/ppermute | solution.py:46
  93.5 11.4 %collective-permute-start.3 = (bf16[8,2048]{1,0:T(8,128)(2,1)S(1)}, bf16[8,2048]{1,0:T(8,128)(2,1)S(1)}, u32[]{:S(2)}, u32[]{:S(2)}) collective-permute-start(bf16[8,2048]{1,0:T(8,128)(2,1)S(1)} %get-tuple-element.46), channel_id=1, source_target_pairs={{0,32},{32,64},{64,96},{96,128},{128,160},{160,192},{192,224},{224... | collective-permute-start | bytes 98312 | tf_op jit(solution)/shard_map/ppermute | solution.py:350
  96.8 13.1 %collective-permute-start.4 = (bf16[8,2048]{1,0:T(8,128)(2,1)S(1)}, bf16[8,2048]{1,0:T(8,128)(2,1)S(1)}, u32[]{:S(2)}, u32[]{:S(2)}) collective-permute-start(bf16[8,2048]{1,0:T(8,128)(2,1)S(1)} %get-tuple-element.47), channel_id=1, source_target_pairs={{32,0},{64,32},{96,64},{128,96},{160,128},{192,160},{224,192},{256... | collective-permute-start | bytes 98312 | tf_op jit(solution)/shard_map/ppermute | solution.py:351
  98.1 13.1 %copy-start.5 = (bf16[512,640]{1,0:T(8,128)(2,1)}, bf16[512,640]{1,0:T(8,128)(2,1)S(1)}, u32[]{:S(2)}) copy-start(bf16[512,640]{1,0:T(8,128)(2,1)S(1)} %collective-permute-done.w1_ref) | copy-start | bytes 1966084
  98.1 18.3 %collective-permute-start.5 = (bf16[512,256]{1,0:T(8,128)(2,1)S(1)}, bf16[512,256]{1,0:T(8,128)(2,1)}, u32[]{:S(2)}, u32[]{:S(2)}) collective-permute-start(bf16[512,256]{1,0:T(8,128)(2,1)S(1)} %bitcast.9), channel_id=1, source_target_pairs={{0,8},{8,16},{16,24},{24,0},{1,9},{9,17},{17,25},{25,1},{2,10},{10... | collective-permute-start | bytes 786440 | tf_op jit(solution)/shard_map/ppermute | solution.py:46
  102.1 9.1 %copy-start.6 = (bf16[512,640]{1,0:T(8,128)(2,1)}, bf16[512,640]{1,0:T(8,128)(2,1)S(1)}, u32[]{:S(2)}) copy-start(bf16[512,640]{1,0:T(8,128)(2,1)S(1)} %collective-permute-done.2.w3_ref) | copy-start | bytes 1966084
  102.1 20.3 %collective-permute-start.6 = (bf16[512,256]{1,0:T(8,128)(2,1)S(1)}, bf16[512,256]{1,0:T(8,128)(2,1)}, u32[]{:S(2)}, u32[]{:S(2)}) collective-permute-start(bf16[512,256]{1,0:T(8,128)(2,1)S(1)} %bitcast.10), channel_id=1, source_target_pairs={{0,16},{8,24},{16,0},{24,8},{1,17},{9,25},{17,1},{25,9},{2,18},{10... | collective-permute-start | bytes 786440 | tf_op jit(solution)/shard_map/ppermute | solution.py:46
  104.9 6.2 %copy-start.8 = (bf16[8,2048]{1,0:T(8,128)(2,1)}, bf16[8,2048]{1,0:T(8,128)(2,1)S(1)}, u32[]{:S(2)}) copy-start(bf16[8,2048]{1,0:T(8,128)(2,1)S(1)} %collective-permute-done.3.lo_ref) | copy-start | bytes 98308
  104.9 20.0 %collective-permute-start.7 = (bf16[512,256]{1,0:T(8,128)(2,1)S(1)}, bf16[512,256]{1,0:T(8,128)(2,1)}, u32[]{:S(2)}, u32[]{:S(2)}) collective-permute-start(bf16[512,256]{1,0:T(8,128)(2,1)S(1)} %bitcast.11), channel_id=1, source_target_pairs={{0,24},{8,0},{16,8},{24,16},{1,25},{9,1},{17,9},{25,17},{2,26},{10... | collective-permute-start | bytes 786440 | tf_op jit(solution)/shard_map/ppermute | solution.py:46
  109.9 1.3 copy-start.9
  111.1 0.8 copy-start.7
  125.0 0.8 copy-start.2
  130.9 18.9 %collective-permute-start.8 = (bf16[4,32,2048]{2,1,0:T(8,128)(2,1)}, bf16[4,32,2048]{2,1,0:T(8,128)(2,1)S(1)}, u32[]{:S(2)}, u32[]{:S(2)}) collective-permute-start(bf16[4,32,2048]{2,1,0:T(8,128)(2,1)} %get-tuple-element.58), channel_id=1, source_target_pairs={{0,1},{1,0},{2,3},{3,2},{4,5},{5,4},{6,7},{7,6},{8,9},{9,8},{10,11... | collective-permute-start | bytes 1572872 | tf_op jit(solution)/shard_map/ppermute | solution.py:380

commit v4 on v3

--- a/solution.py
+++ b/solution.py
@@ -59,8 +59,10 @@
     return jnp.minimum(x, 0.0) - jnp.log1p(jnp.exp(-jnp.abs(x)))
 
 
-def gates_kernel(bias_ref, tok_ref, gain_ref, gw_ref, decay_ref, normed_ref, cols_ref, rows_ref):
+def gates_kernel(bias_ref, tok_ref, gain_ref, gw_ref, decay_ref, normed_ref, cols_ref, rows_ref, ends_ref):
     x = tok_ref[...].astype(f32)
+    ends_ref[:HALO] = tok_ref[:HALO]
+    ends_ref[HALO:] = tok_ref[tok_ref.shape[0] - HALO :]
     count = x.shape[0]
     normed = rms_normed(x, gain_ref[...]).astype(bf16)
     normed_ref[...] = normed
@@ -175,12 +177,10 @@
 def local_kernel(
     w0_ref, w1_ref, w2_ref, w3_ref, normed_ref, lo_ref, hi_ref, gain_ref,
     k_ref, v_ref, cols_ref, rows_ref,
-    q_ref, o_ref, pool_ref, num_ref, den_ref, wm_ref, w_ref, a_ref, b_ref,
+    q_ref, o_ref, pool_ref, num_ref, den_ref, w_ref, a_ref, b_ref,
 ):
     placed_by_source(lax.axis_index("fs"), (w0_ref, w1_ref, w2_ref, w3_ref), w_ref)
     weight = in_order(w_ref)
-    wm_ref[...] = weight[:, 512:]
-    weight = weight[:, :512]
     halo = jnp.concatenate([lo_ref[...], hi_ref[...]], axis=0).astype(f32)
     halo = rms_normed(halo, gain_ref[...]).astype(bf16)
     left = jnp.concatenate([normed_ref[...], halo], axis=0)
@@ -212,7 +212,7 @@
 
 def final_kernel(
     got_ref, mem_ref, nrm_ref, cols_ref, q_ref, o_ref, num_ref, den_ref,
-    gain_ref, pool_ref, wm_ref, w0_ref, w1_ref, w2_ref, w3_ref, keep_ref, give_ref, w_ref,
+    gain_ref, pool_ref, w0_ref, w1_ref, w2_ref, w3_ref, keep_ref, give_ref, w_ref,
 ):
     placed_by_source(lax.axis_index("fs"), (w0_ref, w1_ref, w2_ref, w3_ref), w_ref)
     position = lax.axis_index("sp")
@@ -263,10 +263,8 @@
     scaled = summed * lax.rsqrt(jnp.mean(summed * summed, axis=-1, keepdims=True) + norm_eps)
     gate = 1.0 / (1.0 + jnp.exp(-o_ref[...].astype(f32)))
     memory_out = (scaled * gain_ref[...] * gate).astype(bf16)
-    result = lax.dot_general(memory_out, wm_ref[...], last, preferred_element_type=f32)
-    result = result + lax.dot_general(
-        pool_ref[...], in_order(w_ref), last, preferred_element_type=f32
-    )
+    features = jnp.concatenate([memory_out, pool_ref[...]], axis=1)
+    result = lax.dot_general(features, in_order(w_ref), last, preferred_element_type=f32)
     core = lax.rem(lax.axis_index("tp"), 2)
     own = keep_ref.shape[1]
     for x in range(keep_ref.shape[0]):
@@ -321,9 +319,14 @@
     kv_z, pool_z = lax.optimization_barrier((along_z[:, :256], pool_z))
     kv_weight = from_everyone(kv_z, "fs")
     own_tokens, along_z = lax.optimization_barrier((tokens[0], along_z))
-    normed, cols, rows = call(
+    normed, cols, rows, ends = call(
         gates_kernel,
-        (sds((count, width), bf16), sds((count, 128), f32), sds((8, count), f32)),
+        (
+            sds((count, width), bf16),
+            sds((count, 128), f32),
+            sds((8, count), f32),
+            sds((2 * HALO, width), bf16),
+        ),
         (gate_bias.reshape(4),),
         own_tokens,
         norm_gain[None],
@@ -331,9 +334,9 @@
         decay_extra[0, :, 0][:, None],
         flops=4 * 10**9,
     )
-    first_rest, rows = lax.optimization_barrier((along_z[:, 256:], rows))
+    first_rest, rows = lax.optimization_barrier((along_z[:, 256:768], rows))
     first_from = {}
-    for shift in (1, 3):
+    for shift in (1, 2, 3):
         first_from[shift] = from_shift(first_rest, "fs", shift)
     k, v, packets = call(
         state_kernel,
@@ -342,15 +345,16 @@
         flops=2 * 10**9,
     )
     got = lax.all_to_all(packets, "sp", 0, 0, tiled=True)
-    ends, later_rest, pool_z, k = lax.optimization_barrier(
-        ((own_tokens[:HALO], own_tokens[count - HALO :]), first_rest, pool_z, k)
+    last_rest, k = lax.optimization_barrier(
+        (jnp.concatenate([along_z[:, 768:], pool_z], axis=1), k)
     )
     length = lax.axis_size("sp")
-    first_from[2] = from_shift(later_rest, "fs", 2)
-    low = lax.ppermute(ends[1], "sp", [(i, i + 1) for i in range(length - 1)])
-    high = lax.ppermute(ends[0], "sp", [(i + 1, i) for i in range(length - 1)])
-    last_from = [pool_z] + [from_shift(pool_z, "fs", s) for s in (1, 2, 3)]
-    q, outgate, pool_out, nums, dens, wm = call(
+    last_from = [last_rest]
+    for shift in (1, 2, 3):
+        last_from.append(from_shift(last_rest, "fs", shift))
+    low = lax.ppermute(ends[HALO:], "sp", [(i, i + 1) for i in range(length - 1)])
+    high = lax.ppermute(ends[:HALO], "sp", [(i + 1, i) for i in range(length - 1)])
+    q, outgate, pool_out, nums, dens = call(
         local_kernel,
         (
             sds((count, 128), bf16),
@@ -358,12 +362,11 @@
             sds((count, 256), bf16),
             sds((2, count, 128), f32),
             sds((count, 128), f32),
-            sds((width, 128), bf16),
         ),
-        (), first_rest, first_from[1], first_from[2], first_from[3], normed, low, high,
+        (), first_rest, *(first_from[s] for s in (1, 2, 3)), normed, low, high,
         norm_gain[None], k, v, cols, rows,
         flops=5 * 10**9,
-        scratch=[pltpu.VMEM((NY, NZ * ROWS, 640), bf16)]
+        scratch=[pltpu.VMEM((NY, NZ * ROWS, 512), bf16)]
         + [pltpu.VMEM((count + 32, 256), f32)] * 2,
     )
     cores = 2
@@ -372,9 +375,9 @@
     keep, give = call(
         final_kernel, (sds((chips, own, width), bf16),) * 2, (),
         got, init_memory[0, :, 0], init_normalizer[0, :, 0][:, None], cols, q, outgate,
-        nums, dens, head_gain, pool_out, wm, *last_from,
+        nums, dens, head_gain, pool_out, *last_from,
         flops=2 * 10**9,
-        scratch=[pltpu.VMEM((NY, NZ * ROWS, 256), bf16)],
+        scratch=[pltpu.VMEM((NY, NZ * ROWS, 384), bf16)],
     )
     swap = [(i, i ^ 1) for i in range(chips * cores)]
     taken = lax.ppermute(give, "tp", swap)

time: 165 us -> 158 us (0.958)
  starting transfers between devices: 69.9 us -> 58.8 us
  waiting for transfers between devices: 19.3 us -> 23.7 us
    ppermute x1, starting transfers between devices: 17.1 us -> 5.46 us  [per_device(): taken = lax.ppermute(give, 'tp', swap)]
    ppermute x2, waiting for transfers between devices: 0.01 us -> 5.25 us  [the longest x1 5.25 us: per_device(): lax.ppermute(ends[:HALO], 'sp', [(i + 1, i) for i in range(length - 1)])]
  transfers between devices with their start and end apart: 12 -> 12, of which waited for: 6 -> 5; matrix products, arithmetic and copies ran while one was open for 1% -> 0% of each run, Pallas kernels for 5% -> 5%
where the time goes in v4:
time: 158 us; the launch traced here: 157 us
  starting transfers between devices  58.8 us (37%)
  blocking collectives  50.3 us (32%)
  waiting for transfers between devices  23.7 us (15%)
  Pallas kernels  17.8 us (11%)
  local copies, waits for them, and re-layouts  3.87 us (2%)
  other arithmetic  1.96 us (1%)
    all_gather x1, blocking collectives, per_device(): along_z = lax.all_gather(packed, 'sp', axis=0, tiled=True)  37.9 us
    ppermute x6, starting transfers between devices, from_shift(): lax.ppermute(x, axis, [(i, (i + shift) % count) for i in range(count)])  19 us
    pallas_call x5, Pallas kernels, call(): pl.pallas_call(kernel, in_specs=[smem] * len(scalars) + [vmem] * len(args...  17.8 us
    all_to_all x1, starting transfers between devices, per_device(): lax.all_to_all(pool_copies, 'sp', 0, 0, tiled=True).reshape(NZ * ROWS, 256)  15.9 us
    all_to_all x1, blocking collectives, per_device(): lax.all_to_all(pairs, 'tp', 0, 0, axis_index_groups=groups, tiled=True)  12.4 us
    ppermute x6, waiting for transfers between devices, from_shift(): lax.ppermute(x, axis, [(i, (i + shift) % count) for i in range(count)])  10.5 us
    all_to_all x1, starting transfers between devices, per_device(): got = lax.all_to_all(packets, 'sp', 0, 0, tiled=True)  9.72 us
    all_to_all x1, waiting for transfers between devices, from_everyone(): return lax.all_to_all(copies, axis, split_axis=0, concat_axis=0, tiled=True)  6.23 us
  transfers between devices with their start and end apart: 12, of which 5 were waited for; matrix products, arithmetic and copies ran while one was open for 0% of the time, Pallas kernels for 5%

profile of v4, /device:TPU:1, one launch (start us, length us, event | category | flops | bytes accessed | tf_op | source)
XLA Modules:
  0.0 156.8 jit_solution(16851688565470095402)
XLA Ops:
  0.0 1.5 shard_map.145
  1.6 15.9 %all-to-all-start = ((bf16[16,32,256]{2,1,0:T(8,128)(2,1)}), bf16[16,32,256]{2,1,0:T(8,128)(2,1)S(1)}, u32[]{:S(2)}, u32[]{:S(2)}) async-start(bf16[16,32,256]{2,1,0:T(8,128)(2,1)} %get-tuple-element.30), calls=%async_computation | async-start | bytes 524288 | tf_op jit(solution)/shard_map/all_to_all | solution.py:317
  17.4 0.0 copy-done.5
  17.4 37.9 %all_gather.3 = bf16[512,896]{1,0:T(8,128)(2,1)S(1)} all-gather(bf16[32,896]{1,0:T(8,128)(2,1)S(1)} %copy-done.5), channel_id=1, replica_groups=mesh['sp'=16,'fs'=4,'tp'=8] {'sp'}, dimensions={0}, use_global_device_ids=true | all-gather | bytes 974848 | tf_op jit(solution)/shard_map/all_gather | solution.py:318
  55.4 0.0 all-to-all-done
  55.4 1.0 broadcast_in_dim.7
  56.4 4.2 %all-to-all-start.1 = ((bf16[4,512,256]{2,1,0:T(8,128)(2,1)}), bf16[4,512,256]{2,1,0:T(8,128)(2,1)S(1)}, u32[]{:S(2)}, u32[]{:S(2)}) async-start(bf16[4,512,256]{2,1,0:T(8,128)(2,1)} %broadcast_in_dim.7), calls=%async_computation.1 | async-start | bytes 2097152 | tf_op jit(solution)/shard_map/all_to_all | solution.py:25
  60.6 0.0 copy-start.2
  60.6 3.5 %shard_map.146 = (bf16[256,2048]{1,0:T(8,128)(2,1)}, f32[256,128]{1,0:T(8,128)}, f32[8,256]{1,0:T(8,128)}, bf16[16,2048]{1,0:T(8,128)(2,1)}) custom-call(f32[4]{0:T(128)} %bitcast.17, bf16[256,2048]{1,0:T(8,128)(2,1)} %bitcast.10, f32[1,2048]{1,0:T(1,128)} %bitcast.13, bf16[4,2048]{1,0:T(4,128)(2,1)} %bitcast.12, f32[2,1,256]{2,1,0:T(1,128)} %bitcast.15), custom_call_target="tpu_custom_call" | custom-call | flops 4000000000 | tf_op jit(solution)/shard_map/pallas_call | solution.py:283
  64.1 6.2 %all-to-all-done.1.w_ref = bf16[4,512,256]{2,1,0:T(8,128)(2,1)S(1)} async-done(((bf16[4,512,256]{2,1,0:T(8,128)(2,1)}), bf16[4,512,256]{2,1,0:T(8,128)(2,1)S(1)}, u32[]{:S(2)}, u32[]{:S(2)}) %all-to-all-start.1) | async-done | bytes 1048608 | tf_op jit(solution)/shard_map/all_to_all | solution.py:25
  70.3 1.0 copy-done
  71.3 3.4 %shard_map.147 = (bf16[256,128]{1,0:T(8,128)(2,1)}, bf16[256,128]{1,0:T(8,128)(2,1)}, bf16[16,144,128]{2,1,0:T(8,128)(2,1)}) custom-call(bf16[4,512,256]{2,1,0:T(8,128)(2,1)} %copy-done, bf16[256,2048]{1,0:T(8,128)(2,1)} %get-tuple-element.33.normed_ref, f32[256,128]{1,0:T(8,128)} %get-tuple-element.34.cols_ref, f32[8,256]{1,0:T(8,128)} %get-tuple-element.37.rows_ref), custom_call_target="tpu_custom_call" | custom-call | flops 2000000000 | tf_op jit(solution)/shard_map/pallas_call | solution.py:283
  74.7 9.7 %all-to-all-start.2 = ((bf16[16,144,128]{2,1,0:T(8,128)(2,1)}), bf16[16,144,128]{2,1,0:T(8,128)(2,1)S(1)}, u32[]{:S(2)}, u32[]{:S(2)}) async-start(bf16[16,144,128]{2,1,0:T(8,128)(2,1)} %get-tuple-element.38), calls=%async_computation.2 | async-start | bytes 1179648 | tf_op jit(solution)/shard_map/all_to_all | solution.py:347
  84.4 2.2 %collective-permute-start = (bf16[512,512]{1,0:T(8,128)(2,1)S(1)}, bf16[512,512]{1,0:T(8,128)(2,1)S(1)}, u32[]{:S(2)}, u32[]{:S(2)}) collective-permute-start(bf16[512,512]{1,0:T(8,128)(2,1)S(1)} %slice.16.w0_ref), channel_id=1, source_target_pairs={{0,8},{8,16},{16,24},{24,0},{1,9},{9,17},{17,25},{25,1},{2,10},{10... | collective-permute-start | bytes 1572872 | tf_op jit(solution)/shard_map/ppermute | solution.py:46
  86.6 3.7 %collective-permute-start.1 = (bf16[512,512]{1,0:T(8,128)(2,1)S(1)}, bf16[512,512]{1,0:T(8,128)(2,1)S(1)}, u32[]{:S(2)}, u32[]{:S(2)}) collective-permute-start(bf16[512,512]{1,0:T(8,128)(2,1)S(1)} %slice.16.w0_ref), channel_id=1, source_target_pairs={{0,16},{8,24},{16,0},{24,8},{1,17},{9,25},{17,1},{25,9},{2,18},{10... | collective-permute-start | bytes 1572872 | tf_op jit(solution)/shard_map/ppermute | solution.py:46
  90.3 0.0 copy-done.2
  90.3 2.5 %collective-permute-start.2 = (bf16[512,512]{1,0:T(8,128)(2,1)S(1)}, bf16[512,512]{1,0:T(8,128)(2,1)S(1)}, u32[]{:S(2)}, u32[]{:S(2)}) collective-permute-start(bf16[512,512]{1,0:T(8,128)(2,1)S(1)} %slice.16.w0_ref), channel_id=1, source_target_pairs={{0,24},{8,0},{16,8},{24,16},{1,25},{9,1},{17,9},{25,17},{2,26},{10... | collective-permute-start | bytes 1572872 | tf_op jit(solution)/shard_map/ppermute | solution.py:46
  92.9 0.0 copy-done.4
  92.9 3.3 %collective-permute-start.3 = (bf16[8,2048]{1,0:T(8,128)(2,1)S(1)}, bf16[8,2048]{1,0:T(8,128)(2,1)S(1)}, u32[]{:S(2)}, u32[]{:S(2)}) collective-permute-start(bf16[8,2048]{1,0:T(8,128)(2,1)S(1)} %get-tuple-element.54), channel_id=1, source_target_pairs={{0,32},{32,64},{64,96},{96,128},{128,160},{160,192},{192,224},{224... | collective-permute-start | bytes 98312 | tf_op jit(solution)/shard_map/ppermute | solution.py:355
  96.2 1.3 collective-permute-start.4
  97.5 0.1 pad_maximum_fusion.w0_ref
  97.5 0.0 copy-start.3
  97.5 0.0 collective-permute-done.3.lo_ref
  97.6 0.0 copy-start.10
  97.6 4.1 %collective-permute-start.5 = (bf16[512,384]{1,0:T(8,128)(2,1)S(1)}, bf16[512,384]{1,0:T(8,128)(2,1)S(1)}, u32[]{:S(2)}, u32[]{:S(2)}) collective-permute-start(bf16[512,384]{1,0:T(8,128)(2,1)S(1)} %pad_maximum_fusion.w0_ref), channel_id=1, source_target_pairs={{0,8},{8,16},{16,24},{24,0},{1,9},{9,17},{17,25},{25,1},{2,10},{10... | collective-permute-start | bytes 1179656 | tf_op jit(solution)/shard_map/ppermute | solution.py:46
  101.7 5.2 %collective-permute-done.4.hi_ref = bf16[8,2048]{1,0:T(8,128)(2,1)S(1)} collective-permute-done((bf16[8,2048]{1,0:T(8,128)(2,1)S(1)}, bf16[8,2048]{1,0:T(8,128)(2,1)S(1)}, u32[]{:S(2)}, u32[]{:S(2)}) %collective-permute-start.4) | collective-permute-done | bytes 32800 | tf_op jit(solution)/shard_map/ppermute | solution.py:356
  106.9 1.9 %collective-permute-start.6 = (bf16[512,384]{1,0:T(8,128)(2,1)S(1)}, bf16[512,384]{1,0:T(8,128)(2,1)}, u32[]{:S(2)}, u32[]{:S(2)}) collective-permute-start(bf16[512,384]{1,0:T(8,128)(2,1)S(1)} %pad_maximum_fusion.w0_ref), channel_id=1, source_target_pairs={{0,16},{8,24},{16,0},{24,8},{1,17},{9,25},{17,1},{25,9},{2,18},{10... | collective-permute-start | bytes 1179656 | tf_op jit(solution)/shard_map/ppermute | solution.py:46
  108.8 0.0 collective-permute-done.w1_ref
  108.8 0.0 copy-start.6
  108.8 4.6 %collective-permute-start.7 = (bf16[512,384]{1,0:T(8,128)(2,1)S(1)}, bf16[512,384]{1,0:T(8,128)(2,1)}, u32[]{:S(2)}, u32[]{:S(2)}) collective-permute-start(bf16[512,384]{1,0:T(8,128)(2,1)S(1)} %pad_maximum_fusion.w0_ref), channel_id=1, source_target_pairs={{0,24},{8,0},{16,8},{24,16},{1,25},{9,1},{17,9},{25,17},{2,26},{10... | collective-permute-start | bytes 1179656 | tf_op jit(solution)/shard_map/ppermute | solution.py:46
  113.5 0.0 collective-permute-done.1.w2_ref
  113.5 0.0 collective-permute-done.2.w3_ref
  113.5 0.8 copy-done.8
  114.3 0.0 copy-done.11
  114.3 0.1 copy-done.7
  114.5 4.1 %shard_map.148 = (bf16[256,128]{1,0:T(8,128)(2,1)}, bf16[256,128]{1,0:T(8,128)(2,1)}, bf16[256,256]{1,0:T(8,128)(2,1)}, f32[2,256,128]{2,1,0:T(8,128)}, f32[256,128]{1,0:T(8,128)}) custom-call(bf16[512,512]{1,0:T(8,128)(2,1)} %copy-done.2, bf16[512,512]{1,0:T(8,128)(2,1)} %copy-done.6, bf16[512,512]{1,0:T(8,128)(2,1)} %copy-done.7, ...), custom_call_target="tpu_custom_call" | custom-call | flops 5000000000 | tf_op jit(solution)/shard_map/pallas_call | solution.py:283
  118.6 0.0 copy-done.3
  118.6 3.0 %collective-permute-done.5.w1_ref = bf16[512,384]{1,0:T(8,128)(2,1)S(1)} collective-permute-done((bf16[512,384]{1,0:T(8,128)(2,1)S(1)}, bf16[512,384]{1,0:T(8,128)(2,1)S(1)}, u32[]{:S(2)}, u32[]{:S(2)}) %collective-permute-start.5) | collective-permute-done | bytes 393248 | tf_op jit(solution)/shard_map/ppermute | solution.py:46
  121.6 0.0 collective-permute-done.6.w2_ref
  121.6 7.5 %collective-permute-done.7.w3_ref = bf16[512,384]{1,0:T(8,128)(2,1)} collective-permute-done((bf16[512,384]{1,0:T(8,128)(2,1)S(1)}, bf16[512,384]{1,0:T(8,128)(2,1)}, u32[]{:S(2)}, u32[]{:S(2)}) %collective-permute-start.7) | collective-permute-done | bytes 393248 | tf_op jit(solution)/shard_map/ppermute | solution.py:46
  129.1 0.0 all-to-all-done.2.got_ref
  129.1 0.8 copy-done.1
  129.9 5.3 %shard_map.149 = (bf16[4,32,2048]{2,1,0:T(8,128)(2,1)}, bf16[4,32,2048]{2,1,0:T(8,128)(2,1)}) custom-call(bf16[16,144,128]{2,1,0:T(8,128)(2,1)} %copy-done.1, f32[2,128,128]{2,1,0:T(8,128)} %bitcast.11, f32[2,1,128]{2,1,0:T(1,128)} %bitcast.16, f32[256,128]{1,0:T(8,128)} %get-tuple-element.34.cols_ref, bf16[256,128]{1,0:T(8,128)(2,1)} %get-tuple-element.45.q_ref, ...), custom_call_target="tpu_custom_call" | custom-call | flops 2000000000 | tf_op jit(solution)/shard_map/pallas_call | solution.py:283
  135.2 5.5 %collective-permute-start.8 = (bf16[4,32,2048]{2,1,0:T(8,128)(2,1)}, bf16[4,32,2048]{2,1,0:T(8,128)(2,1)S(1)}, u32[]{:S(2)}, u32[]{:S(2)}) collective-permute-start(bf16[4,32,2048]{2,1,0:T(8,128)(2,1)} %get-tuple-element.52), channel_id=1, source_target_pairs={{0,1},{1,0},{2,3},{3,2},{4,5},{5,4},{6,7},{7,6},{8,9},{9,8},{10,11... | collective-permute-start | bytes 1572872 | tf_op jit(solution)/shard_map/ppermute | solution.py:383
  140.7 1.7 %collective-permute-done.8 = bf16[4,32,2048]{2,1,0:T(8,128)(2,1)S(1)} collective-permute-done((bf16[4,32,2048]{2,1,0:T(8,128)(2,1)}, bf16[4,32,2048]{2,1,0:T(8,128)(2,1)S(1)}, u32[]{:S(2)}, u32[]{:S(2)}) %collective-permute-start.8) | collective-permute-done | bytes 524320 | tf_op jit(solution)/shard_map/ppermute | solution.py:383
  142.4 1.2 add_convert_fusion
  143.6 12.4 %all_to_all.20 = bf16[4,32,2048]{2,1,0:T(8,128)(2,1)S(1)} all-to-all(bf16[4,32,2048]{2,1,0:T(8,128)(2,1)S(1)} %add_convert_fusion), channel_id=1, replica_groups={{0,2,4,6},{1,3,5,7},{8,10,12,14},{9,11,13,15},{16,18,20,22},{17,19,21,2..., dimensions={0} | all-to-all | bytes 1048576 | tf_op jit(solution)/shard_map/all_to_all | solution.py:386
  156.0 0.7 reduce_sum.12
  (15 shorter events, 0.1 us)
Async XLA Ops:
  1.5 15.9 %copy-start.5 = (bf16[32,896]{1,0:T(8,128)(2,1)S(1)}, bf16[32,896]{1,0:T(8,128)(2,1)}, u32[]{:S(2)}) copy-start(bf16[32,896]{1,0:T(8,128)(2,1)} %get-tuple-element.29) | copy-start | bytes 172036
  1.6 53.8 %all-to-all-start = ((bf16[16,32,256]{2,1,0:T(8,128)(2,1)}), bf16[16,32,256]{2,1,0:T(8,128)(2,1)S(1)}, u32[]{:S(2)}, u32[]{:S(2)}) async-start(bf16[16,32,256]{2,1,0:T(8,128)(2,1)} %get-tuple-element.30), calls=%async_computation | async-start | bytes 524288 | tf_op jit(solution)/shard_map/all_to_all | solution.py:317
  56.4 13.9 %all-to-all-start.1 = ((bf16[4,512,256]{2,1,0:T(8,128)(2,1)}), bf16[4,512,256]{2,1,0:T(8,128)(2,1)S(1)}, u32[]{:S(2)}, u32[]{:S(2)}) async-start(bf16[4,512,256]{2,1,0:T(8,128)(2,1)} %broadcast_in_dim.7), calls=%async_computation.1 | async-start | bytes 2097152 | tf_op jit(solution)/shard_map/all_to_all | solution.py:25
  60.6 29.7 %copy-start.2 = (bf16[512,512]{1,0:T(8,128)(2,1)}, bf16[512,512]{1,0:T(8,128)(2,1)S(1)}, u32[]{:S(2)}) copy-start(bf16[512,512]{1,0:T(8,128)(2,1)S(1)} %slice.16.w0_ref) | copy-start | bytes 1572868
  70.3 1.0 copy-start
  74.7 18.2 %copy-start.4 = (bf16[16,2048]{1,0:T(8,128)(2,1)S(1)}, bf16[16,2048]{1,0:T(8,128)(2,1)}, u32[]{:S(2)}) copy-start(bf16[16,2048]{1,0:T(8,128)(2,1)} %get-tuple-element.40) | copy-start | bytes 196612
  74.7 54.4 %all-to-all-start.2 = ((bf16[16,144,128]{2,1,0:T(8,128)(2,1)}), bf16[16,144,128]{2,1,0:T(8,128)(2,1)S(1)}, u32[]{:S(2)}, u32[]{:S(2)}) async-start(bf16[16,144,128]{2,1,0:T(8,128)(2,1)} %get-tuple-element.38), calls=%async_computation.2 | async-start | bytes 1179648 | tf_op jit(solution)/shard_map/all_to_all | solution.py:347
  84.4 24.4 %collective-permute-start = (bf16[512,512]{1,0:T(8,128)(2,1)S(1)}, bf16[512,512]{1,0:T(8,128)(2,1)S(1)}, u32[]{:S(2)}, u32[]{:S(2)}) collective-permute-start(bf16[512,512]{1,0:T(8,128)(2,1)S(1)} %slice.16.w0_ref), channel_id=1, source_target_pairs={{0,8},{8,16},{16,24},{24,0},{1,9},{9,17},{17,25},{25,1},{2,10},{10... | collective-permute-start | bytes 1572872 | tf_op jit(solution)/shard_map/ppermute | solution.py:46
  86.6 26.9 %collective-permute-start.1 = (bf16[512,512]{1,0:T(8,128)(2,1)S(1)}, bf16[512,512]{1,0:T(8,128)(2,1)S(1)}, u32[]{:S(2)}, u32[]{:S(2)}) collective-permute-start(bf16[512,512]{1,0:T(8,128)(2,1)S(1)} %slice.16.w0_ref), channel_id=1, source_target_pairs={{0,16},{8,24},{16,0},{24,8},{1,17},{9,25},{17,1},{25,9},{2,18},{10... | collective-permute-start | bytes 1572872 | tf_op jit(solution)/shard_map/ppermute | solution.py:46
  90.3 23.2 %collective-permute-start.2 = (bf16[512,512]{1,0:T(8,128)(2,1)S(1)}, bf16[512,512]{1,0:T(8,128)(2,1)S(1)}, u32[]{:S(2)}, u32[]{:S(2)}) collective-permute-start(bf16[512,512]{1,0:T(8,128)(2,1)S(1)} %slice.16.w0_ref), channel_id=1, source_target_pairs={{0,24},{8,0},{16,8},{24,16},{1,25},{9,1},{17,9},{25,17},{2,26},{10... | collective-permute-start | bytes 1572872 | tf_op jit(solution)/shard_map/ppermute | solution.py:46
  92.9 4.7 %collective-permute-start.3 = (bf16[8,2048]{1,0:T(8,128)(2,1)S(1)}, bf16[8,2048]{1,0:T(8,128)(2,1)S(1)}, u32[]{:S(2)}, u32[]{:S(2)}) collective-permute-start(bf16[8,2048]{1,0:T(8,128)(2,1)S(1)} %get-tuple-element.54), channel_id=1, source_target_pairs={{0,32},{32,64},{64,96},{96,128},{128,160},{160,192},{192,224},{224... | collective-permute-start | bytes 98312 | tf_op jit(solution)/shard_map/ppermute | solution.py:355
  96.2 10.7 %collective-permute-start.4 = (bf16[8,2048]{1,0:T(8,128)(2,1)S(1)}, bf16[8,2048]{1,0:T(8,128)(2,1)S(1)}, u32[]{:S(2)}, u32[]{:S(2)}) collective-permute-start(bf16[8,2048]{1,0:T(8,128)(2,1)S(1)} %get-tuple-element.53), channel_id=1, source_target_pairs={{32,0},{64,32},{96,64},{128,96},{160,128},{192,160},{224,192},{256... | collective-permute-start | bytes 98312 | tf_op jit(solution)/shard_map/ppermute | solution.py:356
  97.5 21.0 %copy-start.3 = (bf16[512,384]{1,0:T(8,128)(2,1)}, bf16[512,384]{1,0:T(8,128)(2,1)S(1)}, u32[]{:S(2)}) copy-start(bf16[512,384]{1,0:T(8,128)(2,1)S(1)} %pad_maximum_fusion.w0_ref) | copy-start | bytes 1179652
  97.6 16.8 %copy-start.10 = (bf16[8,2048]{1,0:T(8,128)(2,1)}, bf16[8,2048]{1,0:T(8,128)(2,1)S(1)}, u32[]{:S(2)}) copy-start(bf16[8,2048]{1,0:T(8,128)(2,1)S(1)} %collective-permute-done.3.lo_ref) | copy-start | bytes 98308
  97.6 24.0 %collective-permute-start.5 = (bf16[512,384]{1,0:T(8,128)(2,1)S(1)}, bf16[512,384]{1,0:T(8,128)(2,1)S(1)}, u32[]{:S(2)}, u32[]{:S(2)}) collective-permute-start(bf16[512,384]{1,0:T(8,128)(2,1)S(1)} %pad_maximum_fusion.w0_ref), channel_id=1, source_target_pairs={{0,8},{8,16},{16,24},{24,0},{1,9},{9,17},{17,25},{25,1},{2,10},{10... | collective-permute-start | bytes 1179656 | tf_op jit(solution)/shard_map/ppermute | solution.py:46
  106.9 7.4 %copy-start.11 = (bf16[8,2048]{1,0:T(8,128)(2,1)}, bf16[8,2048]{1,0:T(8,128)(2,1)S(1)}, u32[]{:S(2)}) copy-start(bf16[8,2048]{1,0:T(8,128)(2,1)S(1)} %collective-permute-done.4.hi_ref) | copy-start | bytes 98308
  106.9 14.7 %collective-permute-start.6 = (bf16[512,384]{1,0:T(8,128)(2,1)S(1)}, bf16[512,384]{1,0:T(8,128)(2,1)}, u32[]{:S(2)}, u32[]{:S(2)}) collective-permute-start(bf16[512,384]{1,0:T(8,128)(2,1)S(1)} %pad_maximum_fusion.w0_ref), channel_id=1, source_target_pairs={{0,16},{8,24},{16,0},{24,8},{1,17},{9,25},{17,1},{25,9},{2,18},{10... | collective-permute-start | bytes 1179656 | tf_op jit(solution)/shard_map/ppermute | solution.py:46
  108.8 5.5 %copy-start.6 = (bf16[512,512]{1,0:T(8,128)(2,1)}, bf16[512,512]{1,0:T(8,128)(2,1)S(1)}, u32[]{:S(2)}) copy-start(bf16[512,512]{1,0:T(8,128)(2,1)S(1)} %collective-permute-done.w1_ref) | copy-start | bytes 1572868
  108.8 20.2 %collective-permute-start.7 = (bf16[512,384]{1,0:T(8,128)(2,1)S(1)}, bf16[512,384]{1,0:T(8,128)(2,1)}, u32[]{:S(2)}, u32[]{:S(2)}) collective-permute-start(bf16[512,384]{1,0:T(8,128)(2,1)S(1)} %pad_maximum_fusion.w0_ref), channel_id=1, source_target_pairs={{0,24},{8,0},{16,8},{24,16},{1,25},{9,1},{17,9},{25,17},{2,26},{10... | collective-permute-start | bytes 1179656 | tf_op jit(solution)/shard_map/ppermute | solution.py:46
  113.5 1.0 copy-start.7
  113.5 0.8 copy-start.8
  121.6 7.5 %copy-start.9 = (bf16[512,384]{1,0:T(8,128)(2,1)}, bf16[512,384]{1,0:T(8,128)(2,1)S(1)}, u32[]{:S(2)}) copy-start(bf16[512,384]{1,0:T(8,128)(2,1)S(1)} %collective-permute-done.5.w1_ref) | copy-start | bytes 1179652
  129.1 0.8 copy-start.1
  135.2 7.2 %collective-permute-start.8 = (bf16[4,32,2048]{2,1,0:T(8,128)(2,1)}, bf16[4,32,2048]{2,1,0:T(8,128)(2,1)S(1)}, u32[]{:S(2)}, u32[]{:S(2)}) collective-permute-start(bf16[4,32,2048]{2,1,0:T(8,128)(2,1)} %get-tuple-element.52), channel_id=1, source_target_pairs={{0,1},{1,0},{2,3},{3,2},{4,5},{5,4},{6,7},{7,6},{8,9},{9,8},{10,11... | collective-permute-start | bytes 1572872 | tf_op jit(solution)/shard_map/ppermute | solution.py:383

commit v5 on v4

--- a/solution.py
+++ b/solution.py
@@ -177,10 +177,12 @@
 def local_kernel(
     w0_ref, w1_ref, w2_ref, w3_ref, normed_ref, lo_ref, hi_ref, gain_ref,
     k_ref, v_ref, cols_ref, rows_ref,
-    q_ref, o_ref, pool_ref, num_ref, den_ref, w_ref, a_ref, b_ref,
+    q_ref, o_ref, pool_ref, num_ref, den_ref, wo_ref, w_ref, a_ref, b_ref,
 ):
     placed_by_source(lax.axis_index("fs"), (w0_ref, w1_ref, w2_ref, w3_ref), w_ref)
     weight = in_order(w_ref)
+    wo_ref[...] = weight[:, 512:]
+    weight = weight[:, :512]
     halo = jnp.concatenate([lo_ref[...], hi_ref[...]], axis=0).astype(f32)
     halo = rms_normed(halo, gain_ref[...]).astype(bf16)
     left = jnp.concatenate([normed_ref[...], halo], axis=0)
@@ -212,9 +214,8 @@
 
 def final_kernel(
     got_ref, mem_ref, nrm_ref, cols_ref, q_ref, o_ref, num_ref, den_ref,
-    gain_ref, pool_ref, w0_ref, w1_ref, w2_ref, w3_ref, keep_ref, give_ref, w_ref,
+    gain_ref, pool_ref, wo_ref, keep_ref, give_ref,
 ):
-    placed_by_source(lax.axis_index("fs"), (w0_ref, w1_ref, w2_ref, w3_ref), w_ref)
     position = lax.axis_index("sp")
     got_n, got_m, got_f = [], [], []
     for j in range(NZ):
@@ -264,7 +265,7 @@
     gate = 1.0 / (1.0 + jnp.exp(-o_ref[...].astype(f32)))
     memory_out = (scaled * gain_ref[...] * gate).astype(bf16)
     features = jnp.concatenate([memory_out, pool_ref[...]], axis=1)
-    result = lax.dot_general(features, in_order(w_ref), last, preferred_element_type=f32)
+    result = lax.dot_general(features, wo_ref[...], last, preferred_element_type=f32)
     core = lax.rem(lax.axis_index("tp"), 2)
     own = keep_ref.shape[1]
     for x in range(keep_ref.shape[0]):
@@ -334,9 +335,11 @@
         decay_extra[0, :, 0][:, None],
         flops=4 * 10**9,
     )
-    first_rest, rows = lax.optimization_barrier((along_z[:, 256:768], rows))
+    first_rest, rows = lax.optimization_barrier(
+        (jnp.concatenate([along_z[:, 256:], pool_z], axis=1), rows)
+    )
     first_from = {}
-    for shift in (1, 2, 3):
+    for shift in (1, 3):
         first_from[shift] = from_shift(first_rest, "fs", shift)
     k, v, packets = call(
         state_kernel,
@@ -345,16 +348,12 @@
         flops=2 * 10**9,
     )
     got = lax.all_to_all(packets, "sp", 0, 0, tiled=True)
-    last_rest, k = lax.optimization_barrier(
-        (jnp.concatenate([along_z[:, 768:], pool_z], axis=1), k)
-    )
+    later_rest, k = lax.optimization_barrier((first_rest, k))
     length = lax.axis_size("sp")
-    last_from = [last_rest]
-    for shift in (1, 2, 3):
-        last_from.append(from_shift(last_rest, "fs", shift))
+    first_from[2] = from_shift(later_rest, "fs", 2)
     low = lax.ppermute(ends[HALO:], "sp", [(i, i + 1) for i in range(length - 1)])
     high = lax.ppermute(ends[:HALO], "sp", [(i + 1, i) for i in range(length - 1)])
-    q, outgate, pool_out, nums, dens = call(
+    q, outgate, pool_out, nums, dens, wo = call(
         local_kernel,
         (
             sds((count, 128), bf16),
@@ -362,11 +361,12 @@
             sds((count, 256), bf16),
             sds((2, count, 128), f32),
             sds((count, 128), f32),
+            sds((width, 384), bf16),
         ),
         (), first_rest, *(first_from[s] for s in (1, 2, 3)), normed, low, high,
         norm_gain[None], k, v, cols, rows,
         flops=5 * 10**9,
-        scratch=[pltpu.VMEM((NY, NZ * ROWS, 512), bf16)]
+        scratch=[pltpu.VMEM((NY, NZ * ROWS, 896), bf16)]
         + [pltpu.VMEM((count + 32, 256), f32)] * 2,
     )
     cores = 2
@@ -375,9 +375,8 @@
     keep, give = call(
         final_kernel, (sds((chips, own, width), bf16),) * 2, (),
         got, init_memory[0, :, 0], init_normalizer[0, :, 0][:, None], cols, q, outgate,
-        nums, dens, head_gain, pool_out, *last_from,
+        nums, dens, head_gain, pool_out, wo,
         flops=2 * 10**9,
-        scratch=[pltpu.VMEM((NY, NZ * ROWS, 384), bf16)],
     )
     swap = [(i, i ^ 1) for i in range(chips * cores)]
     taken = lax.ppermute(give, "tp", swap)

time: 158 us -> 165 us (1.044)
  waiting for transfers between devices: 23.7 us -> 32.6 us
  starting transfers between devices: 58.8 us -> 56 us
    ppermute x6 -> x3, starting transfers between devices: 19 us -> 7.81 us  [from_shift(): lax.ppermute(x, axis, [(i, (i + shift) % count) for i in range(count)])]
    ppermute x1, starting transfers between devices: 5.46 us -> 13.4 us  [per_device(): taken = lax.ppermute(give, 'tp', swap)]
    ppermute x6 -> x3, waiting for transfers between devices: 10.5 us -> 15 us  [from_shift(): lax.ppermute(x, axis, [(i, (i + shift) % count) for i in range(count)])]
    ppermute x1, waiting for transfers between devices: 5.25 us -> 9.51 us  [per_device(): lax.ppermute(ends[:HALO], 'sp', [(i + 1, i) for i in range(length - 1)])]
  transfers between devices with their start and end apart: 12 -> 9, of which waited for: 5 -> 4; matrix products, arithmetic and copies ran while one was open for 0% -> 0% of each run, Pallas kernels for 5% -> 5%
where the time goes in v5:
time: 165 us; the launch traced here: 164 us
  starting transfers between devices  56 us (34%)
  blocking collectives  50.4 us (31%)
  waiting for transfers between devices  32.6 us (20%)
  Pallas kernels  18.7 us (11%)
  local copies, waits for them, and re-layouts  4.02 us (2%)
  other arithmetic  1.99 us (1%)
    all_gather x1, blocking collectives, per_device(): along_z = lax.all_gather(packed, 'sp', axis=0, tiled=True)  37.9 us
    pallas_call x5, Pallas kernels, call(): pl.pallas_call(kernel, in_specs=[smem] * len(scalars) + [vmem] * len(args...  18.7 us
    all_to_all x1, starting transfers between devices, per_device(): lax.all_to_all(pool_copies, 'sp', 0, 0, tiled=True).reshape(NZ * ROWS, 256)  15.7 us
    ppermute x3, waiting for transfers between devices, from_shift(): lax.ppermute(x, axis, [(i, (i + shift) % count) for i in range(count)])  15 us
    ppermute x1, starting transfers between devices, per_device(): taken = lax.ppermute(give, 'tp', swap)  13.4 us
    all_to_all x1, blocking collectives, per_device(): lax.all_to_all(pairs, 'tp', 0, 0, axis_index_groups=groups, tiled=True)  12.4 us
    all_to_all x1, starting transfers between devices, per_device(): got = lax.all_to_all(packets, 'sp', 0, 0, tiled=True)  9.59 us
    ppermute x1, waiting for transfers between devices, per_device(): lax.ppermute(ends[:HALO], 'sp', [(i + 1, i) for i in range(length - 1)])  9.51 us
  transfers between devices with their start and end apart: 9, of which 4 were waited for; matrix products, arithmetic and copies ran while one was open for 0% of the time, Pallas kernels for 5%

profile of v5, /device:TPU:1, one launch (start us, length us, event | category | flops | bytes accessed | tf_op | source)
XLA Modules:
  0.0 163.8 jit_solution(11079804822395756164)
XLA Ops:
  0.0 1.5 shard_map.145
  1.5 15.7 %all-to-all-start = ((bf16[16,32,256]{2,1,0:T(8,128)(2,1)}), bf16[16,32,256]{2,1,0:T(8,128)(2,1)S(1)}, u32[]{:S(2)}, u32[]{:S(2)}) async-start(bf16[16,32,256]{2,1,0:T(8,128)(2,1)} %get-tuple-element.31), calls=%async_computation | async-start | bytes 524288 | tf_op jit(solution)/shard_map/all_to_all | solution.py:318
  17.3 37.9 %all_gather.3 = bf16[512,896]{1,0:T(8,128)(2,1)S(1)} all-gather(bf16[32,896]{1,0:T(8,128)(2,1)} %get-tuple-element.30), channel_id=1, replica_groups=mesh['sp'=16,'fs'=4,'tp'=8] {'sp'}, dimensions={0}, use_global_device_ids=true | all-gather | bytes 974848 | tf_op jit(solution)/shard_map/all_gather | solution.py:319
  55.2 0.0 copy-start
  55.2 0.0 all-to-all-done
  55.2 1.2 broadcast_in_dim.7
  56.4 4.2 %all-to-all-start.1 = ((bf16[4,512,256]{2,1,0:T(8,128)(2,1)}), bf16[4,512,256]{2,1,0:T(8,128)(2,1)S(1)}, u32[]{:S(2)}, u32[]{:S(2)}) async-start(bf16[4,512,256]{2,1,0:T(8,128)(2,1)} %broadcast_in_dim.7), calls=%async_computation.1 | async-start | bytes 2097152 | tf_op jit(solution)/shard_map/all_to_all | solution.py:25
  60.6 0.0 copy-done
  60.6 0.0 slice-start
  60.6 3.3 %shard_map.146 = (bf16[256,2048]{1,0:T(8,128)(2,1)}, f32[256,128]{1,0:T(8,128)}, f32[8,256]{1,0:T(8,128)}, bf16[16,2048]{1,0:T(8,128)(2,1)}) custom-call(f32[4]{0:T(128)} %bitcast.17, bf16[256,2048]{1,0:T(8,128)(2,1)} %bitcast.10, f32[1,2048]{1,0:T(1,128)} %bitcast.13, bf16[4,2048]{1,0:T(4,128)(2,1)} %bitcast.12, f32[2,1,256]{2,1,0:T(1,128)} %bitcast.15), custom_call_target="tpu_custom_call" | custom-call | flops 4000000000 | tf_op jit(solution)/shard_map/pallas_call | solution.py:284
  63.9 0.0 slice-done
  63.9 0.1 pad_maximum_fusion.w0_ref
  64.0 0.0 copy-start.2
  64.0 6.3 %all-to-all-done.1.w_ref = bf16[4,512,256]{2,1,0:T(8,128)(2,1)S(1)} async-done(((bf16[4,512,256]{2,1,0:T(8,128)(2,1)}), bf16[4,512,256]{2,1,0:T(8,128)(2,1)S(1)}, u32[]{:S(2)}, u32[]{:S(2)}) %all-to-all-start.1) | async-done | bytes 1048608 | tf_op jit(solution)/shard_map/all_to_all | solution.py:25
  70.3 0.0 copy-start.1
  70.3 1.0 copy-done.1
  71.3 0.0 copy-start.4
  71.3 3.4 %shard_map.147 = (bf16[256,128]{1,0:T(8,128)(2,1)}, bf16[256,128]{1,0:T(8,128)(2,1)}, bf16[16,144,128]{2,1,0:T(8,128)(2,1)}) custom-call(bf16[4,512,256]{2,1,0:T(8,128)(2,1)} %copy-done.1, bf16[256,2048]{1,0:T(8,128)(2,1)} %get-tuple-element.34.normed_ref, f32[256,128]{1,0:T(8,128)} %get-tuple-element.35.cols_ref, f32[8,256]{1,0:T(8,128)} %get-tuple-element.39.rows_ref), custom_call_target="tpu_custom_call" | custom-call | flops 2000000000 | tf_op jit(solution)/shard_map/pallas_call | solution.py:284
  74.8 9.6 %all-to-all-start.2 = ((bf16[16,144,128]{2,1,0:T(8,128)(2,1)}), bf16[16,144,128]{2,1,0:T(8,128)(2,1)S(1)}, u32[]{:S(2)}, u32[]{:S(2)}) async-start(bf16[16,144,128]{2,1,0:T(8,128)(2,1)} %get-tuple-element.40), calls=%async_computation.2 | async-start | bytes 1179648 | tf_op jit(solution)/shard_map/all_to_all | solution.py:350
  84.3 2.8 %collective-permute-start.2 = (bf16[512,896]{1,0:T(8,128)(2,1)S(1)}, bf16[512,896]{1,0:T(8,128)(2,1)S(1)}, u32[]{:S(2)}, u32[]{:S(2)}) collective-permute-start(bf16[512,896]{1,0:T(8,128)(2,1)S(1)} %pad_maximum_fusion.w0_ref), channel_id=1, source_target_pairs={{0,24},{8,0},{16,8},{24,16},{1,25},{9,1},{17,9},{25,17},{2,26},{10... | collective-permute-start | bytes 2752520 | tf_op jit(solution)/shard_map/ppermute | solution.py:46
  87.2 2.5 %collective-permute-start = (bf16[512,896]{1,0:T(8,128)(2,1)S(1)}, bf16[512,896]{1,0:T(8,128)(2,1)S(1)}, u32[]{:S(2)}, u32[]{:S(2)}) collective-permute-start(bf16[512,896]{1,0:T(8,128)(2,1)S(1)} %pad_maximum_fusion.w0_ref), channel_id=1, source_target_pairs={{0,8},{8,16},{16,24},{24,0},{1,9},{9,17},{17,25},{25,1},{2,10},{10... | collective-permute-start | bytes 2752520 | tf_op jit(solution)/shard_map/ppermute | solution.py:46
  89.6 2.5 %collective-permute-start.1 = (bf16[512,896]{1,0:T(8,128)(2,1)S(1)}, bf16[512,896]{1,0:T(8,128)(2,1)S(1)}, u32[]{:S(2)}, u32[]{:S(2)}) collective-permute-start(bf16[512,896]{1,0:T(8,128)(2,1)S(1)} %pad_maximum_fusion.w0_ref), channel_id=1, source_target_pairs={{0,16},{8,24},{16,0},{24,8},{1,17},{9,25},{17,1},{25,9},{2,18},{10... | collective-permute-start | bytes 2752520 | tf_op jit(solution)/shard_map/ppermute | solution.py:46
  92.2 0.0 copy-done.4
  92.2 1.3 collective-permute-start.4
  93.5 4.0 %collective-permute-start.3 = (bf16[8,2048]{1,0:T(8,128)(2,1)S(1)}, bf16[8,2048]{1,0:T(8,128)(2,1)S(1)}, u32[]{:S(2)}, u32[]{:S(2)}) collective-permute-start(bf16[8,2048]{1,0:T(8,128)(2,1)S(1)} %get-tuple-element.56), channel_id=1, source_target_pairs={{0,32},{32,64},{64,96},{96,128},{128,160},{160,192},{192,224},{224... | collective-permute-start | bytes 98312 | tf_op jit(solution)/shard_map/ppermute | solution.py:354
  97.5 9.5 %collective-permute-done.4.hi_ref = bf16[8,2048]{1,0:T(8,128)(2,1)S(1)} collective-permute-done((bf16[8,2048]{1,0:T(8,128)(2,1)S(1)}, bf16[8,2048]{1,0:T(8,128)(2,1)S(1)}, u32[]{:S(2)}, u32[]{:S(2)}) %collective-permute-start.4) | collective-permute-done | bytes 32800 | tf_op jit(solution)/shard_map/ppermute | solution.py:355
  107.0 0.0 collective-permute-done.3.lo_ref
  107.0 0.0 collective-permute-done.2.w3_ref
  107.0 0.0 copy-start.5
  107.0 0.0 collective-permute-done.w1_ref
  107.0 0.0 copy-start.6
  107.1 15.0 %collective-permute-done.1.w2_ref = bf16[512,896]{1,0:T(8,128)(2,1)S(1)} collective-permute-done((bf16[512,896]{1,0:T(8,128)(2,1)S(1)}, bf16[512,896]{1,0:T(8,128)(2,1)S(1)}, u32[]{:S(2)}, u32[]{:S(2)}) %collective-permute-start.1) | collective-permute-done | bytes 917536 | tf_op jit(solution)/shard_map/ppermute | solution.py:46
  122.1 0.0 copy-done.6
  122.1 1.0 copy-done.7
  123.1 0.0 copy-done.2
  123.1 0.0 copy-done.8
  123.1 0.0 copy-done.9
  123.1 0.0 copy-done.5
  123.1 5.2 %shard_map.148 = (bf16[256,128]{1,0:T(8,128)(2,1)}, bf16[256,128]{1,0:T(8,128)(2,1)}, bf16[256,256]{1,0:T(8,128)(2,1)}, f32[2,256,128]{2,1,0:T(8,128)}, f32[256,128]{1,0:T(8,128)}, /*index=5*/bf16[2048,384]{1,0:T(8,128)(2,1)}) custom-call(bf16[512,896]{1,0:T(8,128)(2,1)} %copy-done.2, bf16[512,896]{1,0:T(8,128)(2,1)} %copy-done.6, ...), custom_call_target="tpu_custom_call" | custom-call | flops 5000000000 | tf_op jit(solution)/shard_map/pallas_call | solution.py:284
  128.2 0.0 all-to-all-done.2.got_ref
  128.3 0.0 copy-start.3
  128.3 0.8 copy-done.3
  129.1 5.2 %shard_map.149 = (bf16[4,32,2048]{2,1,0:T(8,128)(2,1)}, bf16[4,32,2048]{2,1,0:T(8,128)(2,1)}) custom-call(bf16[16,144,128]{2,1,0:T(8,128)(2,1)} %copy-done.3, f32[2,128,128]{2,1,0:T(8,128)} %bitcast.11, f32[2,1,128]{2,1,0:T(1,128)} %bitcast.16, f32[256,128]{1,0:T(8,128)} %get-tuple-element.35.cols_ref, bf16[256,128]{1,0:T(8,128)(2,1)} %get-tuple-element.47.q_ref, ...), custom_call_target="tpu_custom_call" | custom-call | flops 2000000000 | tf_op jit(solution)/shard_map/pallas_call | solution.py:284
  134.3 13.4 %collective-permute-start.5 = (bf16[4,32,2048]{2,1,0:T(8,128)(2,1)}, bf16[4,32,2048]{2,1,0:T(8,128)(2,1)S(1)}, u32[]{:S(2)}, u32[]{:S(2)}) collective-permute-start(bf16[4,32,2048]{2,1,0:T(8,128)(2,1)} %get-tuple-element.54), channel_id=1, source_target_pairs={{0,1},{1,0},{2,3},{3,2},{4,5},{5,4},{6,7},{7,6},{8,9},{9,8},{10,11... | collective-permute-start | bytes 1572872 | tf_op jit(solution)/shard_map/ppermute | solution.py:382
  147.7 1.7 %collective-permute-done.5 = bf16[4,32,2048]{2,1,0:T(8,128)(2,1)S(1)} collective-permute-done((bf16[4,32,2048]{2,1,0:T(8,128)(2,1)}, bf16[4,32,2048]{2,1,0:T(8,128)(2,1)S(1)}, u32[]{:S(2)}, u32[]{:S(2)}) %collective-permute-start.5) | collective-permute-done | bytes 524320 | tf_op jit(solution)/shard_map/ppermute | solution.py:382
  149.4 1.2 add_convert_fusion
  150.6 12.4 %all_to_all.20 = bf16[4,32,2048]{2,1,0:T(8,128)(2,1)S(1)} all-to-all(bf16[4,32,2048]{2,1,0:T(8,128)(2,1)S(1)} %add_convert_fusion), channel_id=1, replica_groups={{0,2,4,6},{1,3,5,7},{8,10,12,14},{9,11,13,15},{16,18,20,22},{17,19,21,2..., dimensions={0} | all-to-all | bytes 1048576 | tf_op jit(solution)/shard_map/all_to_all | solution.py:385
  163.1 0.7 reduce_sum.12
  (5 shorter events, 0.0 us)
Async XLA Ops:
  1.5 53.7 %all-to-all-start = ((bf16[16,32,256]{2,1,0:T(8,128)(2,1)}), bf16[16,32,256]{2,1,0:T(8,128)(2,1)S(1)}, u32[]{:S(2)}, u32[]{:S(2)}) async-start(bf16[16,32,256]{2,1,0:T(8,128)(2,1)} %get-tuple-element.31), calls=%async_computation | async-start | bytes 524288 | tf_op jit(solution)/shard_map/all_to_all | solution.py:318
  55.2 5.4 %copy-start = (bf16[512,896]{1,0:T(8,128)(2,1)}, bf16[512,896]{1,0:T(8,128)(2,1)S(1)}, u32[]{:S(2)}) copy-start(bf16[512,896]{1,0:T(8,128)(2,1)S(1)} %all_gather.3) | copy-start | bytes 2752516
  56.4 13.9 %all-to-all-start.1 = ((bf16[4,512,256]{2,1,0:T(8,128)(2,1)}), bf16[4,512,256]{2,1,0:T(8,128)(2,1)S(1)}, u32[]{:S(2)}, u32[]{:S(2)}) async-start(bf16[4,512,256]{2,1,0:T(8,128)(2,1)} %broadcast_in_dim.7), calls=%async_computation.1 | async-start | bytes 2097152 | tf_op jit(solution)/shard_map/all_to_all | solution.py:25
  60.6 3.3 %slice-start = ((bf16[512,896]{1,0:T(8,128)(2,1)}), bf16[512,640]{1,0:T(8,128)(2,1)S(1)}, s32[]{:S(2)}) async-start(bf16[512,896]{1,0:T(8,128)(2,1)} %copy-done), calls=%async_computation.4 | async-start | bytes 1310720 | tf_op jit(solution)/shard_map/slice | solution.py:339
  64.0 59.1 %copy-start.2 = (bf16[512,896]{1,0:T(8,128)(2,1)}, bf16[512,896]{1,0:T(8,128)(2,1)S(1)}, u32[]{:S(2)}) copy-start(bf16[512,896]{1,0:T(8,128)(2,1)S(1)} %pad_maximum_fusion.w0_ref) | copy-start | bytes 2752516
  70.3 1.0 copy-start.1
  71.3 20.9 %copy-start.4 = (bf16[16,2048]{1,0:T(8,128)(2,1)S(1)}, bf16[16,2048]{1,0:T(8,128)(2,1)}, u32[]{:S(2)}) copy-start(bf16[16,2048]{1,0:T(8,128)(2,1)} %get-tuple-element.44) | copy-start | bytes 196612
  74.8 53.5 %all-to-all-start.2 = ((bf16[16,144,128]{2,1,0:T(8,128)(2,1)}), bf16[16,144,128]{2,1,0:T(8,128)(2,1)S(1)}, u32[]{:S(2)}, u32[]{:S(2)}) async-start(bf16[16,144,128]{2,1,0:T(8,128)(2,1)} %get-tuple-element.40), calls=%async_computation.2 | async-start | bytes 1179648 | tf_op jit(solution)/shard_map/all_to_all | solution.py:350
  84.3 22.7 %collective-permute-start.2 = (bf16[512,896]{1,0:T(8,128)(2,1)S(1)}, bf16[512,896]{1,0:T(8,128)(2,1)S(1)}, u32[]{:S(2)}, u32[]{:S(2)}) collective-permute-start(bf16[512,896]{1,0:T(8,128)(2,1)S(1)} %pad_maximum_fusion.w0_ref), channel_id=1, source_target_pairs={{0,24},{8,0},{16,8},{24,16},{1,25},{9,1},{17,9},{25,17},{2,26},{10... | collective-permute-start | bytes 2752520 | tf_op jit(solution)/shard_map/ppermute | solution.py:46
  87.2 19.9 %collective-permute-start = (bf16[512,896]{1,0:T(8,128)(2,1)S(1)}, bf16[512,896]{1,0:T(8,128)(2,1)S(1)}, u32[]{:S(2)}, u32[]{:S(2)}) collective-permute-start(bf16[512,896]{1,0:T(8,128)(2,1)S(1)} %pad_maximum_fusion.w0_ref), channel_id=1, source_target_pairs={{0,8},{8,16},{16,24},{24,0},{1,9},{9,17},{17,25},{25,1},{2,10},{10... | collective-permute-start | bytes 2752520 | tf_op jit(solution)/shard_map/ppermute | solution.py:46
  89.6 32.4 %collective-permute-start.1 = (bf16[512,896]{1,0:T(8,128)(2,1)S(1)}, bf16[512,896]{1,0:T(8,128)(2,1)S(1)}, u32[]{:S(2)}, u32[]{:S(2)}) collective-permute-start(bf16[512,896]{1,0:T(8,128)(2,1)S(1)} %pad_maximum_fusion.w0_ref), channel_id=1, source_target_pairs={{0,16},{8,24},{16,0},{24,8},{1,17},{9,25},{17,1},{25,9},{2,18},{10... | collective-permute-start | bytes 2752520 | tf_op jit(solution)/shard_map/ppermute | solution.py:46
  92.2 14.8 %collective-permute-start.4 = (bf16[8,2048]{1,0:T(8,128)(2,1)S(1)}, bf16[8,2048]{1,0:T(8,128)(2,1)S(1)}, u32[]{:S(2)}, u32[]{:S(2)}) collective-permute-start(bf16[8,2048]{1,0:T(8,128)(2,1)S(1)} %get-tuple-element.55), channel_id=1, source_target_pairs={{32,0},{64,32},{96,64},{128,96},{160,128},{192,160},{224,192},{256... | collective-permute-start | bytes 98312 | tf_op jit(solution)/shard_map/ppermute | solution.py:355
  93.5 13.5 %collective-permute-start.3 = (bf16[8,2048]{1,0:T(8,128)(2,1)S(1)}, bf16[8,2048]{1,0:T(8,128)(2,1)S(1)}, u32[]{:S(2)}, u32[]{:S(2)}) collective-permute-start(bf16[8,2048]{1,0:T(8,128)(2,1)S(1)} %get-tuple-element.56), channel_id=1, source_target_pairs={{0,32},{32,64},{64,96},{96,128},{128,160},{160,192},{192,224},{224... | collective-permute-start | bytes 98312 | tf_op jit(solution)/shard_map/ppermute | solution.py:354
  107.0 16.0 %copy-start.8 = (bf16[8,2048]{1,0:T(8,128)(2,1)}, bf16[8,2048]{1,0:T(8,128)(2,1)S(1)}, u32[]{:S(2)}) copy-start(bf16[8,2048]{1,0:T(8,128)(2,1)S(1)} %collective-permute-done.4.hi_ref) | copy-start | bytes 98308
  107.0 16.0 %copy-start.9 = (bf16[8,2048]{1,0:T(8,128)(2,1)}, bf16[8,2048]{1,0:T(8,128)(2,1)S(1)}, u32[]{:S(2)}) copy-start(bf16[8,2048]{1,0:T(8,128)(2,1)S(1)} %collective-permute-done.3.lo_ref) | copy-start | bytes 98308
  107.0 16.0 %copy-start.5 = (bf16[512,896]{1,0:T(8,128)(2,1)}, bf16[512,896]{1,0:T(8,128)(2,1)S(1)}, u32[]{:S(2)}) copy-start(bf16[512,896]{1,0:T(8,128)(2,1)S(1)} %collective-permute-done.2.w3_ref) | copy-start | bytes 2752516
  107.0 15.0 %copy-start.6 = (bf16[512,896]{1,0:T(8,128)(2,1)}, bf16[512,896]{1,0:T(8,128)(2,1)S(1)}, u32[]{:S(2)}) copy-start(bf16[512,896]{1,0:T(8,128)(2,1)S(1)} %collective-permute-done.w1_ref) | copy-start | bytes 2752516
  122.1 1.0 copy-start.7
  128.3 0.8 copy-start.3
  134.3 15.2 %collective-permute-start.5 = (bf16[4,32,2048]{2,1,0:T(8,128)(2,1)}, bf16[4,32,2048]{2,1,0:T(8,128)(2,1)S(1)}, u32[]{:S(2)}, u32[]{:S(2)}) collective-permute-start(bf16[4,32,2048]{2,1,0:T(8,128)(2,1)} %get-tuple-element.54), channel_id=1, source_target_pairs={{0,1},{1,0},{2,3},{3,2},{4,5},{5,4},{6,7},{7,6},{8,9},{9,8},{10,11... | collective-permute-start | bytes 1572872 | tf_op jit(solution)/shard_map/ppermute | solution.py:382

commit v6 on v5

--- a/solution.py
+++ b/solution.py
@@ -46,9 +46,10 @@
     return lax.ppermute(x, axis, [(i, (i + shift) % count) for i in range(count)])
 
 
-def placed_by_source(y, refs, out_ref):
+def placed_by_source(y, refs, out_ref, lo, hi):
     for shift, ref in enumerate(refs):
-        out_ref[lax.rem(y + NY - shift, NY)] = ref[...]
+        piece = ref[...] if ref.shape[1] == hi - lo else ref[:, lo:hi]
+        out_ref[lax.rem(y + NY - shift, NY)] = piece
 
 
 def rms_normed(x, gain):
@@ -177,12 +178,10 @@
 def local_kernel(
     w0_ref, w1_ref, w2_ref, w3_ref, normed_ref, lo_ref, hi_ref, gain_ref,
     k_ref, v_ref, cols_ref, rows_ref,
-    q_ref, o_ref, pool_ref, num_ref, den_ref, wo_ref, w_ref, a_ref, b_ref,
+    q_ref, o_ref, pool_ref, num_ref, den_ref, w_ref, a_ref, b_ref,
 ):
-    placed_by_source(lax.axis_index("fs"), (w0_ref, w1_ref, w2_ref, w3_ref), w_ref)
+    placed_by_source(lax.axis_index("fs"), (w0_ref, w1_ref, w2_ref, w3_ref), w_ref, 0, 512)
     weight = in_order(w_ref)
-    wo_ref[...] = weight[:, 512:]
-    weight = weight[:, :512]
     halo = jnp.concatenate([lo_ref[...], hi_ref[...]], axis=0).astype(f32)
     halo = rms_normed(halo, gain_ref[...]).astype(bf16)
     left = jnp.concatenate([normed_ref[...], halo], axis=0)
@@ -210,6 +209,11 @@
         num_ref[r] = jnp.dot(weights.astype(bf16), v_ref[...], preferred_element_type=f32)
         dens = jnp.where(lane == r, jnp.sum(weights, axis=1, keepdims=True), dens)
     den_ref[...] = dens
+
+
+def outs_kernel(w0_ref, w1_ref, w2_ref, w3_ref, out_ref, w_ref):
+    placed_by_source(lax.axis_index("fs"), (w0_ref, w1_ref, w2_ref, w3_ref), w_ref, 512, 896)
+    out_ref[...] = in_order(w_ref)
 
 
 def final_kernel(
@@ -341,6 +345,9 @@
     first_from = {}
     for shift in (1, 3):
         first_from[shift] = from_shift(first_rest, "fs", shift)
+    length = lax.axis_size("sp")
+    low = lax.ppermute(ends[HALO:], "sp", [(i, i + 1) for i in range(length - 1)])
+    high = lax.ppermute(ends[:HALO], "sp", [(i + 1, i) for i in range(length - 1)])
     k, v, packets = call(
         state_kernel,
         (sds((count, 128), bf16), sds((count, 128), bf16), sds((NZ, PACKET, 128), bf16)),
@@ -349,11 +356,9 @@
     )
     got = lax.all_to_all(packets, "sp", 0, 0, tiled=True)
     later_rest, k = lax.optimization_barrier((first_rest, k))
-    length = lax.axis_size("sp")
-    first_from[2] = from_shift(later_rest, "fs", 2)
-    low = lax.ppermute(ends[HALO:], "sp", [(i, i + 1) for i in range(length - 1)])
-    high = lax.ppermute(ends[:HALO], "sp", [(i + 1, i) for i in range(length - 1)])
-    q, outgate, pool_out, nums, dens, wo = call(
+    first_from[2] = from_shift(later_rest[:, :512], "fs", 2)
+    last_two = from_shift(later_rest[:, 512:], "fs", 2)
+    q, outgate, pool_out, nums, dens = call(
         local_kernel,
         (
             sds((count, 128), bf16),
@@ -361,13 +366,17 @@
             sds((count, 256), bf16),
             sds((2, count, 128), f32),
             sds((count, 128), f32),
-            sds((width, 384), bf16),
         ),
         (), first_rest, *(first_from[s] for s in (1, 2, 3)), normed, low, high,
         norm_gain[None], k, v, cols, rows,
         flops=5 * 10**9,
-        scratch=[pltpu.VMEM((NY, NZ * ROWS, 896), bf16)]
+        scratch=[pltpu.VMEM((NY, NZ * ROWS, 512), bf16)]
         + [pltpu.VMEM((count + 32, 256), f32)] * 2,
+    )
+    wo = call(
+        outs_kernel, sds((width, 384), bf16), (),
+        first_rest, first_from[1], last_two, first_from[3],
+        flops=10**8, scratch=[pltpu.VMEM((NY, NZ * ROWS, 384), bf16)],
     )
     cores = 2
     chips = lax.axis_size("tp") // cores

time: 165 us -> 166 us (level)
  waiting for transfers between devices: 32.6 us -> 25.1 us
  starting transfers between devices: 56 us -> 61.4 us
  Pallas kernels: 18.7 us -> 21.2 us
    ppermute x1, waiting for transfers between devices: 9.51 us -> 0.01 us  [per_device(): lax.ppermute(ends[:HALO], 'sp', [(i + 1, i) for i in range(length - 1)])]
    ppermute x3 -> x4, starting transfers between devices: 7.81 us -> 13.3 us  [from_shift(): lax.ppermute(x, axis, [(i, (i + shift) % count) for i in range(count)])]
    pallas_call x5 -> x6, Pallas kernels: 18.7 us -> 21.2 us  [call(): pl.pallas_call(kernel, in_specs=[smem] * len(scalars) + [vmem] * len(args...]
    ppermute x3 -> x4, waiting for transfers between devices: 15 us -> 17.1 us  [from_shift(): lax.ppermute(x, axis, [(i, (i + shift) % count) for i in range(count)])]
  transfers between devices with their start and end apart: 9 -> 10, of which waited for: 4 -> 3; matrix products, arithmetic and copies ran while one was open for 0% -> 1% of each run, Pallas kernels for 5% -> 7%
where the time goes in v6:
time: 166 us; the launch traced here: 165 us
  starting transfers between devices  61.4 us (37%)
  blocking collectives  50.4 us (30%)
  waiting for transfers between devices  25.1 us (15%)
  Pallas kernels  21.2 us (13%)
  local copies, waits for them, and re-layouts  4.51 us (3%)
  other arithmetic  1.99 us (1%)
    all_gather x1, blocking collectives, per_device(): along_z = lax.all_gather(packed, 'sp', axis=0, tiled=True)  37.9 us
    pallas_call x6, Pallas kernels, call(): pl.pallas_call(kernel, in_specs=[smem] * len(scalars) + [vmem] * len(args...  21.2 us
    ppermute x4, waiting for transfers between devices, from_shift(): lax.ppermute(x, axis, [(i, (i + shift) % count) for i in range(count)])  17.1 us
    all_to_all x1, starting transfers between devices, per_device(): lax.all_to_all(pool_copies, 'sp', 0, 0, tiled=True).reshape(NZ * ROWS, 256)  15.7 us
    ppermute x1, starting transfers between devices, per_device(): taken = lax.ppermute(give, 'tp', swap)  14 us
    ppermute x4, starting transfers between devices, from_shift(): lax.ppermute(x, axis, [(i, (i + shift) % count) for i in range(count)])  13.3 us
    all_to_all x1, blocking collectives, per_device(): lax.all_to_all(pairs, 'tp', 0, 0, axis_index_groups=groups, tiled=True)  12.4 us
    all_to_all x1, starting transfers between devices, per_device(): got = lax.all_to_all(packets, 'sp', 0, 0, tiled=True)  9.72 us
  transfers between devices with their start and end apart: 10, of which 3 were waited for; matrix products, arithmetic and copies ran while one was open for 1% of the time, Pallas kernels for 7%

profile of v6, /device:TPU:1, one launch (start us, length us, event | category | flops | bytes accessed | tf_op | source)
XLA Modules:
  0.0 164.8 jit_solution(13066615586756617151)
XLA Ops:
  0.0 1.5 shard_map.145
  1.5 15.7 %all-to-all-start = ((bf16[16,32,256]{2,1,0:T(8,128)(2,1)}), bf16[16,32,256]{2,1,0:T(8,128)(2,1)S(1)}, u32[]{:S(2)}, u32[]{:S(2)}) async-start(bf16[16,32,256]{2,1,0:T(8,128)(2,1)} %get-tuple-element.30), calls=%async_computation | async-start | bytes 524288 | tf_op jit(solution)/shard_map/all_to_all | solution.py:322
  17.3 37.9 %all_gather.3 = bf16[512,896]{1,0:T(8,128)(2,1)S(1)} all-gather(bf16[32,896]{1,0:T(8,128)(2,1)} %get-tuple-element.29), channel_id=1, replica_groups=mesh['sp'=16,'fs'=4,'tp'=8] {'sp'}, dimensions={0}, use_global_device_ids=true | all-gather | bytes 974848 | tf_op jit(solution)/shard_map/all_gather | solution.py:323
  55.2 0.0 copy-start.1
  55.2 0.0 all-to-all-done
  55.2 1.2 broadcast_in_dim.7
  56.4 4.2 %all-to-all-start.1 = ((bf16[4,512,256]{2,1,0:T(8,128)(2,1)}), bf16[4,512,256]{2,1,0:T(8,128)(2,1)S(1)}, u32[]{:S(2)}, u32[]{:S(2)}) async-start(bf16[4,512,256]{2,1,0:T(8,128)(2,1)} %broadcast_in_dim.7), calls=%async_computation.1 | async-start | bytes 2097152 | tf_op jit(solution)/shard_map/all_to_all | solution.py:25
  60.6 0.0 copy-done.1
  60.6 3.3 %shard_map.146 = (bf16[256,2048]{1,0:T(8,128)(2,1)}, f32[256,128]{1,0:T(8,128)}, f32[8,256]{1,0:T(8,128)}, bf16[16,2048]{1,0:T(8,128)(2,1)}) custom-call(f32[4]{0:T(128)} %bitcast.17, bf16[256,2048]{1,0:T(8,128)(2,1)} %bitcast.10, f32[1,2048]{1,0:T(1,128)} %bitcast.13, bf16[4,2048]{1,0:T(4,128)(2,1)} %bitcast.12, f32[2,1,256]{2,1,0:T(1,128)} %bitcast.15), custom_call_target="tpu_custom_call" | custom-call | flops 4000000000 | tf_op jit(solution)/shard_map/pallas_call | solution.py:288
  63.9 0.0 slice-done
  63.9 0.1 pad_maximum_fusion.w0_ref
  64.0 0.0 copy-start
  64.0 6.3 %all-to-all-done.1.w_ref = bf16[4,512,256]{2,1,0:T(8,128)(2,1)S(1)} async-done(((bf16[4,512,256]{2,1,0:T(8,128)(2,1)}), bf16[4,512,256]{2,1,0:T(8,128)(2,1)S(1)}, u32[]{:S(2)}, u32[]{:S(2)}) %all-to-all-start.1) | async-done | bytes 1048608 | tf_op jit(solution)/shard_map/all_to_all | solution.py:25
  70.3 1.0 copy-done.2
  71.3 3.4 %shard_map.147 = (bf16[256,128]{1,0:T(8,128)(2,1)}, bf16[256,128]{1,0:T(8,128)(2,1)}, bf16[16,144,128]{2,1,0:T(8,128)(2,1)}) custom-call(bf16[4,512,256]{2,1,0:T(8,128)(2,1)} %copy-done.2, bf16[256,2048]{1,0:T(8,128)(2,1)} %get-tuple-element.33.normed_ref, f32[256,128]{1,0:T(8,128)} %get-tuple-element.34.cols_ref, f32[8,256]{1,0:T(8,128)} %get-tuple-element.38.rows_ref), custom_call_target="tpu_custom_call" | custom-call | flops 2000000000 | tf_op jit(solution)/shard_map/pallas_call | solution.py:288
  74.7 9.7 %all-to-all-start.2 = ((bf16[16,144,128]{2,1,0:T(8,128)(2,1)}), bf16[16,144,128]{2,1,0:T(8,128)(2,1)S(1)}, u32[]{:S(2)}, u32[]{:S(2)}) async-start(bf16[16,144,128]{2,1,0:T(8,128)(2,1)} %get-tuple-element.39), calls=%async_computation.2 | async-start | bytes 1179648 | tf_op jit(solution)/shard_map/all_to_all | solution.py:357
  84.4 2.2 %collective-permute-start = (bf16[512,896]{1,0:T(8,128)(2,1)S(1)}, bf16[512,896]{1,0:T(8,128)(2,1)S(1)}, u32[]{:S(2)}, u32[]{:S(2)}) collective-permute-start(bf16[512,896]{1,0:T(8,128)(2,1)S(1)} %pad_maximum_fusion.w0_ref), channel_id=1, source_target_pairs={{0,8},{8,16},{16,24},{24,0},{1,9},{9,17},{17,25},{25,1},{2,10},{10... | collective-permute-start | bytes 2752520 | tf_op jit(solution)/shard_map/ppermute | solution.py:46
  86.6 4.3 %collective-permute-start.2 = (bf16[512,896]{1,0:T(8,128)(2,1)S(1)}, bf16[512,896]{1,0:T(8,128)(2,1)S(1)}, u32[]{:S(2)}, u32[]{:S(2)}) collective-permute-start(bf16[512,896]{1,0:T(8,128)(2,1)S(1)} %pad_maximum_fusion.w0_ref), channel_id=1, source_target_pairs={{0,24},{8,0},{16,8},{24,16},{1,25},{9,1},{17,9},{25,17},{2,26},{10... | collective-permute-start | bytes 2752520 | tf_op jit(solution)/shard_map/ppermute | solution.py:46
  91.0 0.8 slice.20
  91.8 1.9 %collective-permute-start.1 = (bf16[512,512]{1,0:T(8,128)(2,1)}, bf16[512,512]{1,0:T(8,128)(2,1)}, u32[]{:S(2)}, u32[]{:S(2)}) collective-permute-start(bf16[512,512]{1,0:T(8,128)(2,1)} %slice.20), channel_id=1, source_target_pairs={{0,16},{8,24},{16,0},{24,8},{1,17},{9,25},{17,1},{25,9},{2,18},{10... | collective-permute-start | bytes 1572872 | tf_op jit(solution)/shard_map/ppermute | solution.py:46
  93.7 0.0 copy-done
  93.8 4.9 %collective-permute-start.5 = (bf16[512,384]{1,0:T(8,128)(2,1)S(1)}, bf16[512,384]{1,0:T(8,128)(2,1)}, u32[]{:S(2)}, u32[]{:S(2)}) collective-permute-start(bf16[512,384]{1,0:T(8,128)(2,1)S(1)} %slice.23), channel_id=1, source_target_pairs={{0,16},{8,24},{16,0},{24,8},{1,17},{9,25},{17,1},{25,9},{2,18},{10... | collective-permute-start | bytes 1179656 | tf_op jit(solution)/shard_map/ppermute | solution.py:46
  98.6 0.0 copy-done.6
  98.7 3.3 %collective-permute-start.3 = (bf16[8,2048]{1,0:T(8,128)(2,1)S(1)}, bf16[8,2048]{1,0:T(8,128)(2,1)S(1)}, u32[]{:S(2)}, u32[]{:S(2)}) collective-permute-start(bf16[8,2048]{1,0:T(8,128)(2,1)S(1)} %get-tuple-element.54), channel_id=1, source_target_pairs={{0,32},{32,64},{64,96},{96,128},{128,160},{160,192},{192,224},{224... | collective-permute-start | bytes 98312 | tf_op jit(solution)/shard_map/ppermute | solution.py:349
  101.9 0.0 collective-permute-done.w1_ref
  101.9 0.0 copy-start.3
  102.0 1.3 collective-permute-start.4
  103.3 0.0 collective-permute-done.2.w3_ref
  103.3 0.0 copy-start.4
  103.3 17.1 %collective-permute-done.5.w2_ref = bf16[512,384]{1,0:T(8,128)(2,1)} collective-permute-done((bf16[512,384]{1,0:T(8,128)(2,1)S(1)}, bf16[512,384]{1,0:T(8,128)(2,1)}, u32[]{:S(2)}, u32[]{:S(2)}) %collective-permute-start.5) | collective-permute-done | bytes 393248 | tf_op jit(solution)/shard_map/ppermute | solution.py:46
  120.3 0.0 copy-done.3
  120.3 0.0 copy-done.4
  120.4 3.3 %shard_map.149.wo_ref = bf16[2048,384]{1,0:T(8,128)(2,1)} custom-call(bf16[512,896]{1,0:T(8,128)(2,1)} %copy-done, bf16[512,896]{1,0:T(8,128)(2,1)} %copy-done.3, bf16[512,384]{1,0:T(8,128)(2,1)} %collective-permute-done.5.w2_ref, bf16[512,896]{1,0:T(8,128)(2,1)} %copy-done.4), custom_call_target="tpu_custom_call" | custom-call | flops 100000000 | tf_op jit(solution)/shard_map/pallas_call | solution.py:288
  123.7 0.0 collective-permute-done.3.lo_ref
  123.7 0.0 collective-permute-done.4.hi_ref
  123.7 0.0 copy-start.8
  123.7 0.0 collective-permute-done.1.w2_ref
  123.7 0.6 copy-done.7
  124.3 0.0 copy-done.8
  124.3 4.4 %shard_map.148 = (bf16[256,128]{1,0:T(8,128)(2,1)}, bf16[256,128]{1,0:T(8,128)(2,1)}, bf16[256,256]{1,0:T(8,128)(2,1)}, f32[2,256,128]{2,1,0:T(8,128)}, f32[256,128]{1,0:T(8,128)}) custom-call(bf16[512,896]{1,0:T(8,128)(2,1)} %copy-done, bf16[512,896]{1,0:T(8,128)(2,1)} %copy-done.3, bf16[512,512]{1,0:T(8,128)(2,1)} %collective-permute-done.1.w2_ref, ...), custom_call_target="tpu_custom_call" | custom-call | flops 5000000000 | tf_op jit(solution)/shard_map/pallas_call | solution.py:288
  128.7 0.0 all-to-all-done.2.got_ref
  128.7 0.8 copy-done.5
  129.6 5.2 %shard_map.150 = (bf16[4,32,2048]{2,1,0:T(8,128)(2,1)}, bf16[4,32,2048]{2,1,0:T(8,128)(2,1)}) custom-call(bf16[16,144,128]{2,1,0:T(8,128)(2,1)} %copy-done.5, f32[2,128,128]{2,1,0:T(8,128)} %bitcast.11, f32[2,1,128]{2,1,0:T(1,128)} %bitcast.16, f32[256,128]{1,0:T(8,128)} %get-tuple-element.34.cols_ref, bf16[256,128]{1,0:T(8,128)(2,1)} %get-tuple-element.46.q_ref, ...), custom_call_target="tpu_custom_call" | custom-call | flops 2000000000 | tf_op jit(solution)/shard_map/pallas_call | solution.py:288
  134.7 14.0 %collective-permute-start.6 = (bf16[4,32,2048]{2,1,0:T(8,128)(2,1)}, bf16[4,32,2048]{2,1,0:T(8,128)(2,1)S(1)}, u32[]{:S(2)}, u32[]{:S(2)}) collective-permute-start(bf16[4,32,2048]{2,1,0:T(8,128)(2,1)} %get-tuple-element.52), channel_id=1, source_target_pairs={{0,1},{1,0},{2,3},{3,2},{4,5},{5,4},{6,7},{7,6},{8,9},{9,8},{10,11... | collective-permute-start | bytes 1572872 | tf_op jit(solution)/shard_map/ppermute | solution.py:391
  148.7 1.7 %collective-permute-done.6 = bf16[4,32,2048]{2,1,0:T(8,128)(2,1)S(1)} collective-permute-done((bf16[4,32,2048]{2,1,0:T(8,128)(2,1)}, bf16[4,32,2048]{2,1,0:T(8,128)(2,1)S(1)}, u32[]{:S(2)}, u32[]{:S(2)}) %collective-permute-start.6) | collective-permute-done | bytes 524320 | tf_op jit(solution)/shard_map/ppermute | solution.py:391
  150.4 1.2 add_convert_fusion
  151.6 12.4 %all_to_all.20 = bf16[4,32,2048]{2,1,0:T(8,128)(2,1)S(1)} all-to-all(bf16[4,32,2048]{2,1,0:T(8,128)(2,1)S(1)} %add_convert_fusion), channel_id=1, replica_groups={{0,2,4,6},{1,3,5,7},{8,10,12,14},{9,11,13,15},{16,18,20,22},{17,19,21,2..., dimensions={0} | all-to-all | bytes 1048576 | tf_op jit(solution)/shard_map/all_to_all | solution.py:394
  164.1 0.7 reduce_sum.12
  (8 shorter events, 0.1 us)
Async XLA Ops:
  1.5 53.7 %all-to-all-start = ((bf16[16,32,256]{2,1,0:T(8,128)(2,1)}), bf16[16,32,256]{2,1,0:T(8,128)(2,1)S(1)}, u32[]{:S(2)}, u32[]{:S(2)}) async-start(bf16[16,32,256]{2,1,0:T(8,128)(2,1)} %get-tuple-element.30), calls=%async_computation | async-start | bytes 524288 | tf_op jit(solution)/shard_map/all_to_all | solution.py:322
  55.2 5.4 %copy-start.1 = (bf16[512,896]{1,0:T(8,128)(2,1)}, bf16[512,896]{1,0:T(8,128)(2,1)S(1)}, u32[]{:S(2)}) copy-start(bf16[512,896]{1,0:T(8,128)(2,1)S(1)} %all_gather.3) | copy-start | bytes 2752516
  56.4 13.9 %all-to-all-start.1 = ((bf16[4,512,256]{2,1,0:T(8,128)(2,1)}), bf16[4,512,256]{2,1,0:T(8,128)(2,1)S(1)}, u32[]{:S(2)}, u32[]{:S(2)}) async-start(bf16[4,512,256]{2,1,0:T(8,128)(2,1)} %broadcast_in_dim.7), calls=%async_computation.1 | async-start | bytes 2097152 | tf_op jit(solution)/shard_map/all_to_all | solution.py:25
  60.6 3.3 %slice-start = ((bf16[512,896]{1,0:T(8,128)(2,1)}), bf16[512,640]{1,0:T(8,128)(2,1)S(1)}, s32[]{:S(2)}) async-start(bf16[512,896]{1,0:T(8,128)(2,1)} %copy-done.1), calls=%async_computation.4 | async-start | bytes 1310720 | tf_op jit(solution)/shard_map/slice | solution.py:343
  64.0 29.7 %copy-start = (bf16[512,896]{1,0:T(8,128)(2,1)}, bf16[512,896]{1,0:T(8,128)(2,1)S(1)}, u32[]{:S(2)}) copy-start(bf16[512,896]{1,0:T(8,128)(2,1)S(1)} %pad_maximum_fusion.w0_ref) | copy-start | bytes 2752516
  70.3 1.0 copy-start.2
  74.7 23.9 %copy-start.6 = (bf16[16,2048]{1,0:T(8,128)(2,1)S(1)}, bf16[16,2048]{1,0:T(8,128)(2,1)}, u32[]{:S(2)}) copy-start(bf16[16,2048]{1,0:T(8,128)(2,1)} %get-tuple-element.43) | copy-start | bytes 196612
  74.7 54.0 %all-to-all-start.2 = ((bf16[16,144,128]{2,1,0:T(8,128)(2,1)}), bf16[16,144,128]{2,1,0:T(8,128)(2,1)S(1)}, u32[]{:S(2)}, u32[]{:S(2)}) async-start(bf16[16,144,128]{2,1,0:T(8,128)(2,1)} %get-tuple-element.39), calls=%async_computation.2 | async-start | bytes 1179648 | tf_op jit(solution)/shard_map/all_to_all | solution.py:357
  84.4 17.5 %collective-permute-start = (bf16[512,896]{1,0:T(8,128)(2,1)S(1)}, bf16[512,896]{1,0:T(8,128)(2,1)S(1)}, u32[]{:S(2)}, u32[]{:S(2)}) collective-permute-start(bf16[512,896]{1,0:T(8,128)(2,1)S(1)} %pad_maximum_fusion.w0_ref), channel_id=1, source_target_pairs={{0,8},{8,16},{16,24},{24,0},{1,9},{9,17},{17,25},{25,1},{2,10},{10... | collective-permute-start | bytes 2752520 | tf_op jit(solution)/shard_map/ppermute | solution.py:46
  86.6 16.6 %collective-permute-start.2 = (bf16[512,896]{1,0:T(8,128)(2,1)S(1)}, bf16[512,896]{1,0:T(8,128)(2,1)S(1)}, u32[]{:S(2)}, u32[]{:S(2)}) collective-permute-start(bf16[512,896]{1,0:T(8,128)(2,1)S(1)} %pad_maximum_fusion.w0_ref), channel_id=1, source_target_pairs={{0,24},{8,0},{16,8},{24,16},{1,25},{9,1},{17,9},{25,17},{2,26},{10... | collective-permute-start | bytes 2752520 | tf_op jit(solution)/shard_map/ppermute | solution.py:46
  91.8 31.9 %collective-permute-start.1 = (bf16[512,512]{1,0:T(8,128)(2,1)}, bf16[512,512]{1,0:T(8,128)(2,1)}, u32[]{:S(2)}, u32[]{:S(2)}) collective-permute-start(bf16[512,512]{1,0:T(8,128)(2,1)} %slice.20), channel_id=1, source_target_pairs={{0,16},{8,24},{16,0},{24,8},{1,17},{9,25},{17,1},{25,9},{2,18},{10... | collective-permute-start | bytes 1572872 | tf_op jit(solution)/shard_map/ppermute | solution.py:46
  93.8 26.6 %collective-permute-start.5 = (bf16[512,384]{1,0:T(8,128)(2,1)S(1)}, bf16[512,384]{1,0:T(8,128)(2,1)}, u32[]{:S(2)}, u32[]{:S(2)}) collective-permute-start(bf16[512,384]{1,0:T(8,128)(2,1)S(1)} %slice.23), channel_id=1, source_target_pairs={{0,16},{8,24},{16,0},{24,8},{1,17},{9,25},{17,1},{25,9},{2,18},{10... | collective-permute-start | bytes 1179656 | tf_op jit(solution)/shard_map/ppermute | solution.py:46
  98.7 25.0 %collective-permute-start.3 = (bf16[8,2048]{1,0:T(8,128)(2,1)S(1)}, bf16[8,2048]{1,0:T(8,128)(2,1)S(1)}, u32[]{:S(2)}, u32[]{:S(2)}) collective-permute-start(bf16[8,2048]{1,0:T(8,128)(2,1)S(1)} %get-tuple-element.54), channel_id=1, source_target_pairs={{0,32},{32,64},{64,96},{96,128},{128,160},{160,192},{192,224},{224... | collective-permute-start | bytes 98312 | tf_op jit(solution)/shard_map/ppermute | solution.py:349
  101.9 18.4 %copy-start.3 = (bf16[512,896]{1,0:T(8,128)(2,1)}, bf16[512,896]{1,0:T(8,128)(2,1)S(1)}, u32[]{:S(2)}) copy-start(bf16[512,896]{1,0:T(8,128)(2,1)S(1)} %collective-permute-done.w1_ref) | copy-start | bytes 2752516
  102.0 21.7 %collective-permute-start.4 = (bf16[8,2048]{1,0:T(8,128)(2,1)S(1)}, bf16[8,2048]{1,0:T(8,128)(2,1)S(1)}, u32[]{:S(2)}, u32[]{:S(2)}) collective-permute-start(bf16[8,2048]{1,0:T(8,128)(2,1)S(1)} %get-tuple-element.53), channel_id=1, source_target_pairs={{32,0},{64,32},{96,64},{128,96},{160,128},{192,160},{224,192},{256... | collective-permute-start | bytes 98312 | tf_op jit(solution)/shard_map/ppermute | solution.py:350
  103.3 17.1 %copy-start.4 = (bf16[512,896]{1,0:T(8,128)(2,1)}, bf16[512,896]{1,0:T(8,128)(2,1)S(1)}, u32[]{:S(2)}) copy-start(bf16[512,896]{1,0:T(8,128)(2,1)S(1)} %collective-permute-done.2.w3_ref) | copy-start | bytes 2752516
  123.7 0.6 copy-start.7
  123.7 0.6 copy-start.8
  128.7 0.8 copy-start.5
  134.7 15.7 %collective-permute-start.6 = (bf16[4,32,2048]{2,1,0:T(8,128)(2,1)}, bf16[4,32,2048]{2,1,0:T(8,128)(2,1)S(1)}, u32[]{:S(2)}, u32[]{:S(2)}) collective-permute-start(bf16[4,32,2048]{2,1,0:T(8,128)(2,1)} %get-tuple-element.52), channel_id=1, source_target_pairs={{0,1},{1,0},{2,3},{3,2},{4,5},{5,4},{6,7},{7,6},{8,9},{9,8},{10,11... | collective-permute-start | bytes 1572872 | tf_op jit(solution)/shard_map/ppermute | solution.py:391

commit v7 on v6

--- a/solution.py
+++ b/solution.py
@@ -18,6 +18,7 @@
 bf16 = jnp.bfloat16
 smem = pl.BlockSpec(memory_space=pltpu.SMEM)
 vmem = pl.BlockSpec(memory_space=pltpu.VMEM)
+first_columns = pl.BlockSpec((NZ * ROWS, 384), lambda i: (0, 0), memory_space=pltpu.VMEM)
 
 
 def from_everyone(x, axis):
@@ -29,7 +30,7 @@
     for z in range(NZ):
         copies_ref[z] = po_ref[...]
     at = 0
-    for ref in (k_ref, v_ref, q_ref, o_ref, p_ref, m_ref):
+    for ref in (k_ref, v_ref, m_ref, q_ref, o_ref, p_ref):
         width = ref.shape[1]
         out_ref[:, at : at + width] = ref[...]
         at += width
@@ -60,10 +61,13 @@
     return jnp.minimum(x, 0.0) - jnp.log1p(jnp.exp(-jnp.abs(x)))
 
 
-def gates_kernel(bias_ref, tok_ref, gain_ref, gw_ref, decay_ref, normed_ref, cols_ref, rows_ref, ends_ref):
+def gates_kernel(
+    bias_ref, tok_ref, gain_ref, gw_ref, decay_ref, normed_ref, cols_ref, rows_ref,
+    begin_ref, end_ref,
+):
     x = tok_ref[...].astype(f32)
-    ends_ref[:HALO] = tok_ref[:HALO]
-    ends_ref[HALO:] = tok_ref[tok_ref.shape[0] - HALO :]
+    begin_ref[...] = tok_ref[:HALO]
+    end_ref[...] = tok_ref[tok_ref.shape[0] - HALO :]
     count = x.shape[0]
     normed = rms_normed(x, gain_ref[...]).astype(bf16)
     normed_ref[...] = normed
@@ -180,7 +184,7 @@
     k_ref, v_ref, cols_ref, rows_ref,
     q_ref, o_ref, pool_ref, num_ref, den_ref, w_ref, a_ref, b_ref,
 ):
-    placed_by_source(lax.axis_index("fs"), (w0_ref, w1_ref, w2_ref, w3_ref), w_ref, 0, 512)
+    placed_by_source(lax.axis_index("fs"), (w0_ref, w1_ref, w2_ref, w3_ref), w_ref, 384, 896)
     weight = in_order(w_ref)
     halo = jnp.concatenate([lo_ref[...], hi_ref[...]], axis=0).astype(f32)
     halo = rms_normed(halo, gain_ref[...]).astype(bf16)
@@ -211,15 +215,11 @@
     den_ref[...] = dens
 
 
-def outs_kernel(w0_ref, w1_ref, w2_ref, w3_ref, out_ref, w_ref):
-    placed_by_source(lax.axis_index("fs"), (w0_ref, w1_ref, w2_ref, w3_ref), w_ref, 512, 896)
-    out_ref[...] = in_order(w_ref)
-
-
 def final_kernel(
     got_ref, mem_ref, nrm_ref, cols_ref, q_ref, o_ref, num_ref, den_ref,
-    gain_ref, pool_ref, wo_ref, keep_ref, give_ref,
+    gain_ref, pool_ref, w0_ref, w1_ref, w2_ref, w3_ref, keep_ref, give_ref, w_ref,
 ):
+    placed_by_source(lax.axis_index("fs"), (w0_ref, w1_ref, w2_ref, w3_ref), w_ref, 0, 384)
     position = lax.axis_index("sp")
     got_n, got_m, got_f = [], [], []
     for j in range(NZ):
@@ -268,8 +268,8 @@
     scaled = summed * lax.rsqrt(jnp.mean(summed * summed, axis=-1, keepdims=True) + norm_eps)
     gate = 1.0 / (1.0 + jnp.exp(-o_ref[...].astype(f32)))
     memory_out = (scaled * gain_ref[...] * gate).astype(bf16)
-    features = jnp.concatenate([memory_out, pool_ref[...]], axis=1)
-    result = lax.dot_general(features, wo_ref[...], last, preferred_element_type=f32)
+    features = jnp.concatenate([pool_ref[...], memory_out], axis=1)
+    result = lax.dot_general(features, in_order(w_ref), last, preferred_element_type=f32)
     core = lax.rem(lax.axis_index("tp"), 2)
     own = keep_ref.shape[1]
     for x in range(keep_ref.shape[0]):
@@ -283,11 +283,12 @@
     return jax.ShapeDtypeStruct(shape, dtype)
 
 
-def call(kernel, outs, scalars, *args, flops=0, scratch=()):
+def call(kernel, outs, scalars, *args, flops=0, scratch=(), specs=None):
     many = isinstance(outs, tuple)
     return pl.pallas_call(
         kernel,
-        in_specs=[smem] * len(scalars) + [vmem] * len(args),
+        grid=(1,) if specs else (),
+        in_specs=specs or [smem] * len(scalars) + [vmem] * len(args),
         out_specs=(vmem,) * len(outs) if many else vmem,
         out_shape=outs,
         scratch_shapes=list(scratch),
@@ -324,13 +325,14 @@
     kv_z, pool_z = lax.optimization_barrier((along_z[:, :256], pool_z))
     kv_weight = from_everyone(kv_z, "fs")
     own_tokens, along_z = lax.optimization_barrier((tokens[0], along_z))
-    normed, cols, rows, ends = call(
+    normed, cols, rows, begin, end = call(
         gates_kernel,
         (
             sds((count, width), bf16),
             sds((count, 128), f32),
             sds((8, count), f32),
-            sds((2 * HALO, width), bf16),
+            sds((HALO, width), bf16),
+            sds((HALO, width), bf16),
         ),
         (gate_bias.reshape(4),),
         own_tokens,
@@ -340,14 +342,14 @@
         flops=4 * 10**9,
     )
     first_rest, rows = lax.optimization_barrier(
-        (jnp.concatenate([along_z[:, 256:], pool_z], axis=1), rows)
+        (jnp.concatenate([pool_z, along_z[:, 256:]], axis=1), rows)
     )
     first_from = {}
     for shift in (1, 3):
         first_from[shift] = from_shift(first_rest, "fs", shift)
     length = lax.axis_size("sp")
-    low = lax.ppermute(ends[HALO:], "sp", [(i, i + 1) for i in range(length - 1)])
-    high = lax.ppermute(ends[:HALO], "sp", [(i + 1, i) for i in range(length - 1)])
+    low = lax.ppermute(end, "sp", [(i, i + 1) for i in range(length - 1)])
+    high = lax.ppermute(begin, "sp", [(i + 1, i) for i in range(length - 1)])
     k, v, packets = call(
         state_kernel,
         (sds((count, 128), bf16), sds((count, 128), bf16), sds((NZ, PACKET, 128), bf16)),
@@ -356,8 +358,8 @@
     )
     got = lax.all_to_all(packets, "sp", 0, 0, tiled=True)
     later_rest, k = lax.optimization_barrier((first_rest, k))
-    first_from[2] = from_shift(later_rest[:, :512], "fs", 2)
-    last_two = from_shift(later_rest[:, 512:], "fs", 2)
+    first_from[2] = from_shift(later_rest[:, 384:], "fs", 2)
+    last_two = from_shift(later_rest[:, :384], "fs", 2)
     q, outgate, pool_out, nums, dens = call(
         local_kernel,
         (
@@ -373,19 +375,16 @@
         scratch=[pltpu.VMEM((NY, NZ * ROWS, 512), bf16)]
         + [pltpu.VMEM((count + 32, 256), f32)] * 2,
     )
-    wo = call(
-        outs_kernel, sds((width, 384), bf16), (),
-        first_rest, first_from[1], last_two, first_from[3],
-        flops=10**8, scratch=[pltpu.VMEM((NY, NZ * ROWS, 384), bf16)],
-    )
     cores = 2
     chips = lax.axis_size("tp") // cores
     own = count // (chips * cores)
     keep, give = call(
         final_kernel, (sds((chips, own, width), bf16),) * 2, (),
         got, init_memory[0, :, 0], init_normalizer[0, :, 0][:, None], cols, q, outgate,
-        nums, dens, head_gain, pool_out, wo,
-        flops=2 * 10**9,
+        nums, dens, head_gain, pool_out,
+        first_rest, first_from[1], last_two, first_from[3],
+        flops=2 * 10**9, specs=[vmem] * 10 + [first_columns] * 4,
+        scratch=[pltpu.VMEM((NY, NZ * ROWS, 384), bf16)],
     )
     swap = [(i, i ^ 1) for i in range(chips * cores)]
     taken = lax.ppermute(give, "tp", swap)

time: 166 us -> 163 us (0.982)
  starting transfers between devices: 61.4 us -> 66.7 us
  waiting for transfers between devices: 25.1 us -> 20.4 us
  Pallas kernels: 21.2 us -> 18 us
    ppermute x4, waiting for transfers between devices: 17.1 us -> 8.06 us  [from_shift(): lax.ppermute(x, axis, [(i, (i + shift) % count) for i in range(count)])]
    ppermute x1, starting transfers between devices: 14 us -> 19 us  [per_device(): taken = lax.ppermute(give, 'tp', swap)]
    ppermute x2, waiting for transfers between devices: 0.01 us -> 4.24 us  [the longest x1 4.24 us: per_device(): high = lax.ppermute(begin, 'sp', [(i + 1, i) for i in range(length - 1)])]
    pallas_call x6 -> x5, Pallas kernels: 21.2 us -> 18 us  [call(): pl.pallas_call(kernel, grid=(1,) if specs else (), in_specs=specs or [sme...]
  transfers between devices with their start and end apart: 10 -> 10, of which waited for: 3 -> 5; matrix products, arithmetic and copies ran while one was open for 1% -> 0% of each run, Pallas kernels for 7% -> 5%
where the time goes in v7:
time: 163 us; the launch traced here: 161 us
  starting transfers between devices  66.7 us (41%)
  blocking collectives  50.4 us (31%)
  waiting for transfers between devices  20.4 us (13%)
  Pallas kernels  18 us (11%)
  local copies, waits for them, and re-layouts  3.85 us (2%)
  other arithmetic  1.98 us (1%)
    all_gather x1, blocking collectives, per_device(): along_z = lax.all_gather(packed, 'sp', axis=0, tiled=True)  37.9 us
    ppermute x1, starting transfers between devices, per_device(): taken = lax.ppermute(give, 'tp', swap)  19 us
    pallas_call x5, Pallas kernels, call(): pl.pallas_call(kernel, grid=(1,) if specs else (), in_specs=specs or [sme...  18 us
    all_to_all x1, starting transfers between devices, per_device(): lax.all_to_all(pool_copies, 'sp', 0, 0, tiled=True).reshape(NZ * ROWS, 256)  15.7 us
    ppermute x4, starting transfers between devices, from_shift(): lax.ppermute(x, axis, [(i, (i + shift) % count) for i in range(count)])  13.5 us
    all_to_all x1, blocking collectives, per_device(): lax.all_to_all(pairs, 'tp', 0, 0, axis_index_groups=groups, tiled=True)  12.4 us
    all_to_all x1, starting transfers between devices, per_device(): got = lax.all_to_all(packets, 'sp', 0, 0, tiled=True)  9.72 us
    ppermute x4, waiting for transfers between devices, from_shift(): lax.ppermute(x, axis, [(i, (i + shift) % count) for i in range(count)])  8.06 us
  transfers between devices with their start and end apart: 10, of which 5 were waited for; matrix products, arithmetic and copies ran while one was open for 0% of the time, Pallas kernels for 5%

profile of v7, /device:TPU:1, one launch (start us, length us, event | category | flops | bytes accessed | tf_op | source)
XLA Modules:
  0.0 161.4 jit_solution(11068892417295052490)
XLA Ops:
  0.0 1.6 shard_map.145
  1.6 15.7 %all-to-all-start = ((bf16[16,32,256]{2,1,0:T(8,128)(2,1)}), bf16[16,32,256]{2,1,0:T(8,128)(2,1)S(1)}, u32[]{:S(2)}, u32[]{:S(2)}) async-start(bf16[16,32,256]{2,1,0:T(8,128)(2,1)} %get-tuple-element.31), calls=%async_computation | async-start | bytes 524288 | tf_op jit(solution)/shard_map/all_to_all | solution.py:323
  17.3 37.9 %all_gather.3 = bf16[512,896]{1,0:T(8,128)(2,1)S(1)} all-gather(bf16[32,896]{1,0:T(8,128)(2,1)} %get-tuple-element.30), channel_id=1, replica_groups=mesh['sp'=16,'fs'=4,'tp'=8] {'sp'}, dimensions={0}, use_global_device_ids=true | all-gather | bytes 974848 | tf_op jit(solution)/shard_map/all_gather | solution.py:324
  55.2 0.0 copy-start.1
  55.2 0.0 all-to-all-done
  55.2 1.1 broadcast_in_dim.7
  56.4 4.2 %all-to-all-start.1 = ((bf16[4,512,256]{2,1,0:T(8,128)(2,1)}), bf16[4,512,256]{2,1,0:T(8,128)(2,1)S(1)}, u32[]{:S(2)}, u32[]{:S(2)}) async-start(bf16[4,512,256]{2,1,0:T(8,128)(2,1)} %broadcast_in_dim.7), calls=%async_computation.1 | async-start | bytes 2097152 | tf_op jit(solution)/shard_map/all_to_all | solution.py:26
  60.6 0.0 copy-done.1
  60.6 3.3 %shard_map.146 = (bf16[256,2048]{1,0:T(8,128)(2,1)}, f32[256,128]{1,0:T(8,128)}, f32[8,256]{1,0:T(8,128)}, bf16[8,2048]{1,0:T(8,128)(2,1)}, bf16[8,2048]{1,0:T(8,128)(2,1)}) custom-call(f32[4]{0:T(128)} %bitcast.17, bf16[256,2048]{1,0:T(8,128)(2,1)} %bitcast.10, f32[1,2048]{1,0:T(1,128)} %bitcast.13, bf16[4,2048]{1,0:T(4,128)(2,1)} %bitcast.12, ...), custom_call_target="tpu_custom_call" | custom-call | flops 4000000000 | tf_op jit(solution)/shard_map/pallas_call | solution.py:288
  63.9 0.0 slice-done
  63.9 0.1 pad_maximum_fusion.w0_ref
  64.0 0.0 copy-start
  64.0 6.3 %all-to-all-done.1.w_ref = bf16[4,512,256]{2,1,0:T(8,128)(2,1)S(1)} async-done(((bf16[4,512,256]{2,1,0:T(8,128)(2,1)}), bf16[4,512,256]{2,1,0:T(8,128)(2,1)S(1)}, u32[]{:S(2)}, u32[]{:S(2)}) %all-to-all-start.1) | async-done | bytes 1048608 | tf_op jit(solution)/shard_map/all_to_all | solution.py:26
  70.3 0.0 copy-start.2
  70.3 1.0 copy-done.2
  71.3 3.4 %shard_map.147 = (bf16[256,128]{1,0:T(8,128)(2,1)}, bf16[256,128]{1,0:T(8,128)(2,1)}, bf16[16,144,128]{2,1,0:T(8,128)(2,1)}) custom-call(bf16[4,512,256]{2,1,0:T(8,128)(2,1)} %copy-done.2, bf16[256,2048]{1,0:T(8,128)(2,1)} %get-tuple-element.34.normed_ref, f32[256,128]{1,0:T(8,128)} %get-tuple-element.35.cols_ref, f32[8,256]{1,0:T(8,128)} %get-tuple-element.39.rows_ref), custom_call_target="tpu_custom_call" | custom-call | flops 2000000000 | tf_op jit(solution)/shard_map/pallas_call | solution.py:288
  74.6 9.7 %all-to-all-start.2 = ((bf16[16,144,128]{2,1,0:T(8,128)(2,1)}), bf16[16,144,128]{2,1,0:T(8,128)(2,1)S(1)}, u32[]{:S(2)}, u32[]{:S(2)}) async-start(bf16[16,144,128]{2,1,0:T(8,128)(2,1)} %get-tuple-element.40), calls=%async_computation.2 | async-start | bytes 1179648 | tf_op jit(solution)/shard_map/all_to_all | solution.py:359
  84.4 2.2 %collective-permute-start = (bf16[512,896]{1,0:T(8,128)(2,1)S(1)}, bf16[512,896]{1,0:T(8,128)(2,1)S(1)}, u32[]{:S(2)}, u32[]{:S(2)}) collective-permute-start(bf16[512,896]{1,0:T(8,128)(2,1)S(1)} %pad_maximum_fusion.w0_ref), channel_id=1, source_target_pairs={{0,8},{8,16},{16,24},{24,0},{1,9},{9,17},{17,25},{25,1},{2,10},{10... | collective-permute-start | bytes 2752520 | tf_op jit(solution)/shard_map/ppermute | solution.py:47
  86.6 4.3 %collective-permute-start.2 = (bf16[512,896]{1,0:T(8,128)(2,1)S(1)}, bf16[512,896]{1,0:T(8,128)(2,1)S(1)}, u32[]{:S(2)}, u32[]{:S(2)}) collective-permute-start(bf16[512,896]{1,0:T(8,128)(2,1)S(1)} %pad_maximum_fusion.w0_ref), channel_id=1, source_target_pairs={{0,24},{8,0},{16,8},{24,16},{1,25},{9,1},{17,9},{25,17},{2,26},{10... | collective-permute-start | bytes 2752520 | tf_op jit(solution)/shard_map/ppermute | solution.py:47
  90.9 1.9 %collective-permute-start.1 = (bf16[512,512]{1,0:T(8,128)(2,1)S(1)}, bf16[512,512]{1,0:T(8,128)(2,1)S(1)}, u32[]{:S(2)}, u32[]{:S(2)}) collective-permute-start(bf16[512,512]{1,0:T(8,128)(2,1)S(1)} %slice.14), channel_id=1, source_target_pairs={{0,16},{8,24},{16,0},{24,8},{1,17},{9,25},{17,1},{25,9},{2,18},{10... | collective-permute-start | bytes 1572872 | tf_op jit(solution)/shard_map/ppermute | solution.py:47
  92.9 0.0 copy-done.8
  92.9 3.3 %collective-permute-start.3 = (bf16[8,2048]{1,0:T(8,128)(2,1)S(1)}, bf16[8,2048]{1,0:T(8,128)(2,1)S(1)}, u32[]{:S(2)}, u32[]{:S(2)}) collective-permute-start(bf16[8,2048]{1,0:T(8,128)(2,1)S(1)} %copy-done.8), channel_id=1, source_target_pairs={{0,32},{32,64},{64,96},{96,128},{128,160},{160,192},{192,224},{224... | collective-permute-start | bytes 98312 | tf_op jit(solution)/shard_map/ppermute | solution.py:351
  96.1 0.0 copy-done.7
  96.1 1.3 collective-permute-start.4
  97.4 0.0 copy-done
  97.5 0.0 collective-permute-done.3.lo_ref
  97.5 0.0 copy-start.9
  97.5 5.1 %collective-permute-start.5 = (bf16[512,384]{1,0:T(8,128)(2,1)S(1)}, bf16[512,384]{1,0:T(8,128)(2,1)}, u32[]{:S(2)}, u32[]{:S(2)}) collective-permute-start(bf16[512,384]{1,0:T(8,128)(2,1)S(1)} %slice.15), channel_id=1, source_target_pairs={{0,16},{8,24},{16,0},{24,8},{1,17},{9,25},{17,1},{25,9},{2,18},{10... | collective-permute-start | bytes 1179656 | tf_op jit(solution)/shard_map/ppermute | solution.py:47
  102.6 4.2 %collective-permute-done.4.hi_ref = bf16[8,2048]{1,0:T(8,128)(2,1)S(1)} collective-permute-done((bf16[8,2048]{1,0:T(8,128)(2,1)S(1)}, bf16[8,2048]{1,0:T(8,128)(2,1)S(1)}, u32[]{:S(2)}, u32[]{:S(2)}) %collective-permute-start.4) | collective-permute-done | bytes 32800 | tf_op jit(solution)/shard_map/ppermute | solution.py:352
  106.9 0.0 collective-permute-done.w1_ref
  106.9 0.0 collective-permute-done.2.w3_ref
  106.9 0.0 copy-start.5
  106.9 4.8 %collective-permute-done.1.w2_ref = bf16[512,512]{1,0:T(8,128)(2,1)S(1)} collective-permute-done((bf16[512,512]{1,0:T(8,128)(2,1)S(1)}, bf16[512,512]{1,0:T(8,128)(2,1)S(1)}, u32[]{:S(2)}, u32[]{:S(2)}) %collective-permute-start.1) | collective-permute-done | bytes 524320 | tf_op jit(solution)/shard_map/ppermute | solution.py:47
  111.7 0.0 copy-done.5
  111.7 0.0 copy-done.9
  111.7 0.0 copy-done.10
  111.7 0.0 copy-done.4
  111.7 0.8 copy-done.6
  112.5 4.4 %shard_map.148 = (bf16[256,128]{1,0:T(8,128)(2,1)}, bf16[256,128]{1,0:T(8,128)(2,1)}, bf16[256,256]{1,0:T(8,128)(2,1)}, f32[2,256,128]{2,1,0:T(8,128)}, f32[256,128]{1,0:T(8,128)}) custom-call(bf16[512,896]{1,0:T(8,128)(2,1)} %copy-done, bf16[512,896]{1,0:T(8,128)(2,1)} %copy-done.4, bf16[512,512]{1,0:T(8,128)(2,1)} %copy-done.6, ...), custom_call_target="tpu_custom_call" | custom-call | flops 5000000000 | tf_op jit(solution)/shard_map/pallas_call | solution.py:288
  116.9 3.2 %collective-permute-done.5.w2_ref = bf16[512,384]{1,0:T(8,128)(2,1)} collective-permute-done((bf16[512,384]{1,0:T(8,128)(2,1)S(1)}, bf16[512,384]{1,0:T(8,128)(2,1)}, u32[]{:S(2)}, u32[]{:S(2)}) %collective-permute-start.5) | collective-permute-done | bytes 393248 | tf_op jit(solution)/shard_map/ppermute | solution.py:47
  120.2 0.0 all-to-all-done.2.got_ref
  120.2 0.8 copy-done.3
  121.0 5.3 %shard_map.149 = (bf16[4,32,2048]{2,1,0:T(8,128)(2,1)}, bf16[4,32,2048]{2,1,0:T(8,128)(2,1)}) custom-call(bf16[16,144,128]{2,1,0:T(8,128)(2,1)} %copy-done.3, f32[2,128,128]{2,1,0:T(8,128)} %bitcast.11, f32[2,1,128]{2,1,0:T(1,128)} %bitcast.16, f32[256,128]{1,0:T(8,128)} %get-tuple-element.35.cols_ref, bf16[256,128]{1,0:T(8,128)(2,1)} %get-tuple-element.48.q_ref, ...), custom_call_target="tpu_custom_call" | custom-call | flops 2000000000 | tf_op jit(solution)/shard_map/pallas_call | solution.py:288
  126.3 19.0 %collective-permute-start.6 = (bf16[4,32,2048]{2,1,0:T(8,128)(2,1)}, bf16[4,32,2048]{2,1,0:T(8,128)(2,1)S(1)}, u32[]{:S(2)}, u32[]{:S(2)}) collective-permute-start(bf16[4,32,2048]{2,1,0:T(8,128)(2,1)} %get-tuple-element.54), channel_id=1, source_target_pairs={{0,1},{1,0},{2,3},{3,2},{4,5},{5,4},{6,7},{7,6},{8,9},{9,8},{10,11... | collective-permute-start | bytes 1572872 | tf_op jit(solution)/shard_map/ppermute | solution.py:390
  145.3 1.7 %collective-permute-done.6 = bf16[4,32,2048]{2,1,0:T(8,128)(2,1)S(1)} collective-permute-done((bf16[4,32,2048]{2,1,0:T(8,128)(2,1)}, bf16[4,32,2048]{2,1,0:T(8,128)(2,1)S(1)}, u32[]{:S(2)}, u32[]{:S(2)}) %collective-permute-start.6) | collective-permute-done | bytes 524320 | tf_op jit(solution)/shard_map/ppermute | solution.py:390
  147.1 1.2 add_convert_fusion
  148.2 12.4 %all_to_all.20 = bf16[4,32,2048]{2,1,0:T(8,128)(2,1)S(1)} all-to-all(bf16[4,32,2048]{2,1,0:T(8,128)(2,1)S(1)} %add_convert_fusion), channel_id=1, replica_groups={{0,2,4,6},{1,3,5,7},{8,10,12,14},{9,11,13,15},{16,18,20,22},{17,19,21,2..., dimensions={0} | all-to-all | bytes 1048576 | tf_op jit(solution)/shard_map/all_to_all | solution.py:393
  160.7 0.7 reduce_sum.12
  (10 shorter events, 0.1 us)
Async XLA Ops:
  1.6 53.7 %all-to-all-start = ((bf16[16,32,256]{2,1,0:T(8,128)(2,1)}), bf16[16,32,256]{2,1,0:T(8,128)(2,1)S(1)}, u32[]{:S(2)}, u32[]{:S(2)}) async-start(bf16[16,32,256]{2,1,0:T(8,128)(2,1)} %get-tuple-element.31), calls=%async_computation | async-start | bytes 524288 | tf_op jit(solution)/shard_map/all_to_all | solution.py:323
  55.2 5.4 %copy-start.1 = (bf16[512,896]{1,0:T(8,128)(2,1)}, bf16[512,896]{1,0:T(8,128)(2,1)S(1)}, u32[]{:S(2)}) copy-start(bf16[512,896]{1,0:T(8,128)(2,1)S(1)} %all_gather.3) | copy-start | bytes 2752516
  56.4 13.9 %all-to-all-start.1 = ((bf16[4,512,256]{2,1,0:T(8,128)(2,1)}), bf16[4,512,256]{2,1,0:T(8,128)(2,1)S(1)}, u32[]{:S(2)}, u32[]{:S(2)}) async-start(bf16[4,512,256]{2,1,0:T(8,128)(2,1)} %broadcast_in_dim.7), calls=%async_computation.1 | async-start | bytes 2097152 | tf_op jit(solution)/shard_map/all_to_all | solution.py:26
  60.6 3.3 %slice-start = ((bf16[512,896]{1,0:T(8,128)(2,1)}), bf16[512,640]{1,0:T(8,128)(2,1)S(1)}, s32[]{:S(2)}) async-start(bf16[512,896]{1,0:T(8,128)(2,1)} %copy-done.1), calls=%async_computation.4 | async-start | bytes 1310720 | tf_op jit(solution)/shard_map/slice | solution.py:345
  64.0 33.5 %copy-start = (bf16[512,896]{1,0:T(8,128)(2,1)}, bf16[512,896]{1,0:T(8,128)(2,1)S(1)}, u32[]{:S(2)}) copy-start(bf16[512,896]{1,0:T(8,128)(2,1)S(1)} %pad_maximum_fusion.w0_ref) | copy-start | bytes 2752516
  70.3 1.0 copy-start.2
  74.6 18.2 %copy-start.8 = (bf16[8,2048]{1,0:T(8,128)(2,1)S(1)}, bf16[8,2048]{1,0:T(8,128)(2,1)}, u32[]{:S(2)}) copy-start(bf16[8,2048]{1,0:T(8,128)(2,1)} %get-tuple-element.44) | copy-start | bytes 98308
  74.6 21.5 %copy-start.7 = (bf16[8,2048]{1,0:T(8,128)(2,1)S(1)}, bf16[8,2048]{1,0:T(8,128)(2,1)}, u32[]{:S(2)}) copy-start(bf16[8,2048]{1,0:T(8,128)(2,1)} %get-tuple-element.45) | copy-start | bytes 98308
  74.6 45.5 %all-to-all-start.2 = ((bf16[16,144,128]{2,1,0:T(8,128)(2,1)}), bf16[16,144,128]{2,1,0:T(8,128)(2,1)S(1)}, u32[]{:S(2)}, u32[]{:S(2)}) async-start(bf16[16,144,128]{2,1,0:T(8,128)(2,1)} %get-tuple-element.40), calls=%async_computation.2 | async-start | bytes 1179648 | tf_op jit(solution)/shard_map/all_to_all | solution.py:359
  84.4 22.5 %collective-permute-start = (bf16[512,896]{1,0:T(8,128)(2,1)S(1)}, bf16[512,896]{1,0:T(8,128)(2,1)S(1)}, u32[]{:S(2)}, u32[]{:S(2)}) collective-permute-start(bf16[512,896]{1,0:T(8,128)(2,1)S(1)} %pad_maximum_fusion.w0_ref), channel_id=1, source_target_pairs={{0,8},{8,16},{16,24},{24,0},{1,9},{9,17},{17,25},{25,1},{2,10},{10... | collective-permute-start | bytes 2752520 | tf_op jit(solution)/shard_map/ppermute | solution.py:47
  86.6 20.3 %collective-permute-start.2 = (bf16[512,896]{1,0:T(8,128)(2,1)S(1)}, bf16[512,896]{1,0:T(8,128)(2,1)S(1)}, u32[]{:S(2)}, u32[]{:S(2)}) collective-permute-start(bf16[512,896]{1,0:T(8,128)(2,1)S(1)} %pad_maximum_fusion.w0_ref), channel_id=1, source_target_pairs={{0,24},{8,0},{16,8},{24,16},{1,25},{9,1},{17,9},{25,17},{2,26},{10... | collective-permute-start | bytes 2752520 | tf_op jit(solution)/shard_map/ppermute | solution.py:47
  90.9 20.8 %collective-permute-start.1 = (bf16[512,512]{1,0:T(8,128)(2,1)S(1)}, bf16[512,512]{1,0:T(8,128)(2,1)S(1)}, u32[]{:S(2)}, u32[]{:S(2)}) collective-permute-start(bf16[512,512]{1,0:T(8,128)(2,1)S(1)} %slice.14), channel_id=1, source_target_pairs={{0,16},{8,24},{16,0},{24,8},{1,17},{9,25},{17,1},{25,9},{2,18},{10... | collective-permute-start | bytes 1572872 | tf_op jit(solution)/shard_map/ppermute | solution.py:47
  92.9 4.6 %collective-permute-start.3 = (bf16[8,2048]{1,0:T(8,128)(2,1)S(1)}, bf16[8,2048]{1,0:T(8,128)(2,1)S(1)}, u32[]{:S(2)}, u32[]{:S(2)}) collective-permute-start(bf16[8,2048]{1,0:T(8,128)(2,1)S(1)} %copy-done.8), channel_id=1, source_target_pairs={{0,32},{32,64},{64,96},{96,128},{128,160},{160,192},{192,224},{224... | collective-permute-start | bytes 98312 | tf_op jit(solution)/shard_map/ppermute | solution.py:351
  96.1 10.7 %collective-permute-start.4 = (bf16[8,2048]{1,0:T(8,128)(2,1)S(1)}, bf16[8,2048]{1,0:T(8,128)(2,1)S(1)}, u32[]{:S(2)}, u32[]{:S(2)}) collective-permute-start(bf16[8,2048]{1,0:T(8,128)(2,1)S(1)} %copy-done.7), channel_id=1, source_target_pairs={{32,0},{64,32},{96,64},{128,96},{160,128},{192,160},{224,192},{256... | collective-permute-start | bytes 98312 | tf_op jit(solution)/shard_map/ppermute | solution.py:352
  97.5 14.2 %copy-start.9 = (bf16[8,2048]{1,0:T(8,128)(2,1)}, bf16[8,2048]{1,0:T(8,128)(2,1)S(1)}, u32[]{:S(2)}) copy-start(bf16[8,2048]{1,0:T(8,128)(2,1)S(1)} %collective-permute-done.3.lo_ref) | copy-start | bytes 98308
  97.5 22.6 %collective-permute-start.5 = (bf16[512,384]{1,0:T(8,128)(2,1)S(1)}, bf16[512,384]{1,0:T(8,128)(2,1)}, u32[]{:S(2)}, u32[]{:S(2)}) collective-permute-start(bf16[512,384]{1,0:T(8,128)(2,1)S(1)} %slice.15), channel_id=1, source_target_pairs={{0,16},{8,24},{16,0},{24,8},{1,17},{9,25},{17,1},{25,9},{2,18},{10... | collective-permute-start | bytes 1179656 | tf_op jit(solution)/shard_map/ppermute | solution.py:47
  106.9 4.8 %copy-start.10 = (bf16[8,2048]{1,0:T(8,128)(2,1)}, bf16[8,2048]{1,0:T(8,128)(2,1)S(1)}, u32[]{:S(2)}) copy-start(bf16[8,2048]{1,0:T(8,128)(2,1)S(1)} %collective-permute-done.4.hi_ref) | copy-start | bytes 98308
  106.9 4.8 %copy-start.4 = (bf16[512,896]{1,0:T(8,128)(2,1)}, bf16[512,896]{1,0:T(8,128)(2,1)S(1)}, u32[]{:S(2)}) copy-start(bf16[512,896]{1,0:T(8,128)(2,1)S(1)} %collective-permute-done.w1_ref) | copy-start | bytes 2752516
  106.9 4.8 %copy-start.5 = (bf16[512,896]{1,0:T(8,128)(2,1)}, bf16[512,896]{1,0:T(8,128)(2,1)S(1)}, u32[]{:S(2)}) copy-start(bf16[512,896]{1,0:T(8,128)(2,1)S(1)} %collective-permute-done.2.w3_ref) | copy-start | bytes 2752516
  111.7 0.8 copy-start.6
  120.2 0.8 copy-start.3
  126.3 20.8 %collective-permute-start.6 = (bf16[4,32,2048]{2,1,0:T(8,128)(2,1)}, bf16[4,32,2048]{2,1,0:T(8,128)(2,1)S(1)}, u32[]{:S(2)}, u32[]{:S(2)}) collective-permute-start(bf16[4,32,2048]{2,1,0:T(8,128)(2,1)} %get-tuple-element.54), channel_id=1, source_target_pairs={{0,1},{1,0},{2,3},{3,2},{4,5},{5,4},{6,7},{7,6},{8,9},{9,8},{10,11... | collective-permute-start | bytes 1572872 | tf_op jit(solution)/shard_map/ppermute | solution.py:390

commit v8 on v7

--- a/solution.py
+++ b/solution.py
@@ -12,7 +12,7 @@
 NY = 4
 ROWS = 32
 LOWEST = -1e30
-PACKET = 144
+PACKET = 136
 
 f32 = jnp.float32
 bf16 = jnp.bfloat16
@@ -139,9 +139,11 @@
         memory = memory + lax.dot_general(low, k, over_time, preferred_element_type=f32)
         norm = jnp.sum(w * k_wide, axis=0, keepdims=True) * scale
         extra = in_three(norm)
-        extra = extra + in_three(rows_ref[2 + 2 * r : 3 + 2 * r, :128])
-        extra = extra + in_three(rows_ref[3 + 2 * r : 4 + 2 * r, :128])
-        extra = jnp.concatenate(extra + [jnp.zeros((7, 128), f32)], axis=0)
+        level = rows_ref[2 + 2 * r : 3 + 2 * r, :128]
+        total = rows_ref[3 + 2 * r : 4 + 2 * r, :128]
+        lane = lax.broadcasted_iota(jnp.int32, (1, 128), 1)
+        extra = extra + in_three(jnp.where(lane < 64, level, total))
+        extra = jnp.concatenate(extra + [jnp.zeros((2, 128), f32)], axis=0)
         packets.append(jnp.concatenate([memory * scale, extra], axis=0).astype(bf16))
     for j in range(NZ):
 
@@ -225,8 +227,9 @@
     for j in range(NZ):
         extra = got_ref[j, 128:PACKET].astype(f32)
         got_n.append(extra[0:1] + extra[1:2] + extra[2:3])
-        got_m.append(extra[3:4] + extra[4:5] + extra[5:6])
-        got_f.append(extra[6:7] + extra[7:8] + extra[8:9])
+        ends = extra[3:4] + extra[4:5] + extra[5:6]
+        got_m.append(jnp.broadcast_to(ends[:, 0:1], (1, 128)))
+        got_f.append(jnp.broadcast_to(ends[:, 64:65], (1, 128)))
     q = q_ref[...]
     q_wide = q.astype(f32)
     last = (((1,), (1,)), ((), ()))
@@ -271,12 +274,14 @@
     features = jnp.concatenate([pool_ref[...], memory_out], axis=1)
     result = lax.dot_general(features, in_order(w_ref), last, preferred_element_type=f32)
     core = lax.rem(lax.axis_index("tp"), 2)
-    own = keep_ref.shape[1]
-    for x in range(keep_ref.shape[0]):
+    chip = lax.div(lax.axis_index("tp"), 2)
+    chips, own = keep_ref.shape[:2]
+    for x in range(chips):
         south = result[2 * x * own : (2 * x + 1) * own]
         north = result[(2 * x + 1) * own : (2 * x + 2) * own]
-        keep_ref[x] = jnp.where(core == 0, south, north).astype(bf16)
-        give_ref[x] = jnp.where(core == 0, north, south).astype(bf16)
+        slot = lax.rem(x + chips - chip, chips)
+        keep_ref[slot] = jnp.where(core == 0, south, north).astype(bf16)
+        give_ref[slot] = jnp.where(core == 0, north, south).astype(bf16)
 
 
 def sds(shape, dtype):
@@ -388,10 +393,12 @@
     )
     swap = [(i, i ^ 1) for i in range(chips * cores)]
     taken = lax.ppermute(give, "tp", swap)
-    pairs = (keep.astype(f32) + taken.astype(f32)).astype(bf16)
-    groups = [list(range(c, chips * cores, cores)) for c in range(cores)]
-    parts = lax.all_to_all(pairs, "tp", 0, 0, axis_index_groups=groups, tiled=True)
-    mixed = jnp.sum(parts.astype(f32), axis=0).astype(bf16)
+    pairs = [(keep[x].astype(f32) + taken[x].astype(f32)).astype(bf16) for x in range(chips)]
+    total = pairs[0].astype(f32)
+    for shift in range(1, chips):
+        route = [(i, (i + cores * shift) % (chips * cores)) for i in range(chips * cores)]
+        total = total + lax.ppermute(pairs[shift], "tp", route).astype(f32)
+    mixed = total.astype(bf16)
     return mixed.reshape(1, own, width)
 
 

time: 163 us -> 166 us (1.018)
  blocking collectives: 50.4 us -> 37.9 us
  starting transfers between devices: 66.7 us -> 75.3 us
  waiting for transfers between devices: 20.4 us -> 27.2 us
    all_to_all x1 -> x0, blocking collectives: 12.4 us -> none  [per_device(): lax.all_to_all(pairs, 'tp', 0, 0, axis_index_groups=groups, tiled=True)]
    ppermute x0 -> x3, starting transfers between devices: none -> 9.33 us  [per_device(): total = total + lax.ppermute(pairs[shift], 'tp', route).astype(f32)]
    ppermute x0 -> x3, waiting for transfers between devices: none -> 6.17 us  [per_device(): total = total + lax.ppermute(pairs[shift], 'tp', route).astype(f32)]
  transfers between devices with their start and end apart: 10 -> 13, of which waited for: 5 -> 8; matrix products, arithmetic and copies ran while one was open for 0% -> 0% of each run, Pallas kernels for 5% -> 5%
where the time goes in v8:
time: 166 us; the launch traced here: 165 us
  starting transfers between devices  75.3 us (45%)
  blocking collectives  37.9 us (23%)
  waiting for transfers between devices  27.2 us (16%)
  Pallas kernels  17.9 us (11%)
  local copies, waits for them, and re-layouts  3.81 us (2%)
  other arithmetic  2.85 us (2%)
    all_gather x1, blocking collectives, per_device(): along_z = lax.all_gather(packed, 'sp', axis=0, tiled=True)  37.9 us
    ppermute x1, starting transfers between devices, per_device(): taken = lax.ppermute(give, 'tp', swap)  19 us
    pallas_call x5, Pallas kernels, call(): pl.pallas_call(kernel, grid=(1,) if specs else (), in_specs=specs or [sme...  17.9 us
    all_to_all x1, starting transfers between devices, per_device(): lax.all_to_all(pool_copies, 'sp', 0, 0, tiled=True).reshape(NZ * ROWS, 256)  15.7 us
    ppermute x4, starting transfers between devices, from_shift(): lax.ppermute(x, axis, [(i, (i + shift) % count) for i in range(count)])  12.8 us
    all_to_all x1, starting transfers between devices, per_device(): got = lax.all_to_all(packets, 'sp', 0, 0, tiled=True)  9.72 us
    ppermute x3, starting transfers between devices, per_device(): total = total + lax.ppermute(pairs[shift], 'tp', route).astype(f32)  9.33 us
    ppermute x4, waiting for transfers between devices, from_shift(): lax.ppermute(x, axis, [(i, (i + shift) % count) for i in range(count)])  9.1 us
  transfers between devices with their start and end apart: 13, of which 8 were waited for; matrix products, arithmetic and copies ran while one was open for 0% of the time, Pallas kernels for 5%

profile of v8, /device:TPU:1, one launch (start us, length us, event | category | flops | bytes accessed | tf_op | source)
XLA Modules:
  0.0 165.2 jit_solution(9161115433844207178)
XLA Ops:
  0.0 1.5 shard_map.145
  1.5 15.7 %all-to-all-start = ((bf16[16,32,256]{2,1,0:T(8,128)(2,1)}), bf16[16,32,256]{2,1,0:T(8,128)(2,1)S(1)}, u32[]{:S(2)}, u32[]{:S(2)}) async-start(bf16[16,32,256]{2,1,0:T(8,128)(2,1)} %get-tuple-element.31), calls=%async_computation | async-start | bytes 524288 | tf_op jit(solution)/shard_map/all_to_all | solution.py:328
  17.3 37.9 %all_gather.3 = bf16[512,896]{1,0:T(8,128)(2,1)S(1)} all-gather(bf16[32,896]{1,0:T(8,128)(2,1)} %get-tuple-element.30), channel_id=1, replica_groups=mesh['sp'=16,'fs'=4,'tp'=8] {'sp'}, dimensions={0}, use_global_device_ids=true | all-gather | bytes 974848 | tf_op jit(solution)/shard_map/all_gather | solution.py:329
  55.2 0.0 all-to-all-done
  55.2 1.1 broadcast_in_dim.7
  56.4 4.2 %all-to-all-start.1 = ((bf16[4,512,256]{2,1,0:T(8,128)(2,1)}), bf16[4,512,256]{2,1,0:T(8,128)(2,1)S(1)}, u32[]{:S(2)}, u32[]{:S(2)}) async-start(bf16[4,512,256]{2,1,0:T(8,128)(2,1)} %broadcast_in_dim.7), calls=%async_computation.1 | async-start | bytes 2097152 | tf_op jit(solution)/shard_map/all_to_all | solution.py:26
  60.5 0.0 copy-done.1
  60.5 3.3 %shard_map.146 = (bf16[256,2048]{1,0:T(8,128)(2,1)}, f32[256,128]{1,0:T(8,128)}, f32[8,256]{1,0:T(8,128)}, bf16[8,2048]{1,0:T(8,128)(2,1)}, bf16[8,2048]{1,0:T(8,128)(2,1)}) custom-call(f32[4]{0:T(128)} %bitcast.31, bf16[256,2048]{1,0:T(8,128)(2,1)} %bitcast.24, f32[1,2048]{1,0:T(1,128)} %bitcast.27, bf16[4,2048]{1,0:T(4,128)(2,1)} %bitcast.26, ...), custom_call_target="tpu_custom_call" | custom-call | flops 4000000000 | tf_op jit(solution)/shard_map/pallas_call | solution.py:293
  63.9 0.0 slice-done
  63.9 0.1 pad_maximum_fusion.w0_ref
  64.0 0.0 copy-start
  64.0 6.3 %all-to-all-done.1.w_ref = bf16[4,512,256]{2,1,0:T(8,128)(2,1)S(1)} async-done(((bf16[4,512,256]{2,1,0:T(8,128)(2,1)}), bf16[4,512,256]{2,1,0:T(8,128)(2,1)S(1)}, u32[]{:S(2)}, u32[]{:S(2)}) %all-to-all-start.1) | async-done | bytes 1048608 | tf_op jit(solution)/shard_map/all_to_all | solution.py:26
  70.3 1.0 copy-done.2
  71.3 3.4 %shard_map.147 = (bf16[256,128]{1,0:T(8,128)(2,1)}, bf16[256,128]{1,0:T(8,128)(2,1)}, bf16[16,136,128]{2,1,0:T(8,128)(2,1)}) custom-call(bf16[4,512,256]{2,1,0:T(8,128)(2,1)} %copy-done.2, bf16[256,2048]{1,0:T(8,128)(2,1)} %get-tuple-element.34.normed_ref, f32[256,128]{1,0:T(8,128)} %get-tuple-element.35.cols_ref, f32[8,256]{1,0:T(8,128)} %get-tuple-element.39.rows_ref), custom_call_target="tpu_custom_call" | custom-call | flops 2000000000 | tf_op jit(solution)/shard_map/pallas_call | solution.py:293
  74.6 9.7 %all-to-all-start.2 = ((bf16[16,136,128]{2,1,0:T(8,128)(2,1)}), bf16[16,136,128]{2,1,0:T(8,128)(2,1)S(1)}, u32[]{:S(2)}, u32[]{:S(2)}) async-start(bf16[16,136,128]{2,1,0:T(8,128)(2,1)} %get-tuple-element.40), calls=%async_computation.2 | async-start | bytes 1114112 | tf_op jit(solution)/shard_map/all_to_all | solution.py:364
  84.3 2.2 %collective-permute-start = (bf16[512,896]{1,0:T(8,128)(2,1)S(1)}, bf16[512,896]{1,0:T(8,128)(2,1)S(1)}, u32[]{:S(2)}, u32[]{:S(2)}) collective-permute-start(bf16[512,896]{1,0:T(8,128)(2,1)S(1)} %pad_maximum_fusion.w0_ref), channel_id=1, source_target_pairs={{0,8},{8,16},{16,24},{24,0},{1,9},{9,17},{17,25},{25,1},{2,10},{10... | collective-permute-start | bytes 2752520 | tf_op jit(solution)/shard_map/ppermute | solution.py:47
  86.5 4.3 %collective-permute-start.2 = (bf16[512,896]{1,0:T(8,128)(2,1)S(1)}, bf16[512,896]{1,0:T(8,128)(2,1)S(1)}, u32[]{:S(2)}, u32[]{:S(2)}) collective-permute-start(bf16[512,896]{1,0:T(8,128)(2,1)S(1)} %pad_maximum_fusion.w0_ref), channel_id=1, source_target_pairs={{0,24},{8,0},{16,8},{24,16},{1,25},{9,1},{17,9},{25,17},{2,26},{10... | collective-permute-start | bytes 2752520 | tf_op jit(solution)/shard_map/ppermute | solution.py:47
  90.9 1.9 %collective-permute-start.1 = (bf16[512,512]{1,0:T(8,128)(2,1)S(1)}, bf16[512,512]{1,0:T(8,128)(2,1)S(1)}, u32[]{:S(2)}, u32[]{:S(2)}) collective-permute-start(bf16[512,512]{1,0:T(8,128)(2,1)S(1)} %slice.38), channel_id=1, source_target_pairs={{0,16},{8,24},{16,0},{24,8},{1,17},{9,25},{17,1},{25,9},{2,18},{10... | collective-permute-start | bytes 1572872 | tf_op jit(solution)/shard_map/ppermute | solution.py:47
  92.8 0.0 copy-done.8
  92.8 3.3 %collective-permute-start.3 = (bf16[8,2048]{1,0:T(8,128)(2,1)S(1)}, bf16[8,2048]{1,0:T(8,128)(2,1)S(1)}, u32[]{:S(2)}, u32[]{:S(2)}) collective-permute-start(bf16[8,2048]{1,0:T(8,128)(2,1)S(1)} %copy-done.8), channel_id=1, source_target_pairs={{0,32},{32,64},{64,96},{96,128},{128,160},{160,192},{192,224},{224... | collective-permute-start | bytes 98312 | tf_op jit(solution)/shard_map/ppermute | solution.py:356
  96.1 0.0 copy-done.7
  96.1 1.3 collective-permute-start.4
  97.4 0.0 copy-done
  97.5 1.1 collective-permute-done.3.lo_ref
  98.6 4.4 %collective-permute-start.5 = (bf16[512,384]{1,0:T(8,128)(2,1)S(1)}, bf16[512,384]{1,0:T(8,128)(2,1)}, u32[]{:S(2)}, u32[]{:S(2)}) collective-permute-start(bf16[512,384]{1,0:T(8,128)(2,1)S(1)} %slice.39), channel_id=1, source_target_pairs={{0,16},{8,24},{16,0},{24,8},{1,17},{9,25},{17,1},{25,9},{2,18},{10... | collective-permute-start | bytes 1179656 | tf_op jit(solution)/shard_map/ppermute | solution.py:47
  103.0 2.8 %collective-permute-done.4.hi_ref = bf16[8,2048]{1,0:T(8,128)(2,1)S(1)} collective-permute-done((bf16[8,2048]{1,0:T(8,128)(2,1)S(1)}, bf16[8,2048]{1,0:T(8,128)(2,1)S(1)}, u32[]{:S(2)}, u32[]{:S(2)}) %collective-permute-start.4) | collective-permute-done | bytes 32800 | tf_op jit(solution)/shard_map/ppermute | solution.py:357
  105.8 0.0 collective-permute-done.w1_ref
  105.8 0.0 collective-permute-done.2.w3_ref
  105.8 0.0 copy-start.5
  105.8 5.8 %collective-permute-done.1.w2_ref = bf16[512,512]{1,0:T(8,128)(2,1)S(1)} collective-permute-done((bf16[512,512]{1,0:T(8,128)(2,1)S(1)}, bf16[512,512]{1,0:T(8,128)(2,1)S(1)}, u32[]{:S(2)}, u32[]{:S(2)}) %collective-permute-start.1) | collective-permute-done | bytes 524320 | tf_op jit(solution)/shard_map/ppermute | solution.py:47
  111.7 0.0 copy-done.5
  111.7 0.0 copy-done.10
  111.7 0.8 copy-done.6
  112.5 4.4 %shard_map.148 = (bf16[256,128]{1,0:T(8,128)(2,1)}, bf16[256,128]{1,0:T(8,128)(2,1)}, bf16[256,256]{1,0:T(8,128)(2,1)}, f32[2,256,128]{2,1,0:T(8,128)}, f32[256,128]{1,0:T(8,128)}) custom-call(bf16[512,896]{1,0:T(8,128)(2,1)} %copy-done, bf16[512,896]{1,0:T(8,128)(2,1)} %copy-done.4, bf16[512,512]{1,0:T(8,128)(2,1)} %copy-done.6, ...), custom_call_target="tpu_custom_call" | custom-call | flops 5000000000 | tf_op jit(solution)/shard_map/pallas_call | solution.py:293
  116.9 3.3 %collective-permute-done.5.w2_ref = bf16[512,384]{1,0:T(8,128)(2,1)} collective-permute-done((bf16[512,384]{1,0:T(8,128)(2,1)S(1)}, bf16[512,384]{1,0:T(8,128)(2,1)}, u32[]{:S(2)}, u32[]{:S(2)}) %collective-permute-start.5) | collective-permute-done | bytes 393248 | tf_op jit(solution)/shard_map/ppermute | solution.py:47
  120.1 0.0 all-to-all-done.2.got_ref
  120.1 0.8 copy-done.3
  121.0 5.2 %shard_map.149 = (bf16[4,32,2048]{2,1,0:T(8,128)(2,1)}, bf16[4,32,2048]{2,1,0:T(8,128)(2,1)}) custom-call(bf16[16,136,128]{2,1,0:T(8,128)(2,1)} %copy-done.3, f32[2,128,128]{2,1,0:T(8,128)} %bitcast.25, f32[2,1,128]{2,1,0:T(1,128)} %bitcast.30, f32[256,128]{1,0:T(8,128)} %get-tuple-element.35.cols_ref, bf16[256,128]{1,0:T(8,128)(2,1)} %get-tuple-element.48.q_ref, ...), custom_call_target="tpu_custom_call" | custom-call | flops 2000000000 | tf_op jit(solution)/shard_map/pallas_call | solution.py:293
  126.2 19.0 %collective-permute-start.6 = (bf16[4,32,2048]{2,1,0:T(8,128)(2,1)}, bf16[4,32,2048]{2,1,0:T(8,128)(2,1)S(1)}, u32[]{:S(2)}, u32[]{:S(2)}) collective-permute-start(bf16[4,32,2048]{2,1,0:T(8,128)(2,1)} %get-tuple-element.54), channel_id=1, source_target_pairs={{0,1},{1,0},{2,3},{3,2},{4,5},{5,4},{6,7},{7,6},{8,9},{9,8},{10,11... | collective-permute-start | bytes 1572872 | tf_op jit(solution)/shard_map/ppermute | solution.py:395
  145.2 1.7 %collective-permute-done.6 = bf16[4,32,2048]{2,1,0:T(8,128)(2,1)S(1)} collective-permute-done((bf16[4,32,2048]{2,1,0:T(8,128)(2,1)}, bf16[4,32,2048]{2,1,0:T(8,128)(2,1)S(1)}, u32[]{:S(2)}, u32[]{:S(2)}) %collective-permute-start.6) | collective-permute-done | bytes 524320 | tf_op jit(solution)/shard_map/ppermute | solution.py:395
  146.9 1.1 fusion.4
  148.0 4.4 %collective-permute-start.9 = (bf16[32,2048]{1,0:T(8,128)(2,1)S(1)}, bf16[32,2048]{1,0:T(8,128)(2,1)S(1)}, u32[]{:S(2)}, u32[]{:S(2)}) collective-permute-start(bf16[32,2048]{1,0:T(8,128)(2,1)S(1)} %get-tuple-element.56), channel_id=1, source_target_pairs={{0,6},{1,7},{2,0},{3,1},{4,2},{5,3},{6,4},{7,5},{8,14},{9,15},{10,... | collective-permute-start | bytes 393224 | tf_op jit(solution)/shard_map/ppermute | solution.py:400
  152.4 2.4 %collective-permute-start.8 = (bf16[32,2048]{1,0:T(8,128)(2,1)S(1)}, bf16[32,2048]{1,0:T(8,128)(2,1)S(1)}, u32[]{:S(2)}, u32[]{:S(2)}) collective-permute-start(bf16[32,2048]{1,0:T(8,128)(2,1)S(1)} %get-tuple-element.57), channel_id=1, source_target_pairs={{0,4},{1,5},{2,6},{3,7},{4,0},{5,1},{6,2},{7,3},{8,12},{9,13},{10,... | collective-permute-start | bytes 393224 | tf_op jit(solution)/shard_map/ppermute | solution.py:400
  154.9 2.5 %collective-permute-start.7 = (bf16[32,2048]{1,0:T(8,128)(2,1)S(1)}, bf16[32,2048]{1,0:T(8,128)(2,1)S(1)}, u32[]{:S(2)}, u32[]{:S(2)}) collective-permute-start(bf16[32,2048]{1,0:T(8,128)(2,1)S(1)} %get-tuple-element.55), channel_id=1, source_target_pairs={{0,2},{1,3},{2,4},{3,5},{4,6},{5,7},{6,0},{7,1},{8,10},{9,11},{10,... | collective-permute-start | bytes 393224 | tf_op jit(solution)/shard_map/ppermute | solution.py:400
  157.4 0.0 collective-permute-done.9
  157.4 2.8 %collective-permute-done.8 = bf16[32,2048]{1,0:T(8,128)(2,1)S(1)} collective-permute-done((bf16[32,2048]{1,0:T(8,128)(2,1)S(1)}, bf16[32,2048]{1,0:T(8,128)(2,1)S(1)}, u32[]{:S(2)}, u32[]{:S(2)}) %collective-permute-start.8) | collective-permute-done | bytes 131104 | tf_op jit(solution)/shard_map/ppermute | solution.py:400
  160.2 3.3 %collective-permute-done.7 = bf16[32,2048]{1,0:T(8,128)(2,1)S(1)} collective-permute-done((bf16[32,2048]{1,0:T(8,128)(2,1)S(1)}, bf16[32,2048]{1,0:T(8,128)(2,1)S(1)}, u32[]{:S(2)}, u32[]{:S(2)}) %collective-permute-start.7) | collective-permute-done | bytes 131104 | tf_op jit(solution)/shard_map/ppermute | solution.py:400
  163.6 1.6 fusion.7
  (15 shorter events, 0.1 us)
Async XLA Ops:
  1.5 53.7 %all-to-all-start = ((bf16[16,32,256]{2,1,0:T(8,128)(2,1)}), bf16[16,32,256]{2,1,0:T(8,128)(2,1)S(1)}, u32[]{:S(2)}, u32[]{:S(2)}) async-start(bf16[16,32,256]{2,1,0:T(8,128)(2,1)} %get-tuple-element.31), calls=%async_computation | async-start | bytes 524288 | tf_op jit(solution)/shard_map/all_to_all | solution.py:328
  55.2 5.3 %copy-start.1 = (bf16[512,896]{1,0:T(8,128)(2,1)}, bf16[512,896]{1,0:T(8,128)(2,1)S(1)}, u32[]{:S(2)}) copy-start(bf16[512,896]{1,0:T(8,128)(2,1)S(1)} %all_gather.3) | copy-start | bytes 2752516
  56.4 13.9 %all-to-all-start.1 = ((bf16[4,512,256]{2,1,0:T(8,128)(2,1)}), bf16[4,512,256]{2,1,0:T(8,128)(2,1)S(1)}, u32[]{:S(2)}, u32[]{:S(2)}) async-start(bf16[4,512,256]{2,1,0:T(8,128)(2,1)} %broadcast_in_dim.7), calls=%async_computation.1 | async-start | bytes 2097152 | tf_op jit(solution)/shard_map/all_to_all | solution.py:26
  60.5 3.3 %slice-start = ((bf16[512,896]{1,0:T(8,128)(2,1)}), bf16[512,640]{1,0:T(8,128)(2,1)S(1)}, s32[]{:S(2)}) async-start(bf16[512,896]{1,0:T(8,128)(2,1)} %copy-done.1), calls=%async_computation.3 | async-start | bytes 1310720 | tf_op jit(solution)/shard_map/slice | solution.py:350
  64.0 33.5 %copy-start = (bf16[512,896]{1,0:T(8,128)(2,1)}, bf16[512,896]{1,0:T(8,128)(2,1)S(1)}, u32[]{:S(2)}) copy-start(bf16[512,896]{1,0:T(8,128)(2,1)S(1)} %pad_maximum_fusion.w0_ref) | copy-start | bytes 2752516
  70.3 1.0 copy-start.2
  74.6 18.2 %copy-start.8 = (bf16[8,2048]{1,0:T(8,128)(2,1)S(1)}, bf16[8,2048]{1,0:T(8,128)(2,1)}, u32[]{:S(2)}) copy-start(bf16[8,2048]{1,0:T(8,128)(2,1)} %get-tuple-element.44) | copy-start | bytes 98308
  74.6 21.5 %copy-start.7 = (bf16[8,2048]{1,0:T(8,128)(2,1)S(1)}, bf16[8,2048]{1,0:T(8,128)(2,1)}, u32[]{:S(2)}) copy-start(bf16[8,2048]{1,0:T(8,128)(2,1)} %get-tuple-element.45) | copy-start | bytes 98308
  74.6 45.5 %all-to-all-start.2 = ((bf16[16,136,128]{2,1,0:T(8,128)(2,1)}), bf16[16,136,128]{2,1,0:T(8,128)(2,1)S(1)}, u32[]{:S(2)}, u32[]{:S(2)}) async-start(bf16[16,136,128]{2,1,0:T(8,128)(2,1)} %get-tuple-element.40), calls=%async_computation.2 | async-start | bytes 1114112 | tf_op jit(solution)/shard_map/all_to_all | solution.py:364
  84.3 21.5 %collective-permute-start = (bf16[512,896]{1,0:T(8,128)(2,1)S(1)}, bf16[512,896]{1,0:T(8,128)(2,1)S(1)}, u32[]{:S(2)}, u32[]{:S(2)}) collective-permute-start(bf16[512,896]{1,0:T(8,128)(2,1)S(1)} %pad_maximum_fusion.w0_ref), channel_id=1, source_target_pairs={{0,8},{8,16},{16,24},{24,0},{1,9},{9,17},{17,25},{25,1},{2,10},{10... | collective-permute-start | bytes 2752520 | tf_op jit(solution)/shard_map/ppermute | solution.py:47
  86.5 19.3 %collective-permute-start.2 = (bf16[512,896]{1,0:T(8,128)(2,1)S(1)}, bf16[512,896]{1,0:T(8,128)(2,1)S(1)}, u32[]{:S(2)}, u32[]{:S(2)}) collective-permute-start(bf16[512,896]{1,0:T(8,128)(2,1)S(1)} %pad_maximum_fusion.w0_ref), channel_id=1, source_target_pairs={{0,24},{8,0},{16,8},{24,16},{1,25},{9,1},{17,9},{25,17},{2,26},{10... | collective-permute-start | bytes 2752520 | tf_op jit(solution)/shard_map/ppermute | solution.py:47
  90.9 20.8 %collective-permute-start.1 = (bf16[512,512]{1,0:T(8,128)(2,1)S(1)}, bf16[512,512]{1,0:T(8,128)(2,1)S(1)}, u32[]{:S(2)}, u32[]{:S(2)}) collective-permute-start(bf16[512,512]{1,0:T(8,128)(2,1)S(1)} %slice.38), channel_id=1, source_target_pairs={{0,16},{8,24},{16,0},{24,8},{1,17},{9,25},{17,1},{25,9},{2,18},{10... | collective-permute-start | bytes 1572872 | tf_op jit(solution)/shard_map/ppermute | solution.py:47
  92.8 5.7 %collective-permute-start.3 = (bf16[8,2048]{1,0:T(8,128)(2,1)S(1)}, bf16[8,2048]{1,0:T(8,128)(2,1)S(1)}, u32[]{:S(2)}, u32[]{:S(2)}) collective-permute-start(bf16[8,2048]{1,0:T(8,128)(2,1)S(1)} %copy-done.8), channel_id=1, source_target_pairs={{0,32},{32,64},{64,96},{96,128},{128,160},{160,192},{192,224},{224... | collective-permute-start | bytes 98312 | tf_op jit(solution)/shard_map/ppermute | solution.py:356
  96.1 9.7 %collective-permute-start.4 = (bf16[8,2048]{1,0:T(8,128)(2,1)S(1)}, bf16[8,2048]{1,0:T(8,128)(2,1)S(1)}, u32[]{:S(2)}, u32[]{:S(2)}) collective-permute-start(bf16[8,2048]{1,0:T(8,128)(2,1)S(1)} %copy-done.7), channel_id=1, source_target_pairs={{32,0},{64,32},{96,64},{128,96},{160,128},{192,160},{224,192},{256... | collective-permute-start | bytes 98312 | tf_op jit(solution)/shard_map/ppermute | solution.py:357
  98.6 13.1 %copy-start.9 = (bf16[8,2048]{1,0:T(8,128)(2,1)}, bf16[8,2048]{1,0:T(8,128)(2,1)S(1)}, u32[]{:S(2)}) copy-start(bf16[8,2048]{1,0:T(8,128)(2,1)S(1)} %collective-permute-done.3.lo_ref) | copy-start | bytes 98308
  98.6 21.6 %collective-permute-start.5 = (bf16[512,384]{1,0:T(8,128)(2,1)S(1)}, bf16[512,384]{1,0:T(8,128)(2,1)}, u32[]{:S(2)}, u32[]{:S(2)}) collective-permute-start(bf16[512,384]{1,0:T(8,128)(2,1)S(1)} %slice.39), channel_id=1, source_target_pairs={{0,16},{8,24},{16,0},{24,8},{1,17},{9,25},{17,1},{25,9},{2,18},{10... | collective-permute-start | bytes 1179656 | tf_op jit(solution)/shard_map/ppermute | solution.py:47
  105.8 5.9 %copy-start.10 = (bf16[8,2048]{1,0:T(8,128)(2,1)}, bf16[8,2048]{1,0:T(8,128)(2,1)S(1)}, u32[]{:S(2)}) copy-start(bf16[8,2048]{1,0:T(8,128)(2,1)S(1)} %collective-permute-done.4.hi_ref) | copy-start | bytes 98308
  105.8 5.9 %copy-start.4 = (bf16[512,896]{1,0:T(8,128)(2,1)}, bf16[512,896]{1,0:T(8,128)(2,1)S(1)}, u32[]{:S(2)}) copy-start(bf16[512,896]{1,0:T(8,128)(2,1)S(1)} %collective-permute-done.w1_ref) | copy-start | bytes 2752516
  105.8 5.9 %copy-start.5 = (bf16[512,896]{1,0:T(8,128)(2,1)}, bf16[512,896]{1,0:T(8,128)(2,1)S(1)}, u32[]{:S(2)}) copy-start(bf16[512,896]{1,0:T(8,128)(2,1)S(1)} %collective-permute-done.2.w3_ref) | copy-start | bytes 2752516
  111.7 0.8 copy-start.6
  120.1 0.8 copy-start.3
  126.2 20.7 %collective-permute-start.6 = (bf16[4,32,2048]{2,1,0:T(8,128)(2,1)}, bf16[4,32,2048]{2,1,0:T(8,128)(2,1)S(1)}, u32[]{:S(2)}, u32[]{:S(2)}) collective-permute-start(bf16[4,32,2048]{2,1,0:T(8,128)(2,1)} %get-tuple-element.54), channel_id=1, source_target_pairs={{0,1},{1,0},{2,3},{3,2},{4,5},{5,4},{6,7},{7,6},{8,9},{9,8},{10,11... | collective-permute-start | bytes 1572872 | tf_op jit(solution)/shard_map/ppermute | solution.py:395
  148.0 9.4 %collective-permute-start.9 = (bf16[32,2048]{1,0:T(8,128)(2,1)S(1)}, bf16[32,2048]{1,0:T(8,128)(2,1)S(1)}, u32[]{:S(2)}, u32[]{:S(2)}) collective-permute-start(bf16[32,2048]{1,0:T(8,128)(2,1)S(1)} %get-tuple-element.56), channel_id=1, source_target_pairs={{0,6},{1,7},{2,0},{3,1},{4,2},{5,3},{6,4},{7,5},{8,14},{9,15},{10,... | collective-permute-start | bytes 393224 | tf_op jit(solution)/shard_map/ppermute | solution.py:400
  152.4 7.8 %collective-permute-start.8 = (bf16[32,2048]{1,0:T(8,128)(2,1)S(1)}, bf16[32,2048]{1,0:T(8,128)(2,1)S(1)}, u32[]{:S(2)}, u32[]{:S(2)}) collective-permute-start(bf16[32,2048]{1,0:T(8,128)(2,1)S(1)} %get-tuple-element.57), channel_id=1, source_target_pairs={{0,4},{1,5},{2,6},{3,7},{4,0},{5,1},{6,2},{7,3},{8,12},{9,13},{10,... | collective-permute-start | bytes 393224 | tf_op jit(solution)/shard_map/ppermute | solution.py:400
  154.9 8.7 %collective-permute-start.7 = (bf16[32,2048]{1,0:T(8,128)(2,1)S(1)}, bf16[32,2048]{1,0:T(8,128)(2,1)S(1)}, u32[]{:S(2)}, u32[]{:S(2)}) collective-permute-start(bf16[32,2048]{1,0:T(8,128)(2,1)S(1)} %get-tuple-element.55), channel_id=1, source_target_pairs={{0,2},{1,3},{2,4},{3,5},{4,6},{5,7},{6,0},{7,1},{8,10},{9,11},{10,... | collective-permute-start | bytes 393224 | tf_op jit(solution)/shard_map/ppermute | solution.py:400

commit v9 on v7

--- a/solution.py
+++ b/solution.py
@@ -12,7 +12,7 @@
 NY = 4
 ROWS = 32
 LOWEST = -1e30
-PACKET = 144
+PACKET = 136
 
 f32 = jnp.float32
 bf16 = jnp.bfloat16
@@ -139,9 +139,11 @@
         memory = memory + lax.dot_general(low, k, over_time, preferred_element_type=f32)
         norm = jnp.sum(w * k_wide, axis=0, keepdims=True) * scale
         extra = in_three(norm)
-        extra = extra + in_three(rows_ref[2 + 2 * r : 3 + 2 * r, :128])
-        extra = extra + in_three(rows_ref[3 + 2 * r : 4 + 2 * r, :128])
-        extra = jnp.concatenate(extra + [jnp.zeros((7, 128), f32)], axis=0)
+        level = rows_ref[2 + 2 * r : 3 + 2 * r, :128]
+        total = rows_ref[3 + 2 * r : 4 + 2 * r, :128]
+        lane = lax.broadcasted_iota(jnp.int32, (1, 128), 1)
+        extra = extra + in_three(jnp.where(lane < 64, level, total))
+        extra = jnp.concatenate(extra + [jnp.zeros((2, 128), f32)], axis=0)
         packets.append(jnp.concatenate([memory * scale, extra], axis=0).astype(bf16))
     for j in range(NZ):
 
@@ -225,8 +227,9 @@
     for j in range(NZ):
         extra = got_ref[j, 128:PACKET].astype(f32)
         got_n.append(extra[0:1] + extra[1:2] + extra[2:3])
-        got_m.append(extra[3:4] + extra[4:5] + extra[5:6])
-        got_f.append(extra[6:7] + extra[7:8] + extra[8:9])
+        ends = extra[3:4] + extra[4:5] + extra[5:6]
+        got_m.append(jnp.broadcast_to(ends[:, 0:1], (1, 128)))
+        got_f.append(jnp.broadcast_to(ends[:, 64:65], (1, 128)))
     q = q_ref[...]
     q_wide = q.astype(f32)
     last = (((1,), (1,)), ((), ()))
@@ -283,8 +286,19 @@
     return jax.ShapeDtypeStruct(shape, dtype)
 
 
-def call(kernel, outs, scalars, *args, flops=0, scratch=(), specs=None):
+def far(shape, dtype):
+    return pltpu.HBM(shape, dtype)
+
+
+def call(kernel, outs, scalars, *args, flops=0, scratch=(), specs=None, close=None):
     many = isinstance(outs, tuple)
+    grant = None
+    if close is not None:
+        grant = 24 * 2**20
+        args = [
+            pltpu.with_memory_space_constraint(x, pltpu.VMEM if n == close else pltpu.HBM)
+            for n, x in enumerate(args)
+        ]
     return pl.pallas_call(
         kernel,
         grid=(1,) if specs else (),
@@ -293,6 +307,7 @@
         out_shape=outs,
         scratch_shapes=list(scratch),
         cost_estimate=pl.CostEstimate(flops=flops, bytes_accessed=0, transcendentals=0),
+        compiler_params=pltpu.CompilerParams(vmem_limit_bytes=grant),
     )(*scalars, *args)
 
 
@@ -352,9 +367,9 @@
     high = lax.ppermute(begin, "sp", [(i + 1, i) for i in range(length - 1)])
     k, v, packets = call(
         state_kernel,
-        (sds((count, 128), bf16), sds((count, 128), bf16), sds((NZ, PACKET, 128), bf16)),
+        (far((count, 128), bf16), far((count, 128), bf16), far((NZ, PACKET, 128), bf16)),
         (), kv_weight, normed, cols, rows,
-        flops=2 * 10**9,
+        flops=2 * 10**9, close=0,
     )
     got = lax.all_to_all(packets, "sp", 0, 0, tiled=True)
     later_rest, k = lax.optimization_barrier((first_rest, k))
@@ -363,15 +378,15 @@
     q, outgate, pool_out, nums, dens = call(
         local_kernel,
         (
-            sds((count, 128), bf16),
-            sds((count, 128), bf16),
-            sds((count, 256), bf16),
-            sds((2, count, 128), f32),
-            sds((count, 128), f32),
+            far((count, 128), bf16),
+            far((count, 128), bf16),
+            far((count, 256), bf16),
+            far((2, count, 128), f32),
+            far((count, 128), f32),
         ),
         (), first_rest, *(first_from[s] for s in (1, 2, 3)), normed, low, high,
         norm_gain[None], k, v, cols, rows,
-        flops=5 * 10**9,
+        flops=5 * 10**9, close=2,
         scratch=[pltpu.VMEM((NY, NZ * ROWS, 512), bf16)]
         + [pltpu.VMEM((count + 32, 256), f32)] * 2,
     )
@@ -383,7 +398,7 @@
         got, init_memory[0, :, 0], init_normalizer[0, :, 0][:, None], cols, q, outgate,
         nums, dens, head_gain, pool_out,
         first_rest, first_from[1], last_two, first_from[3],
-        flops=2 * 10**9, specs=[vmem] * 10 + [first_columns] * 4,
+        flops=2 * 10**9, close=0, specs=[vmem] * 10 + [first_columns] * 4,
         scratch=[pltpu.VMEM((NY, NZ * ROWS, 384), bf16)],
     )
     swap = [(i, i ^ 1) for i in range(chips * cores)]

time: 163 us -> 158 us (0.969)
  local copies, waits for them, and re-layouts: 3.85 us -> 2.02 us
  Pallas kernels: 18 us -> 16.3 us
    ppermute x4, waiting for transfers between devices: 8.06 us -> 9.99 us  [from_shift(): lax.ppermute(x, axis, [(i, (i + shift) % count) for i in range(count)])]
    unnamed x22 -> x18, local copies, waits for them, and re-layouts: 2.62 us -> 0.78 us
    pallas_call x5, Pallas kernels: 18 us -> 16.3 us  [call(): pl.pallas_call(kernel, grid=(1,) if specs else (), in_specs=specs or [sme...]
  transfers between devices with their start and end apart: 10 -> 10, of which waited for: 5 -> 6; matrix products, arithmetic and copies ran while one was open for 0% -> 0% of each run, Pallas kernels for 5% -> 5%
where the time goes in v9:
time: 158 us; the launch traced here: 157 us
  starting transfers between devices  65.1 us (41%)
  blocking collectives  50.3 us (32%)
  waiting for transfers between devices  21.8 us (14%)
  Pallas kernels  16.3 us (10%)
  local copies, waits for them, and re-layouts  2.02 us (1%)
    all_gather x1, blocking collectives, per_device(): along_z = lax.all_gather(packed, 'sp', axis=0, tiled=True)  37.9 us
    ppermute x1, starting transfers between devices, per_device(): taken = lax.ppermute(give, 'tp', swap)  18.1 us
    pallas_call x5, Pallas kernels, call(): pl.pallas_call(kernel, grid=(1,) if specs else (), in_specs=specs or [sme...  16.3 us
    all_to_all x1, starting transfers between devices, per_device(): lax.all_to_all(pool_copies, 'sp', 0, 0, tiled=True).reshape(NZ * ROWS, 256)  15.7 us
    ppermute x4, starting transfers between devices, from_shift(): lax.ppermute(x, axis, [(i, (i + shift) % count) for i in range(count)])  12.8 us
    all_to_all x1, blocking collectives, per_device(): lax.all_to_all(pairs, 'tp', 0, 0, axis_index_groups=groups, tiled=True)  12.4 us
    ppermute x4, waiting for transfers between devices, from_shift(): lax.ppermute(x, axis, [(i, (i + shift) % count) for i in range(count)])  9.99 us
    all_to_all x1, starting transfers between devices, per_device(): got = lax.all_to_all(packets, 'sp', 0, 0, tiled=True)  9.72 us
  transfers between devices with their start and end apart: 10, of which 6 were waited for; matrix products, arithmetic and copies ran while one was open for 0% of the time, Pallas kernels for 5%

profile of v9, /device:TPU:1, one launch (start us, length us, event | category | flops | bytes accessed | tf_op | source)
XLA Modules:
  0.0 156.6 jit_solution(15054043523892199516)
XLA Ops:
  0.0 1.5 shard_map.145
  1.5 15.7 %all-to-all-start = ((bf16[16,32,256]{2,1,0:T(8,128)(2,1)}), bf16[16,32,256]{2,1,0:T(8,128)(2,1)S(1)}, u32[]{:S(2)}, u32[]{:S(2)}) async-start(bf16[16,32,256]{2,1,0:T(8,128)(2,1)} %get-tuple-element.31), calls=%async_computation | async-start | bytes 524288 | tf_op jit(solution)/shard_map/all_to_all | solution.py:338
  17.3 37.9 %all_gather.3 = bf16[512,896]{1,0:T(8,128)(2,1)S(1)} all-gather(bf16[32,896]{1,0:T(8,128)(2,1)} %get-tuple-element.30), channel_id=1, replica_groups=mesh['sp'=16,'fs'=4,'tp'=8] {'sp'}, dimensions={0}, use_global_device_ids=true | all-gather | bytes 974848 | tf_op jit(solution)/shard_map/all_gather | solution.py:339
  55.2 0.0 copy-start.1
  55.2 0.0 all-to-all-done
  55.2 1.1 broadcast_in_dim.7
  56.4 4.2 %all-to-all-start.1 = ((bf16[4,512,256]{2,1,0:T(8,128)(2,1)}), bf16[4,512,256]{2,1,0:T(8,128)(2,1)S(1)}, u32[]{:S(2)}, u32[]{:S(2)}) async-start(bf16[4,512,256]{2,1,0:T(8,128)(2,1)} %broadcast_in_dim.7), calls=%async_computation.1 | async-start | bytes 2097152 | tf_op jit(solution)/shard_map/all_to_all | solution.py:26
  60.6 0.0 copy-done.1
  60.6 0.0 slice-start
  60.6 3.3 %shard_map.146 = (bf16[256,2048]{1,0:T(8,128)(2,1)}, f32[256,128]{1,0:T(8,128)}, f32[8,256]{1,0:T(8,128)}, bf16[8,2048]{1,0:T(8,128)(2,1)}, bf16[8,2048]{1,0:T(8,128)(2,1)}) custom-call(f32[4]{0:T(128)} %bitcast.17, bf16[256,2048]{1,0:T(8,128)(2,1)} %bitcast.10, f32[1,2048]{1,0:T(1,128)} %bitcast.13, bf16[4,2048]{1,0:T(4,128)(2,1)} %bitcast.12, ...), custom_call_target="tpu_custom_call" | custom-call | flops 4000000000 | tf_op jit(solution)/shard_map/pallas_call | solution.py:302
  63.9 0.0 slice-done
  63.9 0.1 pad_maximum_fusion.w0_ref
  64.0 0.0 copy-start
  64.0 6.3 %all-to-all-done.1.w_ref = bf16[4,512,256]{2,1,0:T(8,128)(2,1)S(1)} async-done(((bf16[4,512,256]{2,1,0:T(8,128)(2,1)}), bf16[4,512,256]{2,1,0:T(8,128)(2,1)S(1)}, u32[]{:S(2)}, u32[]{:S(2)}) %all-to-all-start.1) | async-done | bytes 1048608 | tf_op jit(solution)/shard_map/all_to_all | solution.py:26
  70.3 3.1 %shard_map.147 = (bf16[256,128]{1,0:T(8,128)(2,1)}, bf16[256,128]{1,0:T(8,128)(2,1)}, bf16[16,136,128]{2,1,0:T(8,128)(2,1)}) custom-call(bf16[4,512,256]{2,1,0:T(8,128)(2,1)S(1)} %all-to-all-done.1.w_ref, bf16[256,2048]{1,0:T(8,128)(2,1)} %get-tuple-element.34.normed_ref, f32[256,128]{1,0:T(8,128)} %get-tuple-element.35.cols_ref, ...), custom_call_target="tpu_custom_call" | custom-call | flops 2000000000 | tf_op jit(solution)/shard_map/pallas_call | solution.py:302
  73.5 0.0 copy-start.6
  73.5 0.0 copy-start.5
  73.5 9.7 %all-to-all-start.2 = ((bf16[16,136,128]{2,1,0:T(8,128)(2,1)}), bf16[16,136,128]{2,1,0:T(8,128)(2,1)S(1)}, u32[]{:S(2)}, u32[]{:S(2)}) async-start(bf16[16,136,128]{2,1,0:T(8,128)(2,1)} %get-tuple-element.40), calls=%async_computation.2 | async-start | bytes 1114112 | tf_op jit(solution)/shard_map/all_to_all | solution.py:374
  83.2 2.2 %collective-permute-start = (bf16[512,896]{1,0:T(8,128)(2,1)S(1)}, bf16[512,896]{1,0:T(8,128)(2,1)S(1)}, u32[]{:S(2)}, u32[]{:S(2)}) collective-permute-start(bf16[512,896]{1,0:T(8,128)(2,1)S(1)} %pad_maximum_fusion.w0_ref), channel_id=1, source_target_pairs={{0,8},{8,16},{16,24},{24,0},{1,9},{9,17},{17,25},{25,1},{2,10},{10... | collective-permute-start | bytes 2752520 | tf_op jit(solution)/shard_map/ppermute | solution.py:47
  85.4 4.3 %collective-permute-start.2 = (bf16[512,896]{1,0:T(8,128)(2,1)S(1)}, bf16[512,896]{1,0:T(8,128)(2,1)S(1)}, u32[]{:S(2)}, u32[]{:S(2)}) collective-permute-start(bf16[512,896]{1,0:T(8,128)(2,1)S(1)} %pad_maximum_fusion.w0_ref), channel_id=1, source_target_pairs={{0,24},{8,0},{16,8},{24,16},{1,25},{9,1},{17,9},{25,17},{2,26},{10... | collective-permute-start | bytes 2752520 | tf_op jit(solution)/shard_map/ppermute | solution.py:47
  89.7 1.9 %collective-permute-start.1 = (bf16[512,512]{1,0:T(8,128)(2,1)S(1)}, bf16[512,512]{1,0:T(8,128)(2,1)S(1)}, u32[]{:S(2)}, u32[]{:S(2)}) collective-permute-start(bf16[512,512]{1,0:T(8,128)(2,1)S(1)} %slice.14), channel_id=1, source_target_pairs={{0,16},{8,24},{16,0},{24,8},{1,17},{9,25},{17,1},{25,9},{2,18},{10... | collective-permute-start | bytes 1572872 | tf_op jit(solution)/shard_map/ppermute | solution.py:47
  91.7 0.0 copy-done.6
  91.7 3.3 %collective-permute-start.3 = (bf16[8,2048]{1,0:T(8,128)(2,1)S(1)}, bf16[8,2048]{1,0:T(8,128)(2,1)S(1)}, u32[]{:S(2)}, u32[]{:S(2)}) collective-permute-start(bf16[8,2048]{1,0:T(8,128)(2,1)S(1)} %copy-done.6), channel_id=1, source_target_pairs={{0,32},{32,64},{64,96},{96,128},{128,160},{160,192},{192,224},{224... | collective-permute-start | bytes 98312 | tf_op jit(solution)/shard_map/ppermute | solution.py:366
  94.9 0.0 copy-done.5
  95.0 1.3 collective-permute-start.4
  96.3 0.0 copy-done
  96.3 1.1 collective-permute-done.3.lo_ref
  97.4 0.0 copy-start.7
  97.4 4.4 %collective-permute-start.5 = (bf16[512,384]{1,0:T(8,128)(2,1)S(1)}, bf16[512,384]{1,0:T(8,128)(2,1)S(1)}, u32[]{:S(2)}, u32[]{:S(2)}) collective-permute-start(bf16[512,384]{1,0:T(8,128)(2,1)S(1)} %slice.15), channel_id=1, source_target_pairs={{0,16},{8,24},{16,0},{24,8},{1,17},{9,25},{17,1},{25,9},{2,18},{10... | collective-permute-start | bytes 1179656 | tf_op jit(solution)/shard_map/ppermute | solution.py:47
  101.8 2.8 %collective-permute-done.4.hi_ref = bf16[8,2048]{1,0:T(8,128)(2,1)S(1)} collective-permute-done((bf16[8,2048]{1,0:T(8,128)(2,1)S(1)}, bf16[8,2048]{1,0:T(8,128)(2,1)S(1)}, u32[]{:S(2)}, u32[]{:S(2)}) %collective-permute-start.4) | collective-permute-done | bytes 32800 | tf_op jit(solution)/shard_map/ppermute | solution.py:367
  104.6 0.0 collective-permute-done.w1_ref
  104.7 0.0 collective-permute-done.2.w3_ref
  104.7 0.0 copy-start.3
  104.7 5.8 %collective-permute-done.1.w2_ref = bf16[512,512]{1,0:T(8,128)(2,1)S(1)} collective-permute-done((bf16[512,512]{1,0:T(8,128)(2,1)S(1)}, bf16[512,512]{1,0:T(8,128)(2,1)S(1)}, u32[]{:S(2)}, u32[]{:S(2)}) %collective-permute-start.1) | collective-permute-done | bytes 524320 | tf_op jit(solution)/shard_map/ppermute | solution.py:47
  110.5 0.0 copy-done.7
  110.5 0.0 copy-done.8
  110.5 0.0 copy-done.2
  110.5 0.0 copy-done.3
  110.5 4.3 %shard_map.148 = (bf16[256,128]{1,0:T(8,128)(2,1)}, bf16[256,128]{1,0:T(8,128)(2,1)}, bf16[256,256]{1,0:T(8,128)(2,1)}, f32[2,256,128]{2,1,0:T(8,128)}, f32[256,128]{1,0:T(8,128)}) custom-call(bf16[512,896]{1,0:T(8,128)(2,1)} %copy-done, bf16[512,896]{1,0:T(8,128)(2,1)} %copy-done.2, bf16[512,512]{1,0:T(8,128)(2,1)S(1)} %collective-permute-done.1.w2_ref, ...), custom_call_target="tpu_custom_call" | custom-call | flops 5000000000 | tf_op jit(solution)/shard_map/pallas_call | solution.py:302
  114.8 4.1 %collective-permute-done.5.w2_ref = bf16[512,384]{1,0:T(8,128)(2,1)S(1)} collective-permute-done((bf16[512,384]{1,0:T(8,128)(2,1)S(1)}, bf16[512,384]{1,0:T(8,128)(2,1)S(1)}, u32[]{:S(2)}, u32[]{:S(2)}) %collective-permute-start.5) | collective-permute-done | bytes 393248 | tf_op jit(solution)/shard_map/ppermute | solution.py:47
  119.0 0.0 all-to-all-done.2.got_ref
  119.0 0.7 copy-done.4
  119.7 4.0 %shard_map.149 = (bf16[4,32,2048]{2,1,0:T(8,128)(2,1)S(1)}, bf16[4,32,2048]{2,1,0:T(8,128)(2,1)S(1)}) custom-call(bf16[16,136,128]{2,1,0:T(8,128)(2,1)S(1)} %all-to-all-done.2.got_ref, f32[2,128,128]{2,1,0:T(8,128)} %bitcast.11, f32[2,1,128]{2,1,0:T(1,128)} %bitcast.16, f32[256,128]{1,0:T(8,128)} %get-tuple-element.35.cols_ref, ...), custom_call_target="tpu_custom_call" | custom-call | flops 2000000000 | tf_op jit(solution)/shard_map/pallas_call | solution.py:302
  123.7 18.1 %collective-permute-start.6 = (bf16[4,32,2048]{2,1,0:T(8,128)(2,1)S(1)}, bf16[4,32,2048]{2,1,0:T(8,128)(2,1)S(1)}, u32[]{:S(2)}, u32[]{:S(2)}) collective-permute-start(bf16[4,32,2048]{2,1,0:T(8,128)(2,1)S(1)} %get-tuple-element.54), channel_id=1, source_target_pairs={{0,1},{1,0},{2,3},{3,2},{4,5},{5,4},{6,7},{7,6},{8,9},{9,8},{10,11... | collective-permute-start | bytes 1572872 | tf_op jit(solution)/shard_map/ppermute | solution.py:405
  141.8 1.5 collective-permute-done.6
  143.3 0.1 add_convert_fusion
  143.5 12.4 %all_to_all.20 = bf16[4,32,2048]{2,1,0:T(8,128)(2,1)S(1)} all-to-all(bf16[4,32,2048]{2,1,0:T(8,128)(2,1)S(1)} %add_convert_fusion), channel_id=1, replica_groups={{0,2,4,6},{1,3,5,7},{8,10,12,14},{9,11,13,15},{16,18,20,22},{17,19,21,2..., dimensions={0} | all-to-all | bytes 1048576 | tf_op jit(solution)/shard_map/all_to_all | solution.py:408
  155.9 0.7 reduce_sum.12
  (6 shorter events, 0.1 us)
Async XLA Ops:
  1.5 53.7 %all-to-all-start = ((bf16[16,32,256]{2,1,0:T(8,128)(2,1)}), bf16[16,32,256]{2,1,0:T(8,128)(2,1)S(1)}, u32[]{:S(2)}, u32[]{:S(2)}) async-start(bf16[16,32,256]{2,1,0:T(8,128)(2,1)} %get-tuple-element.31), calls=%async_computation | async-start | bytes 524288 | tf_op jit(solution)/shard_map/all_to_all | solution.py:338
  55.2 5.4 %copy-start.1 = (bf16[512,896]{1,0:T(8,128)(2,1)}, bf16[512,896]{1,0:T(8,128)(2,1)S(1)}, u32[]{:S(2)}) copy-start(bf16[512,896]{1,0:T(8,128)(2,1)S(1)} %all_gather.3) | copy-start | bytes 2752516
  56.4 13.9 %all-to-all-start.1 = ((bf16[4,512,256]{2,1,0:T(8,128)(2,1)}), bf16[4,512,256]{2,1,0:T(8,128)(2,1)S(1)}, u32[]{:S(2)}, u32[]{:S(2)}) async-start(bf16[4,512,256]{2,1,0:T(8,128)(2,1)} %broadcast_in_dim.7), calls=%async_computation.1 | async-start | bytes 2097152 | tf_op jit(solution)/shard_map/all_to_all | solution.py:26
  60.6 3.3 %slice-start = ((bf16[512,896]{1,0:T(8,128)(2,1)}), bf16[512,640]{1,0:T(8,128)(2,1)S(1)}, s32[]{:S(2)}) async-start(bf16[512,896]{1,0:T(8,128)(2,1)} %copy-done.1), calls=%async_computation.4 | async-start | bytes 1310720 | tf_op jit(solution)/shard_map/slice | solution.py:360
  64.0 32.3 %copy-start = (bf16[512,896]{1,0:T(8,128)(2,1)}, bf16[512,896]{1,0:T(8,128)(2,1)S(1)}, u32[]{:S(2)}) copy-start(bf16[512,896]{1,0:T(8,128)(2,1)S(1)} %pad_maximum_fusion.w0_ref) | copy-start | bytes 2752516
  73.5 18.2 %copy-start.6 = (bf16[8,2048]{1,0:T(8,128)(2,1)S(1)}, bf16[8,2048]{1,0:T(8,128)(2,1)}, u32[]{:S(2)}) copy-start(bf16[8,2048]{1,0:T(8,128)(2,1)} %get-tuple-element.44) | copy-start | bytes 98308
  73.5 21.5 %copy-start.5 = (bf16[8,2048]{1,0:T(8,128)(2,1)S(1)}, bf16[8,2048]{1,0:T(8,128)(2,1)}, u32[]{:S(2)}) copy-start(bf16[8,2048]{1,0:T(8,128)(2,1)} %get-tuple-element.45) | copy-start | bytes 98308
  73.5 45.5 %all-to-all-start.2 = ((bf16[16,136,128]{2,1,0:T(8,128)(2,1)}), bf16[16,136,128]{2,1,0:T(8,128)(2,1)S(1)}, u32[]{:S(2)}, u32[]{:S(2)}) async-start(bf16[16,136,128]{2,1,0:T(8,128)(2,1)} %get-tuple-element.40), calls=%async_computation.2 | async-start | bytes 1114112 | tf_op jit(solution)/shard_map/all_to_all | solution.py:374
  83.2 21.5 %collective-permute-start = (bf16[512,896]{1,0:T(8,128)(2,1)S(1)}, bf16[512,896]{1,0:T(8,128)(2,1)S(1)}, u32[]{:S(2)}, u32[]{:S(2)}) collective-permute-start(bf16[512,896]{1,0:T(8,128)(2,1)S(1)} %pad_maximum_fusion.w0_ref), channel_id=1, source_target_pairs={{0,8},{8,16},{16,24},{24,0},{1,9},{9,17},{17,25},{25,1},{2,10},{10... | collective-permute-start | bytes 2752520 | tf_op jit(solution)/shard_map/ppermute | solution.py:47
  85.4 19.3 %collective-permute-start.2 = (bf16[512,896]{1,0:T(8,128)(2,1)S(1)}, bf16[512,896]{1,0:T(8,128)(2,1)S(1)}, u32[]{:S(2)}, u32[]{:S(2)}) collective-permute-start(bf16[512,896]{1,0:T(8,128)(2,1)S(1)} %pad_maximum_fusion.w0_ref), channel_id=1, source_target_pairs={{0,24},{8,0},{16,8},{24,16},{1,25},{9,1},{17,9},{25,17},{2,26},{10... | collective-permute-start | bytes 2752520 | tf_op jit(solution)/shard_map/ppermute | solution.py:47
  89.7 20.8 %collective-permute-start.1 = (bf16[512,512]{1,0:T(8,128)(2,1)S(1)}, bf16[512,512]{1,0:T(8,128)(2,1)S(1)}, u32[]{:S(2)}, u32[]{:S(2)}) collective-permute-start(bf16[512,512]{1,0:T(8,128)(2,1)S(1)} %slice.14), channel_id=1, source_target_pairs={{0,16},{8,24},{16,0},{24,8},{1,17},{9,25},{17,1},{25,9},{2,18},{10... | collective-permute-start | bytes 1572872 | tf_op jit(solution)/shard_map/ppermute | solution.py:47
  91.7 5.7 %collective-permute-start.3 = (bf16[8,2048]{1,0:T(8,128)(2,1)S(1)}, bf16[8,2048]{1,0:T(8,128)(2,1)S(1)}, u32[]{:S(2)}, u32[]{:S(2)}) collective-permute-start(bf16[8,2048]{1,0:T(8,128)(2,1)S(1)} %copy-done.6), channel_id=1, source_target_pairs={{0,32},{32,64},{64,96},{96,128},{128,160},{160,192},{192,224},{224... | collective-permute-start | bytes 98312 | tf_op jit(solution)/shard_map/ppermute | solution.py:366
  95.0 9.7 %collective-permute-start.4 = (bf16[8,2048]{1,0:T(8,128)(2,1)S(1)}, bf16[8,2048]{1,0:T(8,128)(2,1)S(1)}, u32[]{:S(2)}, u32[]{:S(2)}) collective-permute-start(bf16[8,2048]{1,0:T(8,128)(2,1)S(1)} %copy-done.5), channel_id=1, source_target_pairs={{32,0},{64,32},{96,64},{128,96},{160,128},{192,160},{224,192},{256... | collective-permute-start | bytes 98312 | tf_op jit(solution)/shard_map/ppermute | solution.py:367
  97.4 13.1 %copy-start.7 = (bf16[8,2048]{1,0:T(8,128)(2,1)}, bf16[8,2048]{1,0:T(8,128)(2,1)S(1)}, u32[]{:S(2)}) copy-start(bf16[8,2048]{1,0:T(8,128)(2,1)S(1)} %collective-permute-done.3.lo_ref) | copy-start | bytes 98308
  97.4 21.6 %collective-permute-start.5 = (bf16[512,384]{1,0:T(8,128)(2,1)S(1)}, bf16[512,384]{1,0:T(8,128)(2,1)S(1)}, u32[]{:S(2)}, u32[]{:S(2)}) collective-permute-start(bf16[512,384]{1,0:T(8,128)(2,1)S(1)} %slice.15), channel_id=1, source_target_pairs={{0,16},{8,24},{16,0},{24,8},{1,17},{9,25},{17,1},{25,9},{2,18},{10... | collective-permute-start | bytes 1179656 | tf_op jit(solution)/shard_map/ppermute | solution.py:47
  104.6 5.9 %copy-start.8 = (bf16[8,2048]{1,0:T(8,128)(2,1)}, bf16[8,2048]{1,0:T(8,128)(2,1)S(1)}, u32[]{:S(2)}) copy-start(bf16[8,2048]{1,0:T(8,128)(2,1)S(1)} %collective-permute-done.4.hi_ref) | copy-start | bytes 98308
  104.7 5.9 %copy-start.2 = (bf16[512,896]{1,0:T(8,128)(2,1)}, bf16[512,896]{1,0:T(8,128)(2,1)S(1)}, u32[]{:S(2)}) copy-start(bf16[512,896]{1,0:T(8,128)(2,1)S(1)} %collective-permute-done.w1_ref) | copy-start | bytes 2752516
  104.7 5.9 %copy-start.3 = (bf16[512,896]{1,0:T(8,128)(2,1)}, bf16[512,896]{1,0:T(8,128)(2,1)S(1)}, u32[]{:S(2)}) copy-start(bf16[512,896]{1,0:T(8,128)(2,1)S(1)} %collective-permute-done.2.w3_ref) | copy-start | bytes 2752516
  119.0 0.7 copy-start.4
  123.7 19.6 %collective-permute-start.6 = (bf16[4,32,2048]{2,1,0:T(8,128)(2,1)S(1)}, bf16[4,32,2048]{2,1,0:T(8,128)(2,1)S(1)}, u32[]{:S(2)}, u32[]{:S(2)}) collective-permute-start(bf16[4,32,2048]{2,1,0:T(8,128)(2,1)S(1)} %get-tuple-element.54), channel_id=1, source_target_pairs={{0,1},{1,0},{2,3},{3,2},{4,5},{5,4},{6,7},{7,6},{8,9},{9,8},{10,11... | collective-permute-start | bytes 1572872 | tf_op jit(solution)/shard_map/ppermute | solution.py:405

commit v10 on v9

--- a/solution.py
+++ b/solution.py
@@ -219,7 +219,7 @@
 
 def final_kernel(
     got_ref, mem_ref, nrm_ref, cols_ref, q_ref, o_ref, num_ref, den_ref,
-    gain_ref, pool_ref, w0_ref, w1_ref, w2_ref, w3_ref, keep_ref, give_ref, w_ref,
+    gain_ref, pool_ref, w0_ref, w1_ref, w2_ref, w3_ref, out_ref, w_ref,
 ):
     placed_by_source(lax.axis_index("fs"), (w0_ref, w1_ref, w2_ref, w3_ref), w_ref, 0, 384)
     position = lax.axis_index("sp")
@@ -273,13 +273,7 @@
     memory_out = (scaled * gain_ref[...] * gate).astype(bf16)
     features = jnp.concatenate([pool_ref[...], memory_out], axis=1)
     result = lax.dot_general(features, in_order(w_ref), last, preferred_element_type=f32)
-    core = lax.rem(lax.axis_index("tp"), 2)
-    own = keep_ref.shape[1]
-    for x in range(keep_ref.shape[0]):
-        south = result[2 * x * own : (2 * x + 1) * own]
-        north = result[(2 * x + 1) * own : (2 * x + 2) * own]
-        keep_ref[x] = jnp.where(core == 0, south, north).astype(bf16)
-        give_ref[x] = jnp.where(core == 0, north, south).astype(bf16)
+    out_ref[...] = result.astype(bf16)
 
 
 def sds(shape, dtype):
@@ -290,15 +284,12 @@
     return pltpu.HBM(shape, dtype)
 
 
-def call(kernel, outs, scalars, *args, flops=0, scratch=(), specs=None, close=None):
+def call(kernel, outs, scalars, *args, flops=0, scratch=(), specs=None, close=-1):
     many = isinstance(outs, tuple)
-    grant = None
-    if close is not None:
-        grant = 24 * 2**20
-        args = [
-            pltpu.with_memory_space_constraint(x, pltpu.VMEM if n == close else pltpu.HBM)
-            for n, x in enumerate(args)
-        ]
+    args = [
+        pltpu.with_memory_space_constraint(x, pltpu.VMEM if n == close else pltpu.HBM)
+        for n, x in enumerate(args)
+    ]
     return pl.pallas_call(
         kernel,
         grid=(1,) if specs else (),
@@ -307,7 +298,7 @@
         out_shape=outs,
         scratch_shapes=list(scratch),
         cost_estimate=pl.CostEstimate(flops=flops, bytes_accessed=0, transcendentals=0),
-        compiler_params=pltpu.CompilerParams(vmem_limit_bytes=grant),
+        compiler_params=pltpu.CompilerParams(vmem_limit_bytes=24 * 2**20),
     )(*scalars, *args)
 
 
@@ -343,9 +334,9 @@
     normed, cols, rows, begin, end = call(
         gates_kernel,
         (
-            sds((count, width), bf16),
-            sds((count, 128), f32),
-            sds((8, count), f32),
+            far((count, width), bf16),
+            far((count, 128), f32),
+            far((8, count), f32),
             sds((HALO, width), bf16),
             sds((HALO, width), bf16),
         ),
@@ -367,7 +358,7 @@
     high = lax.ppermute(begin, "sp", [(i + 1, i) for i in range(length - 1)])
     k, v, packets = call(
         state_kernel,
-        (far((count, 128), bf16), far((count, 128), bf16), far((NZ, PACKET, 128), bf16)),
+        (far((count, 128), bf16), far((count, 128), bf16), sds((NZ, PACKET, 128), bf16)),
         (), kv_weight, normed, cols, rows,
         flops=2 * 10**9, close=0,
     )
@@ -390,22 +381,16 @@
         scratch=[pltpu.VMEM((NY, NZ * ROWS, 512), bf16)]
         + [pltpu.VMEM((count + 32, 256), f32)] * 2,
     )
-    cores = 2
-    chips = lax.axis_size("tp") // cores
-    own = count // (chips * cores)
-    keep, give = call(
-        final_kernel, (sds((chips, own, width), bf16),) * 2, (),
+    own = count // lax.axis_size("tp")
+    partial = call(
+        final_kernel, sds((count, width), bf16), (),
         got, init_memory[0, :, 0], init_normalizer[0, :, 0][:, None], cols, q, outgate,
         nums, dens, head_gain, pool_out,
         first_rest, first_from[1], last_two, first_from[3],
         flops=2 * 10**9, close=0, specs=[vmem] * 10 + [first_columns] * 4,
         scratch=[pltpu.VMEM((NY, NZ * ROWS, 384), bf16)],
     )
-    swap = [(i, i ^ 1) for i in range(chips * cores)]
-    taken = lax.ppermute(give, "tp", swap)
-    pairs = (keep.astype(f32) + taken.astype(f32)).astype(bf16)
-    groups = [list(range(c, chips * cores, cores)) for c in range(cores)]
-    parts = lax.all_to_all(pairs, "tp", 0, 0, axis_index_groups=groups, tiled=True)
+    parts = lax.all_to_all(partial.reshape(-1, own, width), "tp", 0, 0, tiled=True)
     mixed = jnp.sum(parts.astype(f32), axis=0).astype(bf16)
     return mixed.reshape(1, own, width)
 

time: 158 us -> 161 us (1.019)
  blocking collectives: 50.3 us -> 73.1 us
  starting transfers between devices: 65.1 us -> 46.9 us
  waiting for transfers between devices: 21.8 us -> 19.6 us
    all_to_all x1, blocking collectives: 12.4 us -> 35.2 us  [per_device(): lax.all_to_all(partial.reshape(-1, own, width), 'tp', 0, 0, tiled=True)]
    ppermute x1 -> x0, starting transfers between devices: 18.1 us -> none  [per_device(): taken = lax.ppermute(give, 'tp', swap)]
  transfers between devices with their start and end apart: 10 -> 9, of which waited for: 6 -> 5; matrix products, arithmetic and copies ran while one was open for 0% -> 0% of each run, Pallas kernels for 5% -> 5%
where the time goes in v10:
time: 161 us; the launch traced here: 160 us
  blocking collectives  73.1 us (45%)
  starting transfers between devices  46.9 us (29%)
  waiting for transfers between devices  19.6 us (12%)
  Pallas kernels  16.3 us (10%)
  local copies, waits for them, and re-layouts  2.66 us (2%)
    all_gather x1, blocking collectives, per_device(): along_z = lax.all_gather(packed, 'sp', axis=0, tiled=True)  37.9 us
    all_to_all x1, blocking collectives, per_device(): lax.all_to_all(partial.reshape(-1, own, width), 'tp', 0, 0, tiled=True)  35.2 us
    pallas_call x5, Pallas kernels, call(): pl.pallas_call(kernel, grid=(1,) if specs else (), in_specs=specs or [sme...  16.3 us
    all_to_all x1, starting transfers between devices, per_device(): lax.all_to_all(pool_copies, 'sp', 0, 0, tiled=True).reshape(NZ * ROWS, 256)  15.7 us
    ppermute x4, starting transfers between devices, from_shift(): lax.ppermute(x, axis, [(i, (i + shift) % count) for i in range(count)])  12.8 us
    ppermute x4, waiting for transfers between devices, from_shift(): lax.ppermute(x, axis, [(i, (i + shift) % count) for i in range(count)])  9.99 us
    all_to_all x1, starting transfers between devices, per_device(): got = lax.all_to_all(packets, 'sp', 0, 0, tiled=True)  9.59 us
    all_to_all x1, waiting for transfers between devices, from_everyone(): return lax.all_to_all(copies, axis, split_axis=0, concat_axis=0, tiled=True)  5.66 us
  transfers between devices with their start and end apart: 9, of which 5 were waited for; matrix products, arithmetic and copies ran while one was open for 0% of the time, Pallas kernels for 5%

profile of v10, /device:TPU:1, one launch (start us, length us, event | category | flops | bytes accessed | tf_op | source)
XLA Modules:
  0.0 159.6 jit_solution(12023679016704352330)
XLA Ops:
  0.0 1.5 shard_map.145
  1.5 15.7 %all-to-all-start = ((bf16[16,32,256]{2,1,0:T(8,128)(2,1)}), bf16[16,32,256]{2,1,0:T(8,128)(2,1)S(1)}, u32[]{:S(2)}, u32[]{:S(2)}) async-start(bf16[16,32,256]{2,1,0:T(8,128)(2,1)} %get-tuple-element.29), calls=%async_computation | async-start | bytes 524288 | tf_op jit(solution)/shard_map/all_to_all | solution.py:329
  17.3 37.9 %all_gather.3 = bf16[512,896]{1,0:T(8,128)(2,1)S(1)} all-gather(bf16[32,896]{1,0:T(8,128)(2,1)S(1)} %get-tuple-element.28), channel_id=1, replica_groups=mesh['sp'=16,'fs'=4,'tp'=8] {'sp'}, dimensions={0}, use_global_device_ids=true | all-gather | bytes 974848 | tf_op jit(solution)/shard_map/all_gather | solution.py:330
  55.2 0.0 copy-start.2
  55.2 0.0 all-to-all-done
  55.2 1.1 broadcast_in_dim.7
  56.4 4.2 %all-to-all-start.1 = ((bf16[4,512,256]{2,1,0:T(8,128)(2,1)}), bf16[4,512,256]{2,1,0:T(8,128)(2,1)S(1)}, u32[]{:S(2)}, u32[]{:S(2)}) async-start(bf16[4,512,256]{2,1,0:T(8,128)(2,1)} %broadcast_in_dim.7), calls=%async_computation.1 | async-start | bytes 2097152 | tf_op jit(solution)/shard_map/all_to_all | solution.py:26
  60.5 0.0 copy-start
  60.5 0.0 copy-done.2
  60.6 0.7 copy-done
  61.2 0.0 slice-start
  61.2 3.3 %shard_map.146 = (bf16[256,2048]{1,0:T(8,128)(2,1)}, f32[256,128]{1,0:T(8,128)}, f32[8,256]{1,0:T(8,128)}, bf16[8,2048]{1,0:T(8,128)(2,1)S(1)}, bf16[8,2048]{1,0:T(8,128)(2,1)S(1)}) custom-call(f32[4]{0:T(128)S(1)} %bitcast.11, bf16[256,2048]{1,0:T(8,128)(2,1)} %bitcast.13, f32[1,2048]{1,0:T(1,128)} %bitcast.16, bf16[4,2048]{1,0:T(4,128)(2,1)} %bitcast.15, ...), custom_call_target="tpu_custom_call" | custom-call | flops 4000000000 | tf_op jit(solution)/shard_map/pallas_call | solution.py:293
  64.5 0.0 slice-done
  64.5 0.1 pad_maximum_fusion.w0_ref
  64.6 0.0 copy-start.1
  64.6 5.7 %all-to-all-done.1.w_ref = bf16[4,512,256]{2,1,0:T(8,128)(2,1)S(1)} async-done(((bf16[4,512,256]{2,1,0:T(8,128)(2,1)}), bf16[4,512,256]{2,1,0:T(8,128)(2,1)S(1)}, u32[]{:S(2)}, u32[]{:S(2)}) %all-to-all-start.1) | async-done | bytes 1048608 | tf_op jit(solution)/shard_map/all_to_all | solution.py:26
  70.3 3.2 %shard_map.147 = (bf16[256,128]{1,0:T(8,128)(2,1)}, bf16[256,128]{1,0:T(8,128)(2,1)}, bf16[16,136,128]{2,1,0:T(8,128)(2,1)}) custom-call(bf16[4,512,256]{2,1,0:T(8,128)(2,1)S(1)} %all-to-all-done.1.w_ref, bf16[256,2048]{1,0:T(8,128)(2,1)} %get-tuple-element.32.normed_ref, f32[256,128]{1,0:T(8,128)} %get-tuple-element.33.cols_ref, ...), custom_call_target="tpu_custom_call" | custom-call | flops 2000000000 | tf_op jit(solution)/shard_map/pallas_call | solution.py:293
  73.4 9.6 %all-to-all-start.2 = ((bf16[16,136,128]{2,1,0:T(8,128)(2,1)}), bf16[16,136,128]{2,1,0:T(8,128)(2,1)S(1)}, u32[]{:S(2)}, u32[]{:S(2)}) async-start(bf16[16,136,128]{2,1,0:T(8,128)(2,1)} %get-tuple-element.38), calls=%async_computation.2 | async-start | bytes 1114112 | tf_op jit(solution)/shard_map/all_to_all | solution.py:365
  83.0 2.2 %collective-permute-start = (bf16[512,896]{1,0:T(8,128)(2,1)S(1)}, bf16[512,896]{1,0:T(8,128)(2,1)S(1)}, u32[]{:S(2)}, u32[]{:S(2)}) collective-permute-start(bf16[512,896]{1,0:T(8,128)(2,1)S(1)} %pad_maximum_fusion.w0_ref), channel_id=1, source_target_pairs={{0,8},{8,16},{16,24},{24,0},{1,9},{9,17},{17,25},{25,1},{2,10},{10... | collective-permute-start | bytes 2752520 | tf_op jit(solution)/shard_map/ppermute | solution.py:47
  85.2 4.3 %collective-permute-start.2 = (bf16[512,896]{1,0:T(8,128)(2,1)S(1)}, bf16[512,896]{1,0:T(8,128)(2,1)S(1)}, u32[]{:S(2)}, u32[]{:S(2)}) collective-permute-start(bf16[512,896]{1,0:T(8,128)(2,1)S(1)} %pad_maximum_fusion.w0_ref), channel_id=1, source_target_pairs={{0,24},{8,0},{16,8},{24,16},{1,25},{9,1},{17,9},{25,17},{2,26},{10... | collective-permute-start | bytes 2752520 | tf_op jit(solution)/shard_map/ppermute | solution.py:47
  89.6 1.9 %collective-permute-start.1 = (bf16[512,512]{1,0:T(8,128)(2,1)S(1)}, bf16[512,512]{1,0:T(8,128)(2,1)S(1)}, u32[]{:S(2)}, u32[]{:S(2)}) collective-permute-start(bf16[512,512]{1,0:T(8,128)(2,1)S(1)} %slice.14), channel_id=1, source_target_pairs={{0,16},{8,24},{16,0},{24,8},{1,17},{9,25},{17,1},{25,9},{2,18},{10... | collective-permute-start | bytes 1572872 | tf_op jit(solution)/shard_map/ppermute | solution.py:47
  91.5 3.3 %collective-permute-start.3 = (bf16[8,2048]{1,0:T(8,128)(2,1)S(1)}, bf16[8,2048]{1,0:T(8,128)(2,1)S(1)}, u32[]{:S(2)}, u32[]{:S(2)}) collective-permute-start(bf16[8,2048]{1,0:T(8,128)(2,1)S(1)} %get-tuple-element.42), channel_id=1, source_target_pairs={{0,32},{32,64},{64,96},{96,128},{128,160},{160,192},{192,224},{224... | collective-permute-start | bytes 98312 | tf_op jit(solution)/shard_map/ppermute | solution.py:357
  94.8 1.3 collective-permute-start.4
  96.1 0.0 copy-done.1
  96.2 1.1 collective-permute-done.3.lo_ref
  97.2 0.0 copy-start.6
  97.2 4.4 %collective-permute-start.5 = (bf16[512,384]{1,0:T(8,128)(2,1)S(1)}, bf16[512,384]{1,0:T(8,128)(2,1)S(1)}, u32[]{:S(2)}, u32[]{:S(2)}) collective-permute-start(bf16[512,384]{1,0:T(8,128)(2,1)S(1)} %slice.15), channel_id=1, source_target_pairs={{0,16},{8,24},{16,0},{24,8},{1,17},{9,25},{17,1},{25,9},{2,18},{10... | collective-permute-start | bytes 1179656 | tf_op jit(solution)/shard_map/ppermute | solution.py:47
  101.7 2.8 %collective-permute-done.4.hi_ref = bf16[8,2048]{1,0:T(8,128)(2,1)S(1)} collective-permute-done((bf16[8,2048]{1,0:T(8,128)(2,1)S(1)}, bf16[8,2048]{1,0:T(8,128)(2,1)S(1)}, u32[]{:S(2)}, u32[]{:S(2)}) %collective-permute-start.4) | collective-permute-done | bytes 32800 | tf_op jit(solution)/shard_map/ppermute | solution.py:358
  104.5 0.0 copy-start.7
  104.5 0.0 collective-permute-done.w1_ref
  104.5 0.0 copy-start.3
  104.5 0.0 collective-permute-done.2.w3_ref
  104.5 0.0 copy-start.4
  104.5 5.8 %collective-permute-done.1.w2_ref = bf16[512,512]{1,0:T(8,128)(2,1)S(1)} collective-permute-done((bf16[512,512]{1,0:T(8,128)(2,1)S(1)}, bf16[512,512]{1,0:T(8,128)(2,1)S(1)}, u32[]{:S(2)}, u32[]{:S(2)}) %collective-permute-start.1) | collective-permute-done | bytes 524320 | tf_op jit(solution)/shard_map/ppermute | solution.py:47
  110.4 0.0 copy-done.6
  110.4 0.0 copy-done.7
  110.4 0.0 copy-done.3
  110.4 0.0 copy-done.4
  110.4 4.3 %shard_map.148 = (bf16[256,128]{1,0:T(8,128)(2,1)}, bf16[256,128]{1,0:T(8,128)(2,1)}, bf16[256,256]{1,0:T(8,128)(2,1)}, f32[2,256,128]{2,1,0:T(8,128)}, f32[256,128]{1,0:T(8,128)}) custom-call(bf16[512,896]{1,0:T(8,128)(2,1)} %copy-done.1, bf16[512,896]{1,0:T(8,128)(2,1)} %copy-done.3, bf16[512,512]{1,0:T(8,128)(2,1)S(1)} %collective-permute-done.1.w2_ref, ...), custom_call_target="tpu_custom_call" | custom-call | flops 5000000000 | tf_op jit(solution)/shard_map/pallas_call | solution.py:293
  114.7 4.1 %collective-permute-done.5.w2_ref = bf16[512,384]{1,0:T(8,128)(2,1)S(1)} collective-permute-done((bf16[512,384]{1,0:T(8,128)(2,1)S(1)}, bf16[512,384]{1,0:T(8,128)(2,1)S(1)}, u32[]{:S(2)}, u32[]{:S(2)}) %collective-permute-start.5) | collective-permute-done | bytes 393248 | tf_op jit(solution)/shard_map/ppermute | solution.py:47
  118.8 0.0 copy-start.5
  118.8 0.0 all-to-all-done.2.got_ref
  118.8 0.7 copy-done.5
  119.6 4.0 %shard_map.149 = bf16[256,2048]{1,0:T(8,128)(2,1)S(1)} custom-call(bf16[16,136,128]{2,1,0:T(8,128)(2,1)S(1)} %all-to-all-done.2.got_ref, f32[2,128,128]{2,1,0:T(8,128)} %bitcast.14, f32[2,1,128]{2,1,0:T(1,128)} %bitcast.19, f32[256,128]{1,0:T(8,128)} %get-tuple-element.33.cols_ref, bf16[256,128]{1,0:T(8,128)(2,1)} %get-tuple-element.46.q_ref, ...), custom_call_target="tpu_custom_call" | custom-call | flops 2000000000 | tf_op jit(solution)/shard_map/pallas_call | solution.py:293
  123.5 35.2 %all_to_all.20 = bf16[8,32,2048]{2,1,0:T(8,128)(2,1)S(1)} all-to-all(bf16[8,32,2048]{2,1,0:T(8,128)(2,1)S(1)} %bitcast.10), channel_id=1, replica_groups=mesh['sp'=16,'fs'=4,'tp'=8] {'tp'}, dimensions={0} | all-to-all | bytes 2097152 | tf_op jit(solution)/shard_map/all_to_all | solution.py:393
  158.8 0.8 reduce_sum.12
  (3 shorter events, 0.1 us)
Async XLA Ops:
  1.5 53.7 %all-to-all-start = ((bf16[16,32,256]{2,1,0:T(8,128)(2,1)}), bf16[16,32,256]{2,1,0:T(8,128)(2,1)S(1)}, u32[]{:S(2)}, u32[]{:S(2)}) async-start(bf16[16,32,256]{2,1,0:T(8,128)(2,1)} %get-tuple-element.29), calls=%async_computation | async-start | bytes 524288 | tf_op jit(solution)/shard_map/all_to_all | solution.py:329
  55.2 5.4 %copy-start.2 = (bf16[512,896]{1,0:T(8,128)(2,1)}, bf16[512,896]{1,0:T(8,128)(2,1)S(1)}, u32[]{:S(2)}) copy-start(bf16[512,896]{1,0:T(8,128)(2,1)S(1)} %all_gather.3) | copy-start | bytes 2752516
  56.4 13.9 %all-to-all-start.1 = ((bf16[4,512,256]{2,1,0:T(8,128)(2,1)}), bf16[4,512,256]{2,1,0:T(8,128)(2,1)S(1)}, u32[]{:S(2)}, u32[]{:S(2)}) async-start(bf16[4,512,256]{2,1,0:T(8,128)(2,1)} %broadcast_in_dim.7), calls=%async_computation.1 | async-start | bytes 2097152 | tf_op jit(solution)/shard_map/all_to_all | solution.py:26
  60.5 0.7 copy-start
  61.2 3.3 %slice-start = ((bf16[512,896]{1,0:T(8,128)(2,1)}), bf16[512,640]{1,0:T(8,128)(2,1)S(1)}, s32[]{:S(2)}) async-start(bf16[512,896]{1,0:T(8,128)(2,1)} %copy-done.2), calls=%async_computation.4 | async-start | bytes 1310720 | tf_op jit(solution)/shard_map/slice | solution.py:351
  64.6 31.5 %copy-start.1 = (bf16[512,896]{1,0:T(8,128)(2,1)}, bf16[512,896]{1,0:T(8,128)(2,1)S(1)}, u32[]{:S(2)}) copy-start(bf16[512,896]{1,0:T(8,128)(2,1)S(1)} %pad_maximum_fusion.w0_ref) | copy-start | bytes 2752516
  73.4 45.4 %all-to-all-start.2 = ((bf16[16,136,128]{2,1,0:T(8,128)(2,1)}), bf16[16,136,128]{2,1,0:T(8,128)(2,1)S(1)}, u32[]{:S(2)}, u32[]{:S(2)}) async-start(bf16[16,136,128]{2,1,0:T(8,128)(2,1)} %get-tuple-element.38), calls=%async_computation.2 | async-start | bytes 1114112 | tf_op jit(solution)/shard_map/all_to_all | solution.py:365
  83.0 21.5 %collective-permute-start = (bf16[512,896]{1,0:T(8,128)(2,1)S(1)}, bf16[512,896]{1,0:T(8,128)(2,1)S(1)}, u32[]{:S(2)}, u32[]{:S(2)}) collective-permute-start(bf16[512,896]{1,0:T(8,128)(2,1)S(1)} %pad_maximum_fusion.w0_ref), channel_id=1, source_target_pairs={{0,8},{8,16},{16,24},{24,0},{1,9},{9,17},{17,25},{25,1},{2,10},{10... | collective-permute-start | bytes 2752520 | tf_op jit(solution)/shard_map/ppermute | solution.py:47
  85.2 19.3 %collective-permute-start.2 = (bf16[512,896]{1,0:T(8,128)(2,1)S(1)}, bf16[512,896]{1,0:T(8,128)(2,1)S(1)}, u32[]{:S(2)}, u32[]{:S(2)}) collective-permute-start(bf16[512,896]{1,0:T(8,128)(2,1)S(1)} %pad_maximum_fusion.w0_ref), channel_id=1, source_target_pairs={{0,24},{8,0},{16,8},{24,16},{1,25},{9,1},{17,9},{25,17},{2,26},{10... | collective-permute-start | bytes 2752520 | tf_op jit(solution)/shard_map/ppermute | solution.py:47
  89.6 20.8 %collective-permute-start.1 = (bf16[512,512]{1,0:T(8,128)(2,1)S(1)}, bf16[512,512]{1,0:T(8,128)(2,1)S(1)}, u32[]{:S(2)}, u32[]{:S(2)}) collective-permute-start(bf16[512,512]{1,0:T(8,128)(2,1)S(1)} %slice.14), channel_id=1, source_target_pairs={{0,16},{8,24},{16,0},{24,8},{1,17},{9,25},{17,1},{25,9},{2,18},{10... | collective-permute-start | bytes 1572872 | tf_op jit(solution)/shard_map/ppermute | solution.py:47
  91.5 5.7 %collective-permute-start.3 = (bf16[8,2048]{1,0:T(8,128)(2,1)S(1)}, bf16[8,2048]{1,0:T(8,128)(2,1)S(1)}, u32[]{:S(2)}, u32[]{:S(2)}) collective-permute-start(bf16[8,2048]{1,0:T(8,128)(2,1)S(1)} %get-tuple-element.42), channel_id=1, source_target_pairs={{0,32},{32,64},{64,96},{96,128},{128,160},{160,192},{192,224},{224... | collective-permute-start | bytes 98312 | tf_op jit(solution)/shard_map/ppermute | solution.py:357
  94.8 9.7 %collective-permute-start.4 = (bf16[8,2048]{1,0:T(8,128)(2,1)S(1)}, bf16[8,2048]{1,0:T(8,128)(2,1)S(1)}, u32[]{:S(2)}, u32[]{:S(2)}) collective-permute-start(bf16[8,2048]{1,0:T(8,128)(2,1)S(1)} %get-tuple-element.43), channel_id=1, source_target_pairs={{32,0},{64,32},{96,64},{128,96},{160,128},{192,160},{224,192},{256... | collective-permute-start | bytes 98312 | tf_op jit(solution)/shard_map/ppermute | solution.py:358
  97.2 13.1 %copy-start.6 = (bf16[8,2048]{1,0:T(8,128)(2,1)}, bf16[8,2048]{1,0:T(8,128)(2,1)S(1)}, u32[]{:S(2)}) copy-start(bf16[8,2048]{1,0:T(8,128)(2,1)S(1)} %collective-permute-done.3.lo_ref) | copy-start | bytes 98308
  97.2 21.6 %collective-permute-start.5 = (bf16[512,384]{1,0:T(8,128)(2,1)S(1)}, bf16[512,384]{1,0:T(8,128)(2,1)S(1)}, u32[]{:S(2)}, u32[]{:S(2)}) collective-permute-start(bf16[512,384]{1,0:T(8,128)(2,1)S(1)} %slice.15), channel_id=1, source_target_pairs={{0,16},{8,24},{16,0},{24,8},{1,17},{9,25},{17,1},{25,9},{2,18},{10... | collective-permute-start | bytes 1179656 | tf_op jit(solution)/shard_map/ppermute | solution.py:47
  104.5 5.9 %copy-start.7 = (bf16[8,2048]{1,0:T(8,128)(2,1)}, bf16[8,2048]{1,0:T(8,128)(2,1)S(1)}, u32[]{:S(2)}) copy-start(bf16[8,2048]{1,0:T(8,128)(2,1)S(1)} %collective-permute-done.4.hi_ref) | copy-start | bytes 98308
  104.5 5.9 %copy-start.3 = (bf16[512,896]{1,0:T(8,128)(2,1)}, bf16[512,896]{1,0:T(8,128)(2,1)S(1)}, u32[]{:S(2)}) copy-start(bf16[512,896]{1,0:T(8,128)(2,1)S(1)} %collective-permute-done.w1_ref) | copy-start | bytes 2752516
  104.5 5.9 %copy-start.4 = (bf16[512,896]{1,0:T(8,128)(2,1)}, bf16[512,896]{1,0:T(8,128)(2,1)S(1)}, u32[]{:S(2)}) copy-start(bf16[512,896]{1,0:T(8,128)(2,1)S(1)} %collective-permute-done.2.w3_ref) | copy-start | bytes 2752516
  118.8 0.7 copy-start.5

commit v11 on v9

--- a/solution.py
+++ b/solution.py
@@ -290,15 +290,12 @@
     return pltpu.HBM(shape, dtype)
 
 
-def call(kernel, outs, scalars, *args, flops=0, scratch=(), specs=None, close=None):
+def call(kernel, outs, scalars, *args, flops=0, scratch=(), specs=None, close=-1):
     many = isinstance(outs, tuple)
-    grant = None
-    if close is not None:
-        grant = 24 * 2**20
-        args = [
-            pltpu.with_memory_space_constraint(x, pltpu.VMEM if n == close else pltpu.HBM)
-            for n, x in enumerate(args)
-        ]
+    args = [
+        pltpu.with_memory_space_constraint(x, pltpu.VMEM if n == close else pltpu.HBM)
+        for n, x in enumerate(args)
+    ]
     return pl.pallas_call(
         kernel,
         grid=(1,) if specs else (),
@@ -307,7 +304,7 @@
         out_shape=outs,
         scratch_shapes=list(scratch),
         cost_estimate=pl.CostEstimate(flops=flops, bytes_accessed=0, transcendentals=0),
-        compiler_params=pltpu.CompilerParams(vmem_limit_bytes=grant),
+        compiler_params=pltpu.CompilerParams(vmem_limit_bytes=24 * 2**20),
     )(*scalars, *args)
 
 
@@ -336,16 +333,13 @@
         flops=10**6,
     )
     pool_z = lax.all_to_all(pool_copies, "sp", 0, 0, tiled=True).reshape(NZ * ROWS, 256)
-    along_z = lax.all_gather(packed, "sp", axis=0, tiled=True)
-    kv_z, pool_z = lax.optimization_barrier((along_z[:, :256], pool_z))
-    kv_weight = from_everyone(kv_z, "fs")
-    own_tokens, along_z = lax.optimization_barrier((tokens[0], along_z))
+    own_tokens, packed = lax.optimization_barrier((tokens[0], packed))
     normed, cols, rows, begin, end = call(
         gates_kernel,
         (
-            sds((count, width), bf16),
-            sds((count, 128), f32),
-            sds((8, count), f32),
+            far((count, width), bf16),
+            far((count, 128), f32),
+            far((8, count), f32),
             sds((HALO, width), bf16),
             sds((HALO, width), bf16),
         ),
@@ -356,6 +350,10 @@
         decay_extra[0, :, 0][:, None],
         flops=4 * 10**9,
     )
+    packed, normed = lax.optimization_barrier((packed, normed))
+    along_z = lax.all_gather(packed, "sp", axis=0, tiled=True)
+    kv_z, pool_z = lax.optimization_barrier((along_z[:, :256], pool_z))
+    kv_weight = from_everyone(kv_z, "fs")
     first_rest, rows = lax.optimization_barrier(
         (jnp.concatenate([pool_z, along_z[:, 256:]], axis=1), rows)
     )
@@ -367,7 +365,7 @@
     high = lax.ppermute(begin, "sp", [(i + 1, i) for i in range(length - 1)])
     k, v, packets = call(
         state_kernel,
-        (far((count, 128), bf16), far((count, 128), bf16), far((NZ, PACKET, 128), bf16)),
+        (far((count, 128), bf16), far((count, 128), bf16), sds((NZ, PACKET, 128), bf16)),
         (), kv_weight, normed, cols, rows,
         flops=2 * 10**9, close=0,
     )

time: 158 us -> 158 us (level)
  blocking collectives: 50.3 us -> 46.1 us
  waiting for transfers between devices: 21.8 us -> 25 us
    all_gather x1, blocking collectives: 37.9 us -> 33.7 us  [per_device(): along_z = lax.all_gather(packed, 'sp', axis=0, tiled=True)]
    all_to_all x1, waiting for transfers between devices: 6.31 us -> 9.59 us  [from_everyone(): return lax.all_to_all(copies, axis, split_axis=0, concat_axis=0, tiled=True)]
where the time goes in v11:
time: 158 us; the launch traced here: 156 us
  starting transfers between devices  65.3 us (41%)
  blocking collectives  46.1 us (29%)
  waiting for transfers between devices  25 us (16%)
  Pallas kernels  16.2 us (10%)
  local copies, waits for them, and re-layouts  2.61 us (2%)
    all_gather x1, blocking collectives, per_device(): along_z = lax.all_gather(packed, 'sp', axis=0, tiled=True)  33.7 us
    ppermute x1, starting transfers between devices, per_device(): taken = lax.ppermute(give, 'tp', swap)  18.1 us
    pallas_call x5, Pallas kernels, call(): pl.pallas_call(kernel, grid=(1,) if specs else (), in_specs=specs or [sme...  16.2 us
    all_to_all x1, starting transfers between devices, per_device(): lax.all_to_all(pool_copies, 'sp', 0, 0, tiled=True).reshape(NZ * ROWS, 256)  15.7 us
    ppermute x4, starting transfers between devices, from_shift(): lax.ppermute(x, axis, [(i, (i + shift) % count) for i in range(count)])  12.8 us
    all_to_all x1, blocking collectives, per_device(): lax.all_to_all(pairs, 'tp', 0, 0, axis_index_groups=groups, tiled=True)  12.4 us
    ppermute x4, waiting for transfers between devices, from_shift(): lax.ppermute(x, axis, [(i, (i + shift) % count) for i in range(count)])  9.98 us
    all_to_all x1, starting transfers between devices, per_device(): got = lax.all_to_all(packets, 'sp', 0, 0, tiled=True)  9.89 us
  transfers between devices with their start and end apart: 10, of which 6 were waited for; matrix products, arithmetic and copies ran while one was open for 0% of the time, Pallas kernels for 5%

profile of v11, /device:TPU:1, one launch (start us, length us, event | category | flops | bytes accessed | tf_op | source)
XLA Modules:
  0.0 156.4 jit_solution(15077144016096369649)
XLA Ops:
  0.0 1.5 shard_map.145
  1.5 15.7 %all-to-all-start = ((bf16[16,32,256]{2,1,0:T(8,128)(2,1)}), bf16[16,32,256]{2,1,0:T(8,128)(2,1)S(1)}, u32[]{:S(2)}, u32[]{:S(2)}) async-start(bf16[16,32,256]{2,1,0:T(8,128)(2,1)} %get-tuple-element.37), calls=%async_computation | async-start | bytes 524288 | tf_op jit(solution)/shard_map/all_to_all | solution.py:335
  17.3 0.0 copy-start
  17.3 0.6 copy-done
  17.9 3.3 %shard_map.146 = (bf16[256,2048]{1,0:T(8,128)(2,1)}, f32[256,128]{1,0:T(8,128)}, f32[8,256]{1,0:T(8,128)}, bf16[8,2048]{1,0:T(8,128)(2,1)S(1)}, bf16[8,2048]{1,0:T(8,128)(2,1)S(1)}) custom-call(f32[4]{0:T(128)S(1)} %bitcast.9, bf16[256,2048]{1,0:T(8,128)(2,1)} %bitcast.11, f32[1,2048]{1,0:T(1,128)} %bitcast.14, bf16[4,2048]{1,0:T(4,128)(2,1)} %bitcast.13, ...), custom_call_target="tpu_custom_call" | custom-call | flops 4000000000 | tf_op jit(solution)/shard_map/pallas_call | solution.py:299
  21.2 33.7 %all_gather.3 = bf16[512,896]{1,0:T(8,128)(2,1)S(1)} all-gather(bf16[32,896]{1,0:T(8,128)(2,1)S(1)} %get-tuple-element.36), channel_id=1, replica_groups=mesh['sp'=16,'fs'=4,'tp'=8] {'sp'}, dimensions={0}, use_global_device_ids=true | all-gather | bytes 974848 | tf_op jit(solution)/shard_map/all_gather | solution.py:354
  54.9 0.0 all-to-all-done
  54.9 1.0 broadcast_in_dim.8
  56.0 4.2 %all-to-all-start.1 = ((bf16[4,512,256]{2,1,0:T(8,128)(2,1)}), bf16[4,512,256]{2,1,0:T(8,128)(2,1)S(1)}, u32[]{:S(2)}, u32[]{:S(2)}) async-start(bf16[4,512,256]{2,1,0:T(8,128)(2,1)} %broadcast_in_dim.8), calls=%async_computation.1 | async-start | bytes 2097152 | tf_op jit(solution)/shard_map/all_to_all | solution.py:26
  60.1 0.1 slice.17
  60.2 0.1 pad_maximum_fusion.w0_ref
  60.3 0.0 copy-start.1
  60.3 9.6 %all-to-all-done.1.w_ref = bf16[4,512,256]{2,1,0:T(8,128)(2,1)S(1)} async-done(((bf16[4,512,256]{2,1,0:T(8,128)(2,1)}), bf16[4,512,256]{2,1,0:T(8,128)(2,1)S(1)}, u32[]{:S(2)}, u32[]{:S(2)}) %all-to-all-start.1) | async-done | bytes 1048608 | tf_op jit(solution)/shard_map/all_to_all | solution.py:26
  69.9 3.1 %shard_map.147 = (bf16[256,128]{1,0:T(8,128)(2,1)}, bf16[256,128]{1,0:T(8,128)(2,1)}, bf16[16,136,128]{2,1,0:T(8,128)(2,1)}) custom-call(bf16[4,512,256]{2,1,0:T(8,128)(2,1)S(1)} %all-to-all-done.1.w_ref, bf16[256,2048]{1,0:T(8,128)(2,1)} %get-tuple-element.39.normed_ref, f32[256,128]{1,0:T(8,128)} %get-tuple-element.40.cols_ref, ...), custom_call_target="tpu_custom_call" | custom-call | flops 2000000000 | tf_op jit(solution)/shard_map/pallas_call | solution.py:299
  73.0 9.9 %all-to-all-start.2 = ((bf16[16,136,128]{2,1,0:T(8,128)(2,1)}), bf16[16,136,128]{2,1,0:T(8,128)(2,1)S(1)}, u32[]{:S(2)}, u32[]{:S(2)}) async-start(bf16[16,136,128]{2,1,0:T(8,128)(2,1)} %get-tuple-element.44), calls=%async_computation.2 | async-start | bytes 1114112 | tf_op jit(solution)/shard_map/all_to_all | solution.py:372
  82.9 2.2 %collective-permute-start = (bf16[512,896]{1,0:T(8,128)(2,1)S(1)}, bf16[512,896]{1,0:T(8,128)(2,1)S(1)}, u32[]{:S(2)}, u32[]{:S(2)}) collective-permute-start(bf16[512,896]{1,0:T(8,128)(2,1)S(1)} %pad_maximum_fusion.w0_ref), channel_id=1, source_target_pairs={{0,8},{8,16},{16,24},{24,0},{1,9},{9,17},{17,25},{25,1},{2,10},{10... | collective-permute-start | bytes 2752520 | tf_op jit(solution)/shard_map/ppermute | solution.py:47
  85.1 4.3 %collective-permute-start.2 = (bf16[512,896]{1,0:T(8,128)(2,1)S(1)}, bf16[512,896]{1,0:T(8,128)(2,1)S(1)}, u32[]{:S(2)}, u32[]{:S(2)}) collective-permute-start(bf16[512,896]{1,0:T(8,128)(2,1)S(1)} %pad_maximum_fusion.w0_ref), channel_id=1, source_target_pairs={{0,24},{8,0},{16,8},{24,16},{1,25},{9,1},{17,9},{25,17},{2,26},{10... | collective-permute-start | bytes 2752520 | tf_op jit(solution)/shard_map/ppermute | solution.py:47
  89.5 1.9 %collective-permute-start.1 = (bf16[512,512]{1,0:T(8,128)(2,1)S(1)}, bf16[512,512]{1,0:T(8,128)(2,1)S(1)}, u32[]{:S(2)}, u32[]{:S(2)}) collective-permute-start(bf16[512,512]{1,0:T(8,128)(2,1)S(1)} %slice.14), channel_id=1, source_target_pairs={{0,16},{8,24},{16,0},{24,8},{1,17},{9,25},{17,1},{25,9},{2,18},{10... | collective-permute-start | bytes 1572872 | tf_op jit(solution)/shard_map/ppermute | solution.py:47
  91.4 3.3 %collective-permute-start.3 = (bf16[8,2048]{1,0:T(8,128)(2,1)S(1)}, bf16[8,2048]{1,0:T(8,128)(2,1)S(1)}, u32[]{:S(2)}, u32[]{:S(2)}) collective-permute-start(bf16[8,2048]{1,0:T(8,128)(2,1)S(1)} %get-tuple-element.48), channel_id=1, source_target_pairs={{0,32},{32,64},{64,96},{96,128},{128,160},{160,192},{192,224},{224... | collective-permute-start | bytes 98312 | tf_op jit(solution)/shard_map/ppermute | solution.py:364
  94.7 1.3 collective-permute-start.4
  96.0 0.0 copy-done.1
  96.0 1.1 collective-permute-done.3.lo_ref
  97.1 0.0 copy-start.5
  97.1 4.4 %collective-permute-start.5 = (bf16[512,384]{1,0:T(8,128)(2,1)S(1)}, bf16[512,384]{1,0:T(8,128)(2,1)S(1)}, u32[]{:S(2)}, u32[]{:S(2)}) collective-permute-start(bf16[512,384]{1,0:T(8,128)(2,1)S(1)} %slice.15), channel_id=1, source_target_pairs={{0,16},{8,24},{16,0},{24,8},{1,17},{9,25},{17,1},{25,9},{2,18},{10... | collective-permute-start | bytes 1179656 | tf_op jit(solution)/shard_map/ppermute | solution.py:47
  101.5 2.8 %collective-permute-done.4.hi_ref = bf16[8,2048]{1,0:T(8,128)(2,1)S(1)} collective-permute-done((bf16[8,2048]{1,0:T(8,128)(2,1)S(1)}, bf16[8,2048]{1,0:T(8,128)(2,1)S(1)}, u32[]{:S(2)}, u32[]{:S(2)}) %collective-permute-start.4) | collective-permute-done | bytes 32800 | tf_op jit(solution)/shard_map/ppermute | solution.py:365
  104.4 0.0 copy-start.6
  104.4 0.0 collective-permute-done.w1_ref
  104.4 0.0 copy-start.2
  104.4 0.0 collective-permute-done.2.w3_ref
  104.4 0.0 copy-start.3
  104.4 5.8 %collective-permute-done.1.w2_ref = bf16[512,512]{1,0:T(8,128)(2,1)S(1)} collective-permute-done((bf16[512,512]{1,0:T(8,128)(2,1)S(1)}, bf16[512,512]{1,0:T(8,128)(2,1)S(1)}, u32[]{:S(2)}, u32[]{:S(2)}) %collective-permute-start.1) | collective-permute-done | bytes 524320 | tf_op jit(solution)/shard_map/ppermute | solution.py:47
  110.3 0.0 copy-done.5
  110.3 0.0 copy-done.6
  110.3 0.0 copy-done.2
  110.3 0.0 copy-done.3
  110.3 4.3 %shard_map.148 = (bf16[256,128]{1,0:T(8,128)(2,1)}, bf16[256,128]{1,0:T(8,128)(2,1)}, bf16[256,256]{1,0:T(8,128)(2,1)}, f32[2,256,128]{2,1,0:T(8,128)}, f32[256,128]{1,0:T(8,128)}) custom-call(bf16[512,896]{1,0:T(8,128)(2,1)} %copy-done.1, bf16[512,896]{1,0:T(8,128)(2,1)} %copy-done.2, bf16[512,512]{1,0:T(8,128)(2,1)S(1)} %collective-permute-done.1.w2_ref, ...), custom_call_target="tpu_custom_call" | custom-call | flops 5000000000 | tf_op jit(solution)/shard_map/pallas_call | solution.py:299
  114.6 4.1 %collective-permute-done.5.w2_ref = bf16[512,384]{1,0:T(8,128)(2,1)S(1)} collective-permute-done((bf16[512,384]{1,0:T(8,128)(2,1)S(1)}, bf16[512,384]{1,0:T(8,128)(2,1)S(1)}, u32[]{:S(2)}, u32[]{:S(2)}) %collective-permute-start.5) | collective-permute-done | bytes 393248 | tf_op jit(solution)/shard_map/ppermute | solution.py:47
  118.7 0.0 copy-start.4
  118.7 0.0 all-to-all-done.2.got_ref
  118.7 0.7 copy-done.4
  119.5 4.0 %shard_map.149 = (bf16[4,32,2048]{2,1,0:T(8,128)(2,1)S(1)}, bf16[4,32,2048]{2,1,0:T(8,128)(2,1)S(1)}) custom-call(bf16[16,136,128]{2,1,0:T(8,128)(2,1)S(1)} %all-to-all-done.2.got_ref, f32[2,128,128]{2,1,0:T(8,128)} %bitcast.12, f32[2,1,128]{2,1,0:T(1,128)} %bitcast.17, f32[256,128]{1,0:T(8,128)} %get-tuple-element.40.cols_ref, ...), custom_call_target="tpu_custom_call" | custom-call | flops 2000000000 | tf_op jit(solution)/shard_map/pallas_call | solution.py:299
  123.4 18.1 %collective-permute-start.6 = (bf16[4,32,2048]{2,1,0:T(8,128)(2,1)S(1)}, bf16[4,32,2048]{2,1,0:T(8,128)(2,1)S(1)}, u32[]{:S(2)}, u32[]{:S(2)}) collective-permute-start(bf16[4,32,2048]{2,1,0:T(8,128)(2,1)S(1)} %get-tuple-element.58), channel_id=1, source_target_pairs={{0,1},{1,0},{2,3},{3,2},{4,5},{5,4},{6,7},{7,6},{8,9},{9,8},{10,11... | collective-permute-start | bytes 1572872 | tf_op jit(solution)/shard_map/ppermute | solution.py:403
  141.6 1.5 collective-permute-done.6
  143.1 0.1 add_convert_fusion
  143.2 12.4 %all_to_all.20 = bf16[4,32,2048]{2,1,0:T(8,128)(2,1)S(1)} all-to-all(bf16[4,32,2048]{2,1,0:T(8,128)(2,1)S(1)} %add_convert_fusion), channel_id=1, replica_groups={{0,2,4,6},{1,3,5,7},{8,10,12,14},{9,11,13,15},{16,18,20,22},{17,19,21,2..., dimensions={0} | all-to-all | bytes 1048576 | tf_op jit(solution)/shard_map/all_to_all | solution.py:406
  155.7 0.7 reduce_sum.12
  (3 shorter events, 0.1 us)
Async XLA Ops:
  1.5 53.4 %all-to-all-start = ((bf16[16,32,256]{2,1,0:T(8,128)(2,1)}), bf16[16,32,256]{2,1,0:T(8,128)(2,1)S(1)}, u32[]{:S(2)}, u32[]{:S(2)}) async-start(bf16[16,32,256]{2,1,0:T(8,128)(2,1)} %get-tuple-element.37), calls=%async_computation | async-start | bytes 524288 | tf_op jit(solution)/shard_map/all_to_all | solution.py:335
  17.3 0.7 copy-start
  56.0 13.9 %all-to-all-start.1 = ((bf16[4,512,256]{2,1,0:T(8,128)(2,1)}), bf16[4,512,256]{2,1,0:T(8,128)(2,1)S(1)}, u32[]{:S(2)}, u32[]{:S(2)}) async-start(bf16[4,512,256]{2,1,0:T(8,128)(2,1)} %broadcast_in_dim.8), calls=%async_computation.1 | async-start | bytes 2097152 | tf_op jit(solution)/shard_map/all_to_all | solution.py:26
  60.3 35.7 %copy-start.1 = (bf16[512,896]{1,0:T(8,128)(2,1)}, bf16[512,896]{1,0:T(8,128)(2,1)S(1)}, u32[]{:S(2)}) copy-start(bf16[512,896]{1,0:T(8,128)(2,1)S(1)} %pad_maximum_fusion.w0_ref) | copy-start | bytes 2752516
  73.0 45.7 %all-to-all-start.2 = ((bf16[16,136,128]{2,1,0:T(8,128)(2,1)}), bf16[16,136,128]{2,1,0:T(8,128)(2,1)S(1)}, u32[]{:S(2)}, u32[]{:S(2)}) async-start(bf16[16,136,128]{2,1,0:T(8,128)(2,1)} %get-tuple-element.44), calls=%async_computation.2 | async-start | bytes 1114112 | tf_op jit(solution)/shard_map/all_to_all | solution.py:372
  82.9 21.5 %collective-permute-start = (bf16[512,896]{1,0:T(8,128)(2,1)S(1)}, bf16[512,896]{1,0:T(8,128)(2,1)S(1)}, u32[]{:S(2)}, u32[]{:S(2)}) collective-permute-start(bf16[512,896]{1,0:T(8,128)(2,1)S(1)} %pad_maximum_fusion.w0_ref), channel_id=1, source_target_pairs={{0,8},{8,16},{16,24},{24,0},{1,9},{9,17},{17,25},{25,1},{2,10},{10... | collective-permute-start | bytes 2752520 | tf_op jit(solution)/shard_map/ppermute | solution.py:47
  85.1 19.3 %collective-permute-start.2 = (bf16[512,896]{1,0:T(8,128)(2,1)S(1)}, bf16[512,896]{1,0:T(8,128)(2,1)S(1)}, u32[]{:S(2)}, u32[]{:S(2)}) collective-permute-start(bf16[512,896]{1,0:T(8,128)(2,1)S(1)} %pad_maximum_fusion.w0_ref), channel_id=1, source_target_pairs={{0,24},{8,0},{16,8},{24,16},{1,25},{9,1},{17,9},{25,17},{2,26},{10... | collective-permute-start | bytes 2752520 | tf_op jit(solution)/shard_map/ppermute | solution.py:47
  89.5 20.8 %collective-permute-start.1 = (bf16[512,512]{1,0:T(8,128)(2,1)S(1)}, bf16[512,512]{1,0:T(8,128)(2,1)S(1)}, u32[]{:S(2)}, u32[]{:S(2)}) collective-permute-start(bf16[512,512]{1,0:T(8,128)(2,1)S(1)} %slice.14), channel_id=1, source_target_pairs={{0,16},{8,24},{16,0},{24,8},{1,17},{9,25},{17,1},{25,9},{2,18},{10... | collective-permute-start | bytes 1572872 | tf_op jit(solution)/shard_map/ppermute | solution.py:47
  91.4 5.7 %collective-permute-start.3 = (bf16[8,2048]{1,0:T(8,128)(2,1)S(1)}, bf16[8,2048]{1,0:T(8,128)(2,1)S(1)}, u32[]{:S(2)}, u32[]{:S(2)}) collective-permute-start(bf16[8,2048]{1,0:T(8,128)(2,1)S(1)} %get-tuple-element.48), channel_id=1, source_target_pairs={{0,32},{32,64},{64,96},{96,128},{128,160},{160,192},{192,224},{224... | collective-permute-start | bytes 98312 | tf_op jit(solution)/shard_map/ppermute | solution.py:364
  94.7 9.7 %collective-permute-start.4 = (bf16[8,2048]{1,0:T(8,128)(2,1)S(1)}, bf16[8,2048]{1,0:T(8,128)(2,1)S(1)}, u32[]{:S(2)}, u32[]{:S(2)}) collective-permute-start(bf16[8,2048]{1,0:T(8,128)(2,1)S(1)} %get-tuple-element.49), channel_id=1, source_target_pairs={{32,0},{64,32},{96,64},{128,96},{160,128},{192,160},{224,192},{256... | collective-permute-start | bytes 98312 | tf_op jit(solution)/shard_map/ppermute | solution.py:365
  97.1 13.1 %copy-start.5 = (bf16[8,2048]{1,0:T(8,128)(2,1)}, bf16[8,2048]{1,0:T(8,128)(2,1)S(1)}, u32[]{:S(2)}) copy-start(bf16[8,2048]{1,0:T(8,128)(2,1)S(1)} %collective-permute-done.3.lo_ref) | copy-start | bytes 98308
  97.1 21.6 %collective-permute-start.5 = (bf16[512,384]{1,0:T(8,128)(2,1)S(1)}, bf16[512,384]{1,0:T(8,128)(2,1)S(1)}, u32[]{:S(2)}, u32[]{:S(2)}) collective-permute-start(bf16[512,384]{1,0:T(8,128)(2,1)S(1)} %slice.15), channel_id=1, source_target_pairs={{0,16},{8,24},{16,0},{24,8},{1,17},{9,25},{17,1},{25,9},{2,18},{10... | collective-permute-start | bytes 1179656 | tf_op jit(solution)/shard_map/ppermute | solution.py:47
  104.4 5.9 %copy-start.6 = (bf16[8,2048]{1,0:T(8,128)(2,1)}, bf16[8,2048]{1,0:T(8,128)(2,1)S(1)}, u32[]{:S(2)}) copy-start(bf16[8,2048]{1,0:T(8,128)(2,1)S(1)} %collective-permute-done.4.hi_ref) | copy-start | bytes 98308
  104.4 5.9 %copy-start.2 = (bf16[512,896]{1,0:T(8,128)(2,1)}, bf16[512,896]{1,0:T(8,128)(2,1)S(1)}, u32[]{:S(2)}) copy-start(bf16[512,896]{1,0:T(8,128)(2,1)S(1)} %collective-permute-done.w1_ref) | copy-start | bytes 2752516
  104.4 5.9 %copy-start.3 = (bf16[512,896]{1,0:T(8,128)(2,1)}, bf16[512,896]{1,0:T(8,128)(2,1)S(1)}, u32[]{:S(2)}) copy-start(bf16[512,896]{1,0:T(8,128)(2,1)S(1)} %collective-permute-done.2.w3_ref) | copy-start | bytes 2752516
  118.7 0.8 copy-start.4
  123.4 19.6 %collective-permute-start.6 = (bf16[4,32,2048]{2,1,0:T(8,128)(2,1)S(1)}, bf16[4,32,2048]{2,1,0:T(8,128)(2,1)S(1)}, u32[]{:S(2)}, u32[]{:S(2)}) collective-permute-start(bf16[4,32,2048]{2,1,0:T(8,128)(2,1)S(1)} %get-tuple-element.58), channel_id=1, source_target_pairs={{0,1},{1,0},{2,3},{3,2},{4,5},{5,4},{6,7},{7,6},{8,9},{9,8},{10,11... | collective-permute-start | bytes 1572872 | tf_op jit(solution)/shard_map/ppermute | solution.py:403
